TPU v7x, 512 devices: a whole 4x8x8 slice. The times are simulated.
512 devices in a mesh: sp: 128 (over z, y, core), tp: 4 (over x).
Axes of the slice: x: 4, y: 8, z: 8, core: 2. Of those that a mesh axis runs over, the one named last changes fastest.
Arguments:
- tokens: bfloat16 [32768, 2048], P(('sp', 'tp')), may hold values from -16 to 16
- w_query: bfloat16 [2048, 1024], P(None, 'tp'), may hold values from -1 to 1
- w_key: bfloat16 [2048, 256], P(None, 'tp'), may hold values from -1 to 1
- w_value: bfloat16 [2048, 256], P(None, 'tp'), may hold values from -0.125 to 0.125
- w_gate: bfloat16 [2048, 16], P(None, 'tp'), may hold values from -0.125 to 0.125
- gate_bias: float32 [16], P('tp'), as said below
- w_output: bfloat16 [1024, 2048], P('tp'), may hold values from -0.1875 to 0.1875
Outputs:
- mixed: bfloat16 [32768, 2048], P(('sp', 'tp'))
Inputs may be any that keep to these rules, and one draw needn't show every extreme that they name: `gate_bias`: each head's forget gate bias is 4 or more; there is no upper bound.
All inputs are finite; a program needn't handle non-finite values.
Results may differ from a plain program's by a relative error of at most 0.012.
The roundings to bfloat16 on the way count: a program that leaves them out, or rounds other values in their place, can miss the bound.
Values may be sent and summed in bfloat16 or wider, within the bound.
No kernel may reach another device: no remote copies, remote signals or barrier semaphores. Data moves between devices by JAX's collectives and lax.ppermute only.
A program may use at most 64 MiB of HBM per device.

v0:
```python
import math

import jax
import jax.numpy as jnp
from jax import lax
from jax.sharding import Mesh
from jax.sharding import PartitionSpec as P

HEAD = 64
SP = ("sp_0", "sp_1", "sp_2")
SP_TP = ("sp_0", "sp_1", "sp_2", "tp")


masked_value = -1e30


def copy_for_each(value, axis):
    copies = jnp.broadcast_to(value, (lax.axis_size(axis), *value.shape))
    return lax.all_to_all(copies, axis, split_axis=0, concat_axis=0, tiled=True)


def in_order(pieces, dim):
    lengths = list(pieces.shape[1:])
    lengths[dim] *= pieces.shape[0]
    return jnp.moveaxis(pieces, 0, dim).reshape(lengths)


def collect(value, axis, dim):
    pieces = copy_for_each(value, axis)
    return in_order(pieces, dim)


def all_blocks(value, axes, sequence):
    pieces = value
    for k in sequence:
        pieces = lax.all_gather(pieces, axes[k])
    done = sequence[::-1]
    back = [done.index(k) for k in range(len(axes))]
    pieces = pieces.transpose(*back, *range(len(axes), pieces.ndim))
    return pieces.reshape(-1, *value.shape)


def whole_of(value, axes, sequence, dim):
    return in_order(all_blocks(value, axes, sequence), dim)


def in_blocks(value, dim, count):
    lengths = value.shape
    pieces = value.reshape(*lengths[:dim], count, lengths[dim] // count, *lengths[dim + 1 :])
    return jnp.moveaxis(pieces, dim, 0)


def sum_at_owner(value, axis, dim):
    pieces = in_blocks(value, dim, lax.axis_size(axis))
    arrived = lax.all_to_all(pieces, axis, split_axis=0, concat_axis=0, tiled=True)
    return arrived.astype(jnp.float32).sum(axis=0)


def softmax_update(
    carry_state,
    query_here,
    query_cumul,
    query_position,
    key_here,
    value_here,
    key_cumul,
    key_position,
):
    row_peak, row_mass, row_accum = carry_state
    scores = jnp.einsum(
        "kgtd,skd->kgts", query_here, key_here, preferred_element_type=jnp.float32
    ) * HEAD ** (-0.5)
    scores = scores + query_cumul[:, :, :, None] - key_cumul[:, :, None, :]
    allowed = key_position[None, :] <= query_position[:, None]
    scores = jnp.where(allowed, scores, masked_value)
    new_peak = jnp.maximum(row_peak, jnp.max(scores, axis=3))
    weights = jnp.where(allowed, jnp.exp(scores - new_peak[:, :, :, None]), 0.0)
    rescale = jnp.exp(row_peak - new_peak)
    row_mass = row_mass * rescale + jnp.sum(weights, axis=3)
    row_accum = row_accum * rescale[:, :, :, None] + jnp.einsum(
        "kgts,skd->kgtd",
        weights.astype(jnp.bfloat16),
        value_here,
        preferred_element_type=jnp.float32,
    )
    return (new_peak, row_mass, row_accum)


def shards(tokens, w_query, w_key, w_value, w_gate, gate_bias, w_output):
    sp_count = lax.axis_size(SP)
    sp_rank = lax.axis_index(SP)
    query_cols = w_query.shape[1]
    key_cols = w_key.shape[1]
    heads_here = w_gate.shape[1]
    kv_heads_here = key_cols // HEAD
    group_size = heads_here // kv_heads_here
    joined = jnp.concatenate([w_query, w_key, w_value, w_gate], axis=1)
    projected = jnp.dot(
        collect(tokens, "tp", 0), joined, preferred_element_type=jnp.float32
    ).astype(jnp.bfloat16)
    local_rows = projected.shape[0]
    half_rows = local_rows // 2
    second_block = 2 * sp_rank + 1
    own_gates = jax.nn.log_sigmoid(
        projected[:, query_cols + 2 * key_cols :].astype(jnp.float32) + gate_bias
    )
    totals = jnp.sum(own_gates.reshape(2, half_rows, heads_here), axis=1)
    all_totals = whole_of(totals[None], (("sp_0", "sp_1"), "sp_2"), (0, 1), 0)
    ordered = all_totals.reshape(2 * sp_count, heads_here)
    prefix_sums = jnp.cumsum(ordered, axis=0) - ordered
    queries = (
        projected[:, :query_cols]
        .reshape(2, half_rows, kv_heads_here, group_size, HEAD)
        .transpose(0, 2, 3, 1, 4)
    )
    query_blocks = (2 * sp_rank, second_block)
    query_cumul = []
    query_position = []
    for side_index in range(2):
        base_value = lax.dynamic_index_in_dim(
            prefix_sums, query_blocks[side_index], 0, keepdims=False
        )
        cumul_rows = base_value[None, :] + jnp.cumsum(
            own_gates[side_index * half_rows : (side_index + 1) * half_rows], axis=0
        )
        query_cumul.append(
            cumul_rows.reshape(half_rows, kv_heads_here, group_size).transpose(1, 2, 0)
        )
        query_position.append(
            query_blocks[side_index] * half_rows + jnp.arange(half_rows, dtype=jnp.int32)
        )
    initial = (
        jnp.full((2, kv_heads_here, group_size, half_rows), masked_value, jnp.float32),
        jnp.zeros((2, kv_heads_here, group_size, half_rows), jnp.float32),
        jnp.zeros((2, kv_heads_here, group_size, half_rows, HEAD), jnp.float32),
    )
    gathered = lax.all_gather(projected[:, query_cols:], SP, axis=0, tiled=True)
    row_count = gathered.shape[0]
    piece_blocks = row_count // half_rows
    per_step = math.gcd(piece_blocks, max(1, 1024 // half_rows))
    step_rows = per_step * half_rows
    step_count = row_count // step_rows
    first_row = half_rows * jnp.arange(piece_blocks, dtype=jnp.int32)
    owner_rank = first_row // local_rows
    half_index = first_row % local_rows // half_rows
    block_ids = 2 * owner_rank + half_index
    gate_logs = jax.nn.log_sigmoid(gathered[:, 2 * key_cols :].astype(jnp.float32) + gate_bias)
    gate_logs = gate_logs.reshape(piece_blocks, half_rows, heads_here)
    base_values = jnp.take(prefix_sums, block_ids, axis=0)
    key_cumul_all = (base_values[:, None, :] + jnp.cumsum(gate_logs, axis=1)).reshape(
        row_count, kv_heads_here, group_size
    )
    key_position_all = (
        block_ids[:, None] * half_rows + jnp.arange(half_rows, dtype=jnp.int32)[None, :]
    ).reshape(row_count)
    earliest = jnp.min(block_ids.reshape(step_count, per_step), axis=1)

    def one_step(step_index, inner_state):
        start_row = step_index * step_rows
        block_rows = lax.dynamic_slice_in_dim(gathered, start_row, step_rows, 0)
        key_here = block_rows[:, :key_cols].reshape(step_rows, kv_heads_here, HEAD)
        value_here = block_rows[:, key_cols : 2 * key_cols].reshape(step_rows, kv_heads_here, HEAD)
        key_cumul = lax.dynamic_slice_in_dim(key_cumul_all, start_row, step_rows, 0).transpose(
            1, 2, 0
        )
        key_position = lax.dynamic_slice_in_dim(key_position_all, start_row, step_rows, 0)
        first_id = earliest[step_index]
        results = []
        for side_index in range(2):
            head_state = tuple((member[side_index] for member in inner_state))

            def compute(head_state, side_index=side_index):
                return softmax_update(
                    head_state,
                    queries[side_index],
                    query_cumul[side_index],
                    query_position[side_index],
                    key_here,
                    value_here,
                    key_cumul,
                    key_position,
                )

            head_state = lax.cond(
                first_id <= query_blocks[side_index],
                compute,
                lambda unchanged: unchanged,
                head_state,
            )
            results.append(head_state)
        return tuple((jnp.stack([results[0][member], results[1][member]]) for member in range(3)))

    row_peak, row_mass, row_accum = lax.fori_loop(0, step_count, one_step, initial)
    attended = (row_accum / row_mass[:, :, :, :, None]).astype(jnp.bfloat16)
    attended = attended.transpose(0, 3, 1, 2, 4).reshape(local_rows, heads_here * HEAD)
    mixed = sum_at_owner(
        jnp.dot(attended, w_output, preferred_element_type=jnp.float32).astype(jnp.bfloat16),
        "tp",
        0,
    )
    return mixed.astype(jnp.bfloat16)


def solution(mesh):
    finer = Mesh(mesh.devices.reshape(8, 8, 2, mesh.shape["tp"]), ("sp_0", "sp_1", "sp_2", "tp"))
    placed = (
        P(SP_TP, None),
        P(None, "tp"),
        P(None, "tp"),
        P(None, "tp"),
        P(None, "tp"),
        P("tp"),
        P("tp", None),
    )
    return jax.shard_map(
        shards, mesh=finer, in_specs=placed, out_specs=P(SP_TP, None), check_vma=False
    )
```

profile of v0, /device:TPU:504, one launch (start us, length us, event | category | flops | bytes accessed | tf_op | source)
XLA Modules:
  0.0 388.9 jit_solution(7107253783128811441)
XLA Ops:
  8.7 4.3 %all-to-all-start = ((bf16[4,64,2048]{2,1,0:T(8,128)(2,1)}), bf16[4,64,2048]{2,1,0:T(8,128)(2,1)S(1)}, u32[]{:S(2)}, u32[]{:S(2)}) async-start(bf16[4,64,2048]{2,1,0:T(8,128)(2,1)} %broadcast_in_dim.67), calls=%async_computation | async-start | bytes 2097152 | tf_op jit(solution)/shard_map/all_to_all | solution.py:19
  14.7 13.4 %all-to-all-done = bf16[4,64,2048]{2,1,0:T(8,128)(2,1)S(1)} async-done(((bf16[4,64,2048]{2,1,0:T(8,128)(2,1)}), bf16[4,64,2048]{2,1,0:T(8,128)(2,1)S(1)}, u32[]{:S(2)}, u32[]{:S(2)}) %all-to-all-start) | async-done | bytes 1048608 | tf_op jit(solution)/shard_map/all_to_all | solution.py:19
  28.1 2.5 fusion.47
  31.9 47.2 %all-gather.2 = f32[64,2,4]{2,1,0:T(2,128)S(1)} all-gather(f32[1,2,4]{2,1,0:T(2,128)S(1)} %bitcast.213), channel_id=2, replica_groups=mesh['sp_0'=8,'sp_1'=8,'sp_2'=2,'tp'=4] {'sp_0','sp_1'}, dimensions={0}, use_global_device_ids=true | all-gather | bytes 2080 | tf_op jit(solution)/shard_map/all_gather | solution.py:36
  84.7 35.0 %all-gather.5.cloned.1.call-done = bf16[32768,132]{0,1:T(8,128)(2,1)} async-done(((bf16[256,132]{0,1:T(8,128)(2,1)}), bf16[32768,132]{0,1:T(8,128)(2,1)}) %all-gather.5.cloned.1.call-update) | async-done | bytes 8650768 | tf_op jit(solution)/shard_map/all_gather | solution.py:137
  122.7 238.2 %while.18 = (s32[]{:T(128)}, f32[2,1,4,128]{3,2,1,0:T(4,128)S(1)}, f32[2,1,4,128]{3,2,1,0:T(4,128)S(1)}, f32[2,1,4,128,64]{3,4,2,1,0:T(8,128)S(1)}, s32[32]{0:T(...) while((s32[]{:T(128)}, f32[2,1,4,128]{3,2,1,0:T(4,128)S(1)}, ...), condition=%wide.region_16.17_spmd.clone, body=%wide.region_7.16_spmd.clone.sunk | while | flops 280433920 | bytes 16568903 | solution.py:193
  125.1 2.2 conditional.6
  127.9 2.2 conditional.7
  132.5 2.2 conditional.6
  135.4 2.2 conditional.7
  140.0 2.2 conditional.6
  142.8 2.2 conditional.7
  147.4 2.2 conditional.6
  150.2 2.2 conditional.7
  157.7 2.2 conditional.7
  162.3 2.2 conditional.6
  165.1 2.2 conditional.7
  172.6 2.2 conditional.7
  177.2 2.2 conditional.6
  180.0 2.2 conditional.7
  187.5 2.2 conditional.7
  192.1 2.2 conditional.6
  194.9 2.2 conditional.7
  202.4 2.2 conditional.7
  207.0 2.2 conditional.6
  209.8 2.2 conditional.7
  217.2 2.2 conditional.7
  221.8 2.2 conditional.6
  224.7 2.2 conditional.7
  232.1 2.2 conditional.7
  239.6 2.2 conditional.7
  247.0 2.2 conditional.7
  254.5 2.2 conditional.7
  261.9 2.2 conditional.7
  269.4 2.2 conditional.7
  276.8 2.2 conditional.7
  284.2 2.2 conditional.7
  291.7 2.2 conditional.7
  299.1 2.2 conditional.7
  306.6 2.2 conditional.7
  314.0 2.2 conditional.7
  321.5 2.2 conditional.7
  328.9 2.2 conditional.7
  336.4 2.2 conditional.7
  343.8 2.2 conditional.7
  351.2 2.2 conditional.7
  358.7 2.2 conditional.7
  361.6 19.5 %all_to_all.10 = bf16[4,64,2048]{2,1,0:T(8,128)(2,1)S(1)} all-to-all(bf16[4,64,2048]{2,1,0:T(8,128)(2,1)S(1)} %bitcast.197), channel_id=1, replica_groups=mesh['sp_0'=8,'sp_1'=8,'sp_2'=2,'tp'=4] {'tp'}, dimensions={0} | all-to-all | bytes 2097152 | tf_op jit(solution)/shard_map/all_to_all | solution.py:55
  (891 shorter events, 255.7 us)
Async XLA Ops:
  6.5 354.6 %copy-start = (bf16[256,2048]{1,0:T(8,128)(2,1)S(1)}, bf16[256,2048]{1,0:T(8,128)(2,1)}, u32[]{:S(2)}) copy-start(bf16[256,2048]{1,0:T(8,128)(2,1)} %param.19) | copy-start | bytes 3145732
  6.5 6.5 %copy-start.3 = (bf16[2048,4]{0,1:T(4,128)(2,1)S(1)}, bf16[2048,4]{0,1:T(4,128)(2,1)}, u32[]{:S(2)}) copy-start(bf16[2048,4]{0,1:T(4,128)(2,1)} %param.17) | copy-start | bytes 49156
  6.5 7.6 %copy-start.1 = (bf16[2048,64]{0,1:T(8,128)(2,1)S(1)}, bf16[2048,64]{0,1:T(8,128)(2,1)}, u32[]{:S(2)}) copy-start(bf16[2048,64]{0,1:T(8,128)(2,1)} %param.16) | copy-start | bytes 786436
  6.5 7.8 %copy-start.2 = (bf16[2048,64]{0,1:T(8,128)(2,1)S(1)}, bf16[2048,64]{0,1:T(8,128)(2,1)}, u32[]{:S(2)}) copy-start(bf16[2048,64]{0,1:T(8,128)(2,1)} %param.15) | copy-start | bytes 786436
  8.7 19.4 %all-to-all-start = ((bf16[4,64,2048]{2,1,0:T(8,128)(2,1)}), bf16[4,64,2048]{2,1,0:T(8,128)(2,1)S(1)}, u32[]{:S(2)}, u32[]{:S(2)}) async-start(bf16[4,64,2048]{2,1,0:T(8,128)(2,1)} %broadcast_in_dim.67), calls=%async_computation | async-start | bytes 2097152 | tf_op jit(solution)/shard_map/all_to_all | solution.py:19
  13.0 106.7 %all-gather.5.cloned.1.call-start = ((), (), s32[]{:S(2)}) async-start(), calls=%async_computation.2 | async-start | bytes 8982528 | tf_op jit(solution)/shard_map/all_gather | solution.py:137
  28.1 3.5 copy-start.4
Sparse Core Ops, SparseCore 0:
  31.4 88.1 all-gather.4
where the time goes:
time: 390 us; the launch traced here: 389 us
  matrix products  91.4 us (23%)
  blocking collectives  68.7 us (18%)
  local copies, waits for them, and re-layouts  59.3 us (15%)
  other arithmetic  55.4 us (14%)
  waiting for transfers between devices  48.4 us (12%)
  loops' own time  47.7 us (12%)
  between operations  13.7 us (4%)
  starting transfers between devices  4.29 us (1%)
    all_gather x2, blocking collectives, all_blocks(): pieces = lax.all_gather(pieces, axes[k])  49.1 us
    dot_general x64, matrix products, softmax_update(): jnp.einsum('kgtd,skd->kgts', query_here, key_here, preferred_element_type...  48.9 us
    another operation x1, loops' own time, shards(): lax.fori_loop(0, step_count, one_step, initial)  45.3 us
    dot_general x64, matrix products, softmax_update(): jnp.einsum('kgts,skd->kgtd', weights.astype(jnp.bfloat16), value_here, pr...  39.5 us
    reduce_sum x64, other arithmetic, softmax_update(): row_mass = row_mass * rescale + jnp.sum(weights, axis=3)  37.9 us
    all_gather x1, waiting for transfers between devices, shards(): gathered = lax.all_gather(projected[:, query_cols:], SP, axis=0, tiled=True)  35 us
    reshape x32, local copies, waits for them, and re-layouts, one_step(): block_rows[:, key_cols:2 * key_cols].reshape(step_rows, kv_heads_here, HEAD)  31.8 us
    all_to_all x1, blocking collectives, sum_at_owner(): lax.all_to_all(pieces, axis, split_axis=0, concat_axis=0, tiled=True)  19.5 us
  transfers between devices with their start and end apart: 2, of which 2 were waited for; matrix products, arithmetic and copies ran while one was open for 1% of the time, Pallas kernels for 0%

commit v1 on v0

v1 whole, which is shorter than its diff:
```python
import functools
import jax, jax.numpy as jnp
from jax import lax
from jax.experimental import pallas as pl
from jax.experimental.pallas import tpu as pltpu
from jax.sharding import Mesh
from jax.sharding import PartitionSpec as P

f32, bf16 = jnp.float32, jnp.bfloat16
HEAD = 64
NEG = -1e30

def split3(x):
    a = x.astype(bf16).astype(f32)
    r = x - a
    b = r.astype(bf16).astype(f32)
    c = (r - b).astype(bf16).astype(f32)
    return a, b, c

def log_sigmoid(u):
    x = jnp.exp(-jnp.abs(u))
    series = x * (1 - x * (1 / 2 - x * (1 / 3 - x * (1 / 4 - x * (1 / 5 - x * (1 / 6 - x * (1 / 7)))))))
    return jnp.minimum(u, 0.0) - jnp.where(x < 0.0625, series, jnp.log(1 + x))

def dot(a, b):
    return jnp.dot(a, b, preferred_element_type=f32)

def attend_kernel(info, kv, q, bias, acc_out, ml_out, cum, aug, rhs, acc, ml, *, chips, blk):
    core, low, high, low_side = info[0], info[1], info[2], info[3]
    rows = chips * 8
    gates = kv[:, 128:136, :].astype(f32) + bias[...][None, :, :1]
    logs = log_sigmoid(gates).reshape(rows, blk)
    tri = (lax.broadcasted_iota(jnp.int32, (blk, blk), 0) <= lax.broadcasted_iota(jnp.int32, (blk, blk), 1)).astype(bf16)
    inner = sum(dot(p.astype(bf16), tri) for p in split3(logs))
    r0 = lax.broadcasted_iota(jnp.int32, (rows, rows), 0)
    r1 = lax.broadcasted_iota(jnp.int32, (rows, rows), 1)
    before = ((r1 < r0) & (((r0 - r1) & 3) == 0)).astype(bf16)
    last = jnp.broadcast_to(inner[:, blk - 1:], (rows, blk))
    outer = sum(dot(before, p.astype(bf16)) for p in split3(last))
    total = (inner + outer).reshape(chips, 8, blk)
    cum[...] = total
    own = jnp.where(core == 0, total[:, :4], total[:, 4:])
    parts = split3(-own)
    ones = jnp.ones((chips, 4, blk), f32)
    aug[...] = jnp.concatenate([*parts, ones], axis=1).astype(bf16)
    row16 = lax.broadcasted_iota(jnp.int32, (16, blk), 0)
    for side in range(2):
        which = low_side if side == 0 else 1 - low_side
        chip = low if side == 0 else high
        here = cum[chip]
        here = jnp.where(which == 0, here[:4], here[4:])
        pa, pb, pc = split3(here)
        for h in range(4):
            tail = jnp.where((row16 < 12) & ((row16 & 3) == h), 1.0, 0.0)
            tail = jnp.where(row16 == 12, pa[h:h + 1], tail)
            tail = jnp.where(row16 == 13, pb[h:h + 1], tail)
            tail = jnp.where(row16 == 14, pc[h:h + 1], tail)
            qh = q[which, h * HEAD:(h + 1) * HEAD, :].astype(f32) * 0.125
            rhs[side * 4 + h] = jnp.concatenate([qh, tail, jnp.zeros((48, blk), f32)], axis=0).astype(bf16)
    acc[...] = jnp.zeros_like(acc)
    ml[0:8] = jnp.full((8, blk), NEG, f32)
    ml[8:16] = jnp.zeros((8, blk), f32)
    zeros = jnp.zeros((48, blk), bf16)

    def tile(jj, sides):
        lhs, vals = [], []
        for e in range(2):
            j = 2 * jj + e
            lhs.append(jnp.concatenate([kv[j, 0:64, :], aug[j], zeros], axis=0).T)
            vals.append(kv[j, 64:128, :])
        keys = jnp.concatenate(lhs, axis=0)
        for side, masked in sides:
            if masked:
                which = low_side if side == 0 else 1 - low_side
                chip = low if side == 0 else high
                qpos = (2 * chip + which) * blk + lax.broadcasted_iota(jnp.int32, (2 * blk, blk), 1)
                row = lax.broadcasted_iota(jnp.int32, (2 * blk, blk), 0)
                kpos = row + (row // blk) * blk + (4 * jj + core) * blk
                allowed = kpos <= qpos
            for h in range(4):
                u = side * 4 + h
                s = dot(keys, rhs[u])
                if masked:
                    s = jnp.where(allowed, s, NEG)
                m_old = ml[u:u + 1]
                m_new = jnp.maximum(m_old, jnp.max(s, axis=0, keepdims=True))
                p = jnp.exp(s - m_new)
                if masked:
                    p = jnp.where(allowed, p, 0.0)
                scale = jnp.exp(m_old - m_new)
                ml[u:u + 1] = m_new
                ml[8 + u:9 + u] = ml[8 + u:9 + u] * scale + jnp.sum(p, axis=0, keepdims=True)
                pb = p.astype(bf16)
                out = dot(vals[0], pb[:blk]) + dot(vals[1], pb[blk:])
                acc[u * HEAD:(u + 1) * HEAD] = acc[u * HEAD:(u + 1) * HEAD] * scale + out

    def both(jj, _):
        tile(jj, ((0, False), (1, False)))
        return _

    def one(jj, _):
        tile(jj, ((1, False),))
        return _

    lax.fori_loop(0, low // 2, both, 0)
    tile(low // 2, ((0, True), (1, False)))
    lax.fori_loop(low // 2 + 1, high // 2, one, 0)
    tile(high // 2, ((1, True),))
    for side in range(2):
        which = low_side if side == 0 else 1 - low_side
        acc_out[which] = acc[side * 256:(side + 1) * 256]
        ml_out[which] = jnp.concatenate([ml[side * 4:side * 4 + 4], ml[8 + side * 4:12 + side * 4]], axis=0)

def attend(info, kv, q, bias8, interpret=False):
    chips, _, blk = kv.shape
    vm = pl.BlockSpec(memory_space=pltpu.VMEM)
    return pl.pallas_call(
        functools.partial(attend_kernel, chips=chips, blk=blk),
        out_shape=(jax.ShapeDtypeStruct((2, 256, blk), f32), jax.ShapeDtypeStruct((2, 8, blk), f32)),
        in_specs=[pl.BlockSpec(memory_space=pltpu.SMEM), vm, vm, vm],
        out_specs=(vm, vm),
        scratch_shapes=[pltpu.VMEM((chips, 8, blk), f32), pltpu.VMEM((chips, 16, blk), bf16),
                        pltpu.VMEM((8, 128, blk), bf16), pltpu.VMEM((512, blk), f32), pltpu.VMEM((16, blk), f32)],
        compiler_params=pltpu.CompilerParams(vmem_limit_bytes=48 * 1024 * 1024),
        interpret=interpret, name='attend',
    )(info, kv, q, bias8)


SP = ("sp_0", "sp_1", "sp_2")
SP_TP = ("sp_0", "sp_1", "sp_2", "tp")


def sum_at_owner(value):
    pieces = value.reshape(4, value.shape[0] // 4, value.shape[1])
    arrived = lax.all_to_all(pieces, "tp", split_axis=0, concat_axis=0, tiled=True)
    return arrived.astype(f32).sum(axis=0)


def shards(tokens, w_query, w_key, w_value, w_gate, gate_bias, w_output):
    rows, cols = lax.axis_size("sp_0"), lax.axis_size("sp_1")
    chips = rows * cols
    core = lax.axis_index("sp_2")
    chip = lax.axis_index("sp_0") * cols + lax.axis_index("sp_1")
    other = chips - 1 - chip
    copies = jnp.broadcast_to(tokens, (4, *tokens.shape))
    here = lax.all_to_all(copies, "tp", split_axis=0, concat_axis=0, tiled=True)
    here = here.reshape(-1, tokens.shape[1])
    joined = jnp.concatenate([w_query, w_key, w_value, w_gate], axis=1)
    projected = lax.dot_general(joined, here, (((0,), (1,)), ((), ())), preferred_element_type=f32).astype(bf16)
    query = projected[:256]
    gates = projected[384:388]
    swapped = lax.ppermute(gates, "sp_2", [(0, 1), (1, 0)])
    first = jnp.where(core == 0, gates, swapped)
    second = jnp.where(core == 0, swapped, gates)
    payload = jnp.concatenate([projected[256:384], first, second], axis=0)
    blk = payload.shape[1]
    spread = jnp.broadcast_to(payload, (cols, *payload.shape))
    row = lax.all_to_all(spread, "sp_1", split_axis=0, concat_axis=0, tiled=True)
    kv = lax.all_gather(row, "sp_0").reshape(chips, 136, blk)
    moves = []
    for c in range(chips):
        moves.append((2 * c, 2 * c + 1))
        moves.append((2 * c + 1, 2 * (chips - 1 - c)))
    arrived = lax.ppermute(query, SP, moves)
    far = [(2 * c + 1, 2 * (chips - 1 - c) + 1) for c in range(chips)]
    crossed = lax.ppermute(query, SP, far)
    q = jnp.stack([jnp.where(core == 0, query, arrived), jnp.where(core == 0, arrived, crossed)])
    info = jnp.stack([core, jnp.minimum(chip, other), jnp.maximum(chip, other), (chip > other).astype(jnp.int32)])
    bias8 = jnp.broadcast_to(jnp.tile(gate_bias, 2)[:, None], (8, 128))
    acc, ml = attend(info.astype(jnp.int32), kv, q, bias8)
    state = jnp.concatenate([acc, ml], axis=1)
    give = lax.dynamic_index_in_dim(state, 1 - core, 0, keepdims=False)
    keep = lax.dynamic_index_in_dim(state, core, 0, keepdims=False)
    got = lax.ppermute(give, "sp_2", [(0, 1), (1, 0)])
    peak = jnp.maximum(keep[256:260], got[256:260])
    wa, wb = jnp.exp(keep[256:260] - peak), jnp.exp(got[256:260] - peak)
    mass = keep[260:264] * wa + got[260:264] * wb
    accum = keep[:256].reshape(4, 64, blk) * wa[:, None] + got[:256].reshape(4, 64, blk) * wb[:, None]
    attended = (accum / mass[:, None]).astype(bf16).reshape(256, blk)
    returned = lax.ppermute(attended, SP, far)
    attended = jnp.where(core == 0, attended, returned)
    partial = lax.dot_general(attended, w_output, (((0,), (0,)), ((), ())), preferred_element_type=f32).astype(bf16)
    return sum_at_owner(partial).astype(bf16)


def solution(mesh):
    finer = Mesh(mesh.devices.reshape(8, 8, 2, mesh.shape["tp"]), SP_TP)
    placed = (P(SP_TP, None), P(None, "tp"), P(None, "tp"), P(None, "tp"), P(None, "tp"), P("tp"), P("tp", None))
    return jax.shard_map(shards, mesh=finer, in_specs=placed, out_specs=P(SP_TP, None), check_vma=False)
```

time: 390 us -> 221 us (0.57)
  the two profiles are of different devices: /device:TPU:504 before, /device:TPU:9 now
where the time goes in v1:
time: 221 us; the launch traced here: 220 us
  waiting for transfers between devices  63.6 us (29%)
  Pallas kernels  61.1 us (28%)
  blocking collectives  35.3 us (16%)
  starting transfers between devices  33.7 us (15%)
  between operations  13.6 us (6%)
  local copies, waits for them, and re-layouts  8.98 us (4%)
  matrix products  3.04 us (1%)
    pallas_call x1, Pallas kernels, attend(): pl.pallas_call(functools.partial(attend_kernel, chips=chips, blk=blk), ou...  61.1 us
    all_gather x1, waiting for transfers between devices, shards(): kv = lax.all_gather(row, 'sp_0').reshape(chips, 136, blk)  38.8 us
    all_to_all x1, blocking collectives, shards(): lax.all_to_all(spread, 'sp_1', split_axis=0, concat_axis=0, tiled=True)  21.8 us
    ppermute x1, starting transfers between devices, shards(): arrived = lax.ppermute(query, SP, moves)  14.5 us
    all_to_all x1, blocking collectives, sum_at_owner(): lax.all_to_all(pieces, 'tp', split_axis=0, concat_axis=0, tiled=True)  13.5 us
    all_to_all x1, waiting for transfers between devices, shards(): here = lax.all_to_all(copies, 'tp', split_axis=0, concat_axis=0, tiled=True)  9.93 us
    ppermute x1, waiting for transfers between devices, shards(): crossed = lax.ppermute(query, SP, far)  8.81 us
    ppermute x1, starting transfers between devices, shards(): returned = lax.ppermute(attended, SP, far)  6.81 us
  transfers between devices with their start and end apart: 7, of which 6 were waited for; matrix products, arithmetic and copies ran while one was open for 2% of the time, Pallas kernels for 0%

profile of v1, /device:TPU:9, one launch (start us, length us, event | category | flops | bytes accessed | tf_op | source)
XLA Modules:
  0.0 220.4 jit_solution(17240139780302067883)
XLA Ops:
  6.5 0.0 copy-start
  6.5 2.1 broadcast_in_dim.16
  8.7 4.0 %all-to-all-start = ((bf16[4,64,2048]{2,1,0:T(8,128)(2,1)}), bf16[4,64,2048]{2,1,0:T(8,128)(2,1)S(1)}, u32[]{:S(2)}, u32[]{:S(2)}) async-start(bf16[4,64,2048]{2,1,0:T(8,128)(2,1)} %broadcast_in_dim.16), calls=%async_computation | async-start | bytes 2097152 | tf_op jit(solution)/shard_map/all_to_all | solution.py:146
  12.7 0.0 all-gather.3.cloned.1.call-start
  12.7 1.8 copy.13
  14.5 1.2 copy.12
  15.7 1.2 copy.11
  17.0 9.9 %all-to-all-done = bf16[4,64,2048]{2,1,0:T(8,128)(2,1)S(1)} async-done(((bf16[4,64,2048]{2,1,0:T(8,128)(2,1)}), bf16[4,64,2048]{2,1,0:T(8,128)(2,1)S(1)}, u32[]{:S(2)}, u32[]{:S(2)}) %all-to-all-start) | async-done | bytes 1048608 | tf_op jit(solution)/shard_map/all_to_all | solution.py:146
  26.9 0.0 copy-start.2
  26.9 2.6 %fusion.8 = bf16[388,256]{1,0:T(8,128)(2,1)S(1)} fusion(bf16[256,2048]{1,0:T(8,128)(2,1)S(1)} %bitcast.49, bf16[2048,4]{1,0:T(8,128)(2,1)} %copy.13, bf16[2048,64]{1,0:T(8,128)(2,1)S(1)} %copy.12, bf16[2048,64]{1,0:T(8,128)(2,1)S(1)} %copy.11, bf16[2048,256]{1,0:T(8,128)(2,1)} %param.8), kind=kOutput, calls=%fused_computation.9 | convolution fusion | flops 413303808 | bytes 2836480 | tf_op jit(solution)/shard_map/dot_general | solution.py:149
  29.5 3.7 %collective-permute-start = (bf16[4,256]{1,0:T(4,128)(2,1)S(1)}, bf16[4,256]{1,0:T(4,128)(2,1)S(1)}, u32[]{:S(2)}, u32[]{:S(2)}) collective-permute-start(bf16[4,256]{1,0:T(4,128)(2,1)S(1)} %slice.48), channel_id=1, source_target_pairs={{0,4},{4,0},{1,5},{5,1},{2,6},{6,2},{3,7},{7,3},{8,12},{12,8},{9,1... | collective-permute-start | bytes 6152 | tf_op jit(solution)/shard_map/ppermute | solution.py:152
  33.3 0.8 collective-permute-done
  34.1 21.8 %all_to_all.15 = bf16[8,136,256]{2,1,0:T(8,128)(2,1)} all-to-all(bf16[8,136,256]{2,1,0:T(8,128)(2,1)S(1)} %broadcast_in_dim.17), channel_id=1, replica_groups=mesh['sp_0'=8,'sp_1'=8,'sp_2'=2,'tp'=4] {'sp_1'}, dimensions={0} | all-to-all | bytes 1114112 | tf_op jit(solution)/shard_map/all_to_all | solution.py:158
  55.9 0.0 all-gather.3.cloned.1.call-update
  55.9 14.5 %collective-permute-start.1 = (bf16[256,256]{1,0:T(8,128)(2,1)S(1)}, bf16[256,256]{1,0:T(8,128)(2,1)S(1)}, u32[]{:S(2)}, u32[]{:S(2)}) collective-permute-start(bf16[256,256]{1,0:T(8,128)(2,1)S(1)} %slice.49), channel_id=1, source_target_pairs={{0,4},{4,504},{8,12},{12,496},{16,20},{20,488},{24,28},{28,480},{3... | collective-permute-start | bytes 393224 | tf_op jit(solution)/shard_map/ppermute | solution.py:164
  70.4 1.9 collective-permute-start.2
  72.3 0.0 copy-done.2
  72.4 0.1 broadcast_in_dim.18
  72.5 0.1 pad_add_fusion.info
  72.5 0.0 collective-permute-done.1
  72.5 8.8 %collective-permute-done.2 = bf16[256,256]{1,0:T(8,128)(2,1)S(1)} collective-permute-done((bf16[256,256]{1,0:T(8,128)(2,1)S(1)}, bf16[256,256]{1,0:T(8,128)(2,1)S(1)}, u32[]{:S(2)}, u32[]{:S(2)}) %collective-permute-start.2) | collective-permute-done | bytes 131104 | tf_op jit(solution)/shard_map/ppermute | solution.py:166
  81.4 38.8 %all-gather.3.cloned.1.call-done.kv = bf16[64,136,256]{2,1,0:T(8,128)(2,1)} async-done(((bf16[8,136,256]{2,1,0:T(8,128)(2,1)}), bf16[64,136,256]{2,1,0:T(8,128)(2,1)}) %all-gather.3.cloned.1.call-update) | async-done | bytes 4456464 | tf_op jit(solution)/shard_map/all_gather | solution.py:159
  120.2 0.1 broadcast_in_dim.19.bias
  120.3 0.0 copy-start.1
  120.3 2.3 %copy-done.1 = bf16[64,136,256]{2,1,0:T(8,128)(2,1)S(1)} copy-done((bf16[64,136,256]{2,1,0:T(8,128)(2,1)S(1)}, bf16[64,136,256]{2,1,0:T(8,128)(2,1)}, u32[]{:S(2)}) %copy-start.1) | copy-done | bytes 4456472
  122.6 61.1 %attend.1 = (f32[2,256,256]{2,1,0:T(8,128)S(1)}, f32[2,8,256]{2,1,0:T(8,128)S(1)}) custom-call(s32[4]{0:T(128)S(1)} %pad_add_fusion.info, bf16[64,136,256]{2,1,0:T(8,128)(2,1)S(1)} %copy-done.1, bf16[2,256,256]{2,1,0:T(8,128)(2,1)S(1)} %pad_maximum_fusion.q, f32[8,128]{1,0:T(8,128)S(1)} %broadcast_in_dim.19.bias), custom_call_target="tpu_custom_call" | custom-call | tf_op jit(solution)/shard_map/attend/pallas_call | solution.py:117
  183.8 2.8 %collective-permute-start.3 = (f32[264,256]{1,0:T(8,128)S(1)}, f32[264,256]{1,0:T(8,128)S(1)}, u32[]{:S(2)}, u32[]{:S(2)}) collective-permute-start(f32[264,256]{1,0:T(8,128)S(1)} %dynamic-slice_bitcast_fusion), channel_id=1, source_target_pairs={{0,4},{4,0},{1,5},{5,1},{2,6},{6,2},{3,7},{7,3},{8,12},{12,8},{9,1... | collective-permute-start | bytes 811016 | tf_op jit(solution)/shard_map/ppermute | solution.py:174
  186.5 1.2 collective-permute-done.3
  187.7 0.1 fusion.14
  187.8 6.8 %collective-permute-start.4 = (bf16[256,256]{1,0:T(8,128)(2,1)S(1)}, bf16[256,256]{1,0:T(8,128)(2,1)S(1)}, u32[]{:S(2)}, u32[]{:S(2)}) collective-permute-start(bf16[256,256]{1,0:T(8,128)(2,1)S(1)} %fusion.14), channel_id=1, source_target_pairs={{4,508},{12,500},{20,492},{28,484},{36,476},{44,468},{52,460},{60,... | collective-permute-start | bytes 393224 | tf_op jit(solution)/shard_map/ppermute | solution.py:180
  194.6 4.1 %collective-permute-done.4 = bf16[256,256]{1,0:T(8,128)(2,1)S(1)} collective-permute-done((bf16[256,256]{1,0:T(8,128)(2,1)S(1)}, bf16[256,256]{1,0:T(8,128)(2,1)S(1)}, u32[]{:S(2)}, u32[]{:S(2)}) %collective-permute-start.4) | collective-permute-done | bytes 131104 | tf_op jit(solution)/shard_map/ppermute | solution.py:180
  198.7 0.0 copy-done
  198.7 0.5 convolution_convert_fusion
  199.1 13.5 %all_to_all.16 = bf16[4,64,2048]{2,1,0:T(8,128)(2,1)S(1)} all-to-all(bf16[4,64,2048]{2,1,0:T(8,128)(2,1)S(1)} %bitcast.48), channel_id=1, replica_groups=mesh['sp_0'=8,'sp_1'=8,'sp_2'=2,'tp'=4] {'tp'}, dimensions={0} | all-to-all | bytes 2097152 | tf_op jit(solution)/shard_map/all_to_all | solution.py:135
  212.7 0.9 reduce_sum.12
  (13 shorter events, 0.2 us)
Async XLA Ops:
  6.5 192.1 %copy-start = (bf16[256,2048]{1,0:T(8,128)(2,1)S(1)}, bf16[256,2048]{1,0:T(8,128)(2,1)}, u32[]{:S(2)}) copy-start(bf16[256,2048]{1,0:T(8,128)(2,1)} %param.13) | copy-start | bytes 3145732
  8.7 18.3 %all-to-all-start = ((bf16[4,64,2048]{2,1,0:T(8,128)(2,1)}), bf16[4,64,2048]{2,1,0:T(8,128)(2,1)S(1)}, u32[]{:S(2)}, u32[]{:S(2)}) async-start(bf16[4,64,2048]{2,1,0:T(8,128)(2,1)} %broadcast_in_dim.16), calls=%async_computation | async-start | bytes 2097152 | tf_op jit(solution)/shard_map/all_to_all | solution.py:146
  12.7 107.6 %all-gather.3.cloned.1.call-start = ((), (), s32[]{:S(2)}) async-start(), calls=%async_computation.3 | async-start | bytes 5013504 | tf_op jit(solution)/shard_map/all_gather | solution.py:159
  26.9 45.4 %copy-start.2 = (f32[4]{0:T(128)S(1)}, f32[4]{0:T(128)}, u32[]{:S(2)}) copy-start(f32[4]{0:T(128)} %param.12) | copy-start | bytes 52
  29.5 4.5 %collective-permute-start = (bf16[4,256]{1,0:T(4,128)(2,1)S(1)}, bf16[4,256]{1,0:T(4,128)(2,1)S(1)}, u32[]{:S(2)}, u32[]{:S(2)}) collective-permute-start(bf16[4,256]{1,0:T(4,128)(2,1)S(1)} %slice.48), channel_id=1, source_target_pairs={{0,4},{4,0},{1,5},{5,1},{2,6},{6,2},{3,7},{7,3},{8,12},{12,8},{9,1... | collective-permute-start | bytes 6152 | tf_op jit(solution)/shard_map/ppermute | solution.py:152
  55.9 16.6 %collective-permute-start.1 = (bf16[256,256]{1,0:T(8,128)(2,1)S(1)}, bf16[256,256]{1,0:T(8,128)(2,1)S(1)}, u32[]{:S(2)}, u32[]{:S(2)}) collective-permute-start(bf16[256,256]{1,0:T(8,128)(2,1)S(1)} %slice.49), channel_id=1, source_target_pairs={{0,4},{4,504},{8,12},{12,496},{16,20},{20,488},{24,28},{28,480},{3... | collective-permute-start | bytes 393224 | tf_op jit(solution)/shard_map/ppermute | solution.py:164
  70.4 10.9 %collective-permute-start.2 = (bf16[256,256]{1,0:T(8,128)(2,1)S(1)}, bf16[256,256]{1,0:T(8,128)(2,1)S(1)}, u32[]{:S(2)}, u32[]{:S(2)}) collective-permute-start(bf16[256,256]{1,0:T(8,128)(2,1)S(1)} %slice.49), channel_id=1, source_target_pairs={{4,508},{12,500},{20,492},{28,484},{36,476},{44,468},{52,460},{60,... | collective-permute-start | bytes 393224 | tf_op jit(solution)/shard_map/ppermute | solution.py:166
  120.3 2.3 %copy-start.1 = (bf16[64,136,256]{2,1,0:T(8,128)(2,1)S(1)}, bf16[64,136,256]{2,1,0:T(8,128)(2,1)}, u32[]{:S(2)}) copy-start(bf16[64,136,256]{2,1,0:T(8,128)(2,1)} %all-gather.3.cloned.1.call-done.kv) | copy-start | bytes 13369348
  183.8 3.9 %collective-permute-start.3 = (f32[264,256]{1,0:T(8,128)S(1)}, f32[264,256]{1,0:T(8,128)S(1)}, u32[]{:S(2)}, u32[]{:S(2)}) collective-permute-start(f32[264,256]{1,0:T(8,128)S(1)} %dynamic-slice_bitcast_fusion), channel_id=1, source_target_pairs={{0,4},{4,0},{1,5},{5,1},{2,6},{6,2},{3,7},{7,3},{8,12},{12,8},{9,1... | collective-permute-start | bytes 811016 | tf_op jit(solution)/shard_map/ppermute | solution.py:174
  187.8 10.9 %collective-permute-start.4 = (bf16[256,256]{1,0:T(8,128)(2,1)S(1)}, bf16[256,256]{1,0:T(8,128)(2,1)S(1)}, u32[]{:S(2)}, u32[]{:S(2)}) collective-permute-start(bf16[256,256]{1,0:T(8,128)(2,1)S(1)} %fusion.14), channel_id=1, source_target_pairs={{4,508},{12,500},{20,492},{28,484},{36,476},{44,468},{52,460},{60,... | collective-permute-start | bytes 393224 | tf_op jit(solution)/shard_map/ppermute | solution.py:180
Sparse Core Ops, SparseCore 0:
  56.0 64.1 all-gather.2

commit v2 on v1

v2 whole, which is shorter than its diff:
```python
import functools
import jax, jax.numpy as jnp
from jax import lax
from jax.experimental import pallas as pl
from jax.experimental.pallas import tpu as pltpu
from jax.sharding import Mesh
from jax.sharding import PartitionSpec as P

f32, bf16 = jnp.float32, jnp.bfloat16
HEAD = 64
NEG = -1e30
LOW = -1e20

def split3(x):
    a = x.astype(bf16).astype(f32)
    r = x - a
    b = r.astype(bf16).astype(f32)
    return a, b, r - b

def log_sigmoid(u):
    x = jnp.exp(-jnp.abs(u))
    series = x * (1 - x * (1 / 2 - x * (1 / 3 - x * (1 / 4 - x * (1 / 5 - x * (1 / 6 - x * (1 / 7)))))))
    return jnp.minimum(u, 0.0) - jnp.where(x < 0.0625, series, jnp.log(1 + x))

def dot(a, b):
    return jnp.dot(a, b, preferred_element_type=f32)

def attend_kernel(*refs, count, chips, blk):
    info, q, bias = refs[:3]
    kvs = refs[3:3 + count]
    acc, stat, tot = refs[3 + count:6 + count]
    aug, rhs, keys, scores, tops = refs[6 + count:]
    core = info[0]
    rows = chips * 8
    tri = (lax.broadcasted_iota(jnp.int32, (blk, blk), 0) <= lax.broadcasted_iota(jnp.int32, (blk, blk), 1)).astype(bf16)
    r0 = lax.broadcasted_iota(jnp.int32, (rows, rows), 0)
    r1 = lax.broadcasted_iota(jnp.int32, (rows, rows), 1)
    before = ((r1 < r0) & (((r0 - r1) & 3) == 0)).astype(bf16)
    row16 = lax.broadcasted_iota(jnp.int32, (16, blk), 0)
    for side in range(2):
        for h in range(4):
            mark = jnp.where((row16 < 12) & ((row16 & 3) == h), 1.0, 0.0).astype(bf16)
            qh = q[side, h * HEAD:(h + 1) * HEAD, :] * jnp.asarray(0.125, bf16)
            rhs[side * 4 + h] = jnp.concatenate([qh, mark, jnp.zeros((48, blk), bf16)], axis=0)
    zeros = jnp.zeros((48, blk), bf16)
    for n in range(count):
        kv = kvs[n]
        gates = kv[:, 128:136, :].astype(f32) + bias[...][None, :, :1]
        logs = log_sigmoid(gates).reshape(rows, blk)
        inner = sum(dot(p.astype(bf16), tri) for p in split3(logs))
        last = jnp.broadcast_to(inner[:, blk - 1:], (rows, blk))
        outer = sum(dot(before, p.astype(bf16)) for p in split3(last))
        total = (inner + outer).reshape(chips, 8, blk)
        own = jnp.where(core == 0, total[:, :4], total[:, 4:])
        tot[n] = jnp.broadcast_to(total[chips - 1][:, blk - 1:], (8, 128))
        aug[...] = jnp.concatenate([*split3(-own), jnp.zeros((chips, 4, blk), f32)], axis=1).astype(bf16)
        acc[n] = jnp.zeros((2, 256, blk), f32)
        for side in range(2):
            stat[n, side, 0:32] = jnp.zeros((32, blk), f32)
            stat[n, side, 32:64] = jnp.full((32, blk), LOW, f32)
        first = info[3 + n] * chips
        rel = [info[1] - first, info[2] - first]
        full = [jnp.clip(x, 0, chips) // 2 for x in rel]
        steps = full[0] + full[1]

        def place(it):
            side = (it >= full[0]).astype(jnp.int32)
            return side, jnp.minimum(it - side * full[0], chips // 2 - 1)

        def load_keys(slot, jj):
            for e in range(2):
                keys[slot, e * blk:(e + 1) * blk] = jnp.concatenate([kv[2 * jj + e, 0:64, :], aug[2 * jj + e], zeros], axis=0).T

        def score(slot, key_slot, side, h, allowed=None):
            s = dot(keys[key_slot], rhs[side * 4 + h])
            if allowed is not None:
                s = jnp.where(allowed, s, NEG)
            scores[slot] = s
            tops[slot] = jnp.max(s.reshape(2 * blk // 8, 8, blk), axis=0)

        def soften(slot, jj, side, h):
            old = stat[n, side, 32 + 8 * h:40 + 8 * h]
            new = jnp.maximum(old, jnp.max(tops[slot], axis=0, keepdims=True))
            scale = jnp.exp(old - new)
            mass = stat[n, side, 8 * h:8 * h + 8] * scale
            out = jnp.zeros((64, blk), f32)
            for e in range(2):
                s = scores[slot, e * blk:(e + 1) * blk].reshape(blk // 8, 8, blk)
                p = jnp.exp(s - new[None])
                mass = mass + jnp.sum(p, axis=0)
                out = out + dot(kv[2 * jj + e, 64:128, :], p.reshape(blk, blk).astype(bf16))
            stat[n, side, 8 * h:8 * h + 8] = mass
            stat[n, side, 32 + 8 * h:40 + 8 * h] = new
            a = acc[n, side, h * HEAD:(h + 1) * HEAD].reshape(8, 8, blk) * scale[None]
            acc[n, side, h * HEAD:(h + 1) * HEAD] = a.reshape(64, blk) + out

        @pl.when(steps > 0)
        def _():
            side, jj = place(0)
            load_keys(0, jj)
            score(0, 0, side, 0)

            def body(it, carry):
                slot = it & 1
                side, jj = place(it)
                side_next, jj_next = place(jnp.minimum(it + 1, steps - 1))
                load_keys(1 - slot, jj_next)
                for h in range(4):
                    if h < 3:
                        score((h + 1) & 1, slot, side, h + 1)
                    else:
                        score(0, 1 - slot, side_next, 0)
                    soften(h & 1, jj, side, h)
                return carry

            lax.fori_loop(0, steps, body, 0)

        def edge(side, carry):
            where = jnp.where(side == 0, rel[0], rel[1])

            @pl.when((where >= 0) & (where < chips))
            def _():
                jj = jnp.clip(where, 0, chips - 1) // 2
                par = jnp.where(side == 0, info[7], 1 - info[7])
                qpos = (2 * where + par) * blk + lax.broadcasted_iota(jnp.int32, (2 * blk, blk), 1)
                row = lax.broadcasted_iota(jnp.int32, (2 * blk, blk), 0)
                kpos = row + (row // blk) * blk + (4 * jj + core) * blk
                allowed = kpos <= qpos
                load_keys(0, jj)
                score(0, 0, side, 0, allowed)
                for h in range(4):
                    if h < 3:
                        score((h + 1) & 1, 0, side, h + 1, allowed)
                    soften(h & 1, jj, side, h)

            return carry

        lax.fori_loop(0, 2, edge, 0)

def attend_chunks(info, q, bias8, kvs):
    count = len(kvs)
    chips, _, blk = kvs[0].shape
    vm = pl.BlockSpec(memory_space=pltpu.VMEM)
    return pl.pallas_call(
        functools.partial(attend_kernel, count=count, chips=chips, blk=blk),
        out_shape=(jax.ShapeDtypeStruct((count, 2, 256, blk), f32), jax.ShapeDtypeStruct((count, 2, 64, blk), f32),
                   jax.ShapeDtypeStruct((count, 8, 128), f32)),
        in_specs=[pl.BlockSpec(memory_space=pltpu.SMEM), vm, vm] + [vm] * count,
        out_specs=(vm, vm, vm),
        scratch_shapes=[pltpu.VMEM((chips, 16, blk), bf16), pltpu.VMEM((8, 128, blk), bf16),
                        pltpu.VMEM((2, 2 * blk, 128), bf16), pltpu.VMEM((2, 2 * blk, blk), f32), pltpu.VMEM((2, 8, blk), f32)],
        compiler_params=pltpu.CompilerParams(vmem_limit_bytes=32 * 1024 * 1024),
    )(info, q, bias8, *kvs)

def merge_kernel(*refs, counts):
    info = refs[0]
    k = len(counts)
    accs, stats, tots = refs[1:1 + k], refs[1 + k:1 + 2 * k], refs[1 + 2 * k:1 + 3 * k]
    keep, give = refs[1 + 3 * k:]
    flat = [(i, n) for i in range(k) for n in range(counts[i])]
    rows = [info[2 + j] for j in range(len(flat))]
    base = []
    for j in range(len(flat)):
        b = jnp.zeros((4, 128), f32)
        for j2, (i2, n2) in enumerate(flat):
            if j2 != j:
                b = b + jnp.where(rows[j2] < rows[j], tots[i2][n2, 4:8], 0.0)
        base.append(b[:, :1])
    for which in range(2):
        dst = keep if which == 0 else give
        side = info[which]
        for h in range(4):
            tops = [stats[i][n, side, 32 + 8 * h:40 + 8 * h] - base[j][h:h + 1] for j, (i, n) in enumerate(flat)]
            top = functools.reduce(jnp.maximum, tops)
            w = [jnp.exp(t - top) for t in tops]
            mass = sum(stats[i][n, side, 8 * h:8 * h + 8] * w[j] for j, (i, n) in enumerate(flat))
            dst[256 + h:257 + h] = top[:1]
            dst[260 + h:261 + h] = jnp.sum(mass, axis=0, keepdims=True)
            tot = None
            for j, (i, n) in enumerate(flat):
                a = accs[i][n, side, h * HEAD:(h + 1) * HEAD].reshape(8, 8, 256) * w[j][None]
                tot = a if tot is None else tot + a
            dst[h * HEAD:(h + 1) * HEAD] = tot.reshape(HEAD, 256)

def merge(info, parts):
    counts = [p[0].shape[0] for p in parts]
    vm = pl.BlockSpec(memory_space=pltpu.VMEM)
    shape = jax.ShapeDtypeStruct((264, 256), f32)
    return pl.pallas_call(
        functools.partial(merge_kernel, counts=counts), out_shape=(shape, shape),
        in_specs=[pl.BlockSpec(memory_space=pltpu.SMEM)] + [vm] * (3 * len(parts)), out_specs=(vm, vm),
        compiler_params=pltpu.CompilerParams(vmem_limit_bytes=32 * 1024 * 1024), name='merge',
    )(info, *[p[0] for p in parts], *[p[1] for p in parts], *[p[2] for p in parts])

def finish_kernel(keep, got, out):
    peak = jnp.maximum(keep[256:260], got[256:260])
    wa, wb = jnp.exp(keep[256:260] - peak), jnp.exp(got[256:260] - peak)
    mass = keep[260:264] * wa + got[260:264] * wb
    for h in range(4):
        s = slice(h * HEAD, (h + 1) * HEAD)
        out[s] = ((keep[s] * wa[h:h + 1] + got[s] * wb[h:h + 1]) / mass[h:h + 1]).astype(bf16)

def finish(keep, got):
    vm = pl.BlockSpec(memory_space=pltpu.VMEM)
    return pl.pallas_call(finish_kernel, out_shape=jax.ShapeDtypeStruct((256, 256), bf16), in_specs=[vm, vm], out_specs=vm,
                          name='finish')(keep, got)


SP = ("sp_0", "sp_1", "sp_2")
SP_TP = ("sp_0", "sp_1", "sp_2", "tp")


def ring(count, step):
    return [(i, (i + step) % count) for i in range(count)]


def sum_at_owner(value):
    pieces = value.reshape(4, value.shape[0] // 4, value.shape[1])
    arrived = lax.all_to_all(pieces, "tp", split_axis=0, concat_axis=0, tiled=True)
    return arrived.astype(f32).sum(axis=0)


def shards(tokens, w_query, w_key, w_value, w_gate, gate_bias, w_output):
    rows, cols = lax.axis_size("sp_0"), lax.axis_size("sp_1")
    chips = rows * cols
    core = lax.axis_index("sp_2")
    row = lax.axis_index("sp_0")
    chip = row * cols + lax.axis_index("sp_1")
    other = chips - 1 - chip
    copies = jnp.broadcast_to(tokens, (4, *tokens.shape))
    here = lax.all_to_all(copies, "tp", split_axis=0, concat_axis=0, tiled=True)
    here = here.reshape(-1, tokens.shape[1])
    joined = jnp.concatenate([w_query, w_gate, w_key, w_value], axis=1)
    projected = lax.dot_general(joined, here, (((0,), (1,)), ((), ())), preferred_element_type=f32).astype(bf16)
    query, gates = projected[:256], projected[256:260]
    swapped = lax.ppermute(projected[:260], "sp_2", [(0, 1), (1, 0)])
    first = jnp.where(core == 0, gates, swapped[256:])
    second = jnp.where(core == 0, swapped[256:], gates)
    payload = jnp.concatenate([projected[260:], first, second], axis=0)
    even = jnp.where(core == 0, query, swapped[:256])
    odd = jnp.where(core == 0, swapped[:256], query)
    far = [(2 * c + e, 2 * (chips - 1 - c) + e) for c in range(chips) for e in range(2)]
    crossed = lax.ppermute(odd, SP, far)
    spread = jnp.broadcast_to(payload, (cols, *payload.shape))
    own = lax.all_to_all(spread, "sp_1", split_axis=0, concat_axis=0, tiled=True)
    own, crossed = lax.optimization_barrier((own, crossed))
    behind = chip > other
    q = jnp.stack([jnp.where(behind, crossed, even), jnp.where(behind, even, crossed)])
    bias8 = jnp.broadcast_to(jnp.tile(gate_bias, 2)[:, None], (8, 128))
    low, high = jnp.minimum(chip, other), jnp.maximum(chip, other)
    low_core = behind.astype(jnp.int32)

    def run(chunks, at):
        at = (list(at) + [jnp.int32(0)] * 4)[:4]
        info = jnp.stack([core, low, high, *at, low_core]).astype(jnp.int32)
        return attend_chunks(info, q, bias8, chunks)

    parts, order = [], []
    up, down = own, own
    pending, where = [own], [row]
    for step in range(1, rows // 2 + 1):
        up = lax.ppermute(up, "sp_0", ring(rows, 1))
        following, places = [up], [(row - step) % rows]
        if 2 * step < rows:
            down = lax.ppermute(down, "sp_0", ring(rows, -1))
            following.append(down)
            places.append((row + step) % rows)
        parts.append(run(pending, where))
        order += where
        pending, where = following, places
    parts.append(run(pending, where))
    order += where
    mine = jnp.where(behind, 1 - core, core)
    keep, give = merge(jnp.stack([mine, 1 - mine, *order]).astype(jnp.int32), parts)
    got = lax.ppermute(give, "sp_2", [(0, 1), (1, 0)])
    attended = finish(keep, got)
    back = [(2 * c + 1, 2 * (chips - 1 - c) + 1) for c in range(chips)]
    returned = lax.ppermute(attended, SP, back)
    attended = jnp.where(core == 0, attended, returned)
    partial = lax.dot_general(attended, w_output, (((0,), (0,)), ((), ())), preferred_element_type=f32).astype(bf16)
    return sum_at_owner(partial).astype(bf16)


def solution(mesh):
    finer = Mesh(mesh.devices.reshape(8, 8, 2, mesh.shape["tp"]), SP_TP)
    placed = (P(SP_TP, None), P(None, "tp"), P(None, "tp"), P(None, "tp"), P(None, "tp"), P("tp"), P("tp", None))

    return jax.shard_map(shards, mesh=finer, in_specs=placed, out_specs=P(SP_TP, None), check_vma=False)
```

time: 221 us -> 195 us (0.88)
  the two profiles are of different devices: /device:TPU:9 before, /device:TPU:1 now
where the time goes in v2:
time: 195 us; the launch traced here: 194 us
  starting transfers between devices  66.4 us (34%)
  waiting for transfers between devices  54.2 us (28%)
  Pallas kernels  47.5 us (24%)
  blocking collectives  12.2 us (6%)
  local copies, waits for them, and re-layouts  8.39 us (4%)
  matrix products  3.28 us (2%)
  other arithmetic  1.99 us (1%)
    pallas_call x5, Pallas kernels, attend_chunks(): pl.pallas_call(functools.partial(attend_kernel, count=count, chips=chips,...  44.7 us
    ppermute x4, waiting for transfers between devices, shards(): up = lax.ppermute(up, 'sp_0', ring(rows, 1))  22.8 us
    ppermute x1, waiting for transfers between devices, shards(): crossed = lax.ppermute(odd, SP, far)  16.6 us
    ppermute x3, starting transfers between devices, shards(): down = lax.ppermute(down, 'sp_0', ring(rows, -1))  13.1 us
    ppermute x1, starting transfers between devices, shards(): crossed = lax.ppermute(odd, SP, far)  13.1 us
    all_to_all x1, blocking collectives, sum_at_owner(): lax.all_to_all(pieces, 'tp', split_axis=0, concat_axis=0, tiled=True)  12.2 us
    ppermute x1, starting transfers between devices, shards(): swapped = lax.ppermute(projected[:260], 'sp_2', [(0, 1), (1, 0)])  8.55 us
    ppermute x4, starting transfers between devices, shards(): up = lax.ppermute(up, 'sp_0', ring(rows, 1))  8.26 us
  transfers between devices with their start and end apart: 13, of which 8 were waited for; matrix products, arithmetic and copies ran while one was open for 2% of the time, Pallas kernels for 20%

profile of v2, /device:TPU:1, one launch (start us, length us, event | category | flops | bytes accessed | tf_op | source)
XLA Modules:
  0.0 194.3 jit_solution(13232702842435905571)
XLA Ops:
  0.0 2.2 %broadcast_in_dim.13 = bf16[4,64,2048]{2,1,0:T(8,128)(2,1)} broadcast(bf16[64,2048]{1,0:T(8,128)(2,1)} %param.7), dimensions={1,2} | broadcast | bytes 1310720 | tf_op jit(solution)/shard_map/broadcast_in_dim | solution.py:230
  2.2 5.0 %all-to-all-start = ((bf16[4,64,2048]{2,1,0:T(8,128)(2,1)}), bf16[4,64,2048]{2,1,0:T(8,128)(2,1)S(1)}, u32[]{:S(2)}, u32[]{:S(2)}) async-start(bf16[4,64,2048]{2,1,0:T(8,128)(2,1)} %broadcast_in_dim.13), calls=%async_computation | async-start | bytes 2097152 | tf_op jit(solution)/shard_map/all_to_all | solution.py:231
  7.1 0.3 copy.10
  7.4 1.2 copy.9
  8.7 1.1 copy.8
  9.7 7.2 %all-to-all-done = bf16[4,64,2048]{2,1,0:T(8,128)(2,1)S(1)} async-done(((bf16[4,64,2048]{2,1,0:T(8,128)(2,1)}), bf16[4,64,2048]{2,1,0:T(8,128)(2,1)S(1)}, u32[]{:S(2)}, u32[]{:S(2)}) %all-to-all-start) | async-done | bytes 1048608 | tf_op jit(solution)/shard_map/all_to_all | solution.py:231
  16.9 2.8 %fusion.8 = bf16[388,256]{1,0:T(8,128)(2,1)S(1)} fusion(bf16[256,2048]{1,0:T(8,128)(2,1)S(1)} %bitcast.23, bf16[2048,64]{1,0:T(8,128)(2,1)S(1)} %copy.10, bf16[2048,64]{1,0:T(8,128)(2,1)S(1)} %copy.9, bf16[2048,4]{1,0:T(8,128)(2,1)} %copy.8, bf16[2048,256]{1,0:T(8,128)(2,1)} %param.8), kind=kOutput, calls=%fused_computation.9 | convolution fusion | flops 413303808 | bytes 2836480 | tf_op jit(solution)/shard_map/dot_general | solution.py:234
  19.7 8.6 %collective-permute-start = (bf16[260,256]{1,0:T(8,128)(2,1)S(1)}, bf16[260,256]{1,0:T(8,128)(2,1)S(1)}, u32[]{:S(2)}, u32[]{:S(2)}) collective-permute-start(bf16[260,256]{1,0:T(8,128)(2,1)S(1)} %slice.28), channel_id=1, source_target_pairs={{0,4},{4,0},{1,5},{5,1},{2,6},{6,2},{3,7},{7,3},{8,12},{12,8},{9,1... | collective-permute-start | bytes 399368 | tf_op jit(solution)/shard_map/ppermute | solution.py:236
  28.3 0.9 collective-permute-done
  29.3 0.9 broadcast_in_dim.14
  30.2 6.5 %all-to-all-start.1 = ((bf16[8,136,256]{2,1,0:T(8,128)(2,1)}), bf16[8,136,256]{2,1,0:T(8,128)(2,1)S(1)}, u32[]{:S(2)}, u32[]{:S(2)}) async-start(bf16[8,136,256]{2,1,0:T(8,128)(2,1)} %broadcast_in_dim.14), calls=%async_computation.1 | async-start | bytes 1114112 | tf_op jit(solution)/shard_map/all_to_all | solution.py:245
  36.7 13.1 %collective-permute-start.1 = (bf16[256,256]{1,0:T(8,128)(2,1)S(1)}, bf16[256,256]{1,0:T(8,128)(2,1)S(1)}, u32[]{:S(2)}, u32[]{:S(2)}) collective-permute-start(bf16[256,256]{1,0:T(8,128)(2,1)S(1)} %broadcast_select_fusion.1), channel_id=1, source_target_pairs={{0,504},{4,508},{8,496},{12,500},{16,488},{20,492},{24,480},{28,48... | collective-permute-start | bytes 393224 | tf_op jit(solution)/shard_map/ppermute | solution.py:243
  49.8 16.6 %collective-permute-done.1 = bf16[256,256]{1,0:T(8,128)(2,1)S(1)} collective-permute-done((bf16[256,256]{1,0:T(8,128)(2,1)S(1)}, bf16[256,256]{1,0:T(8,128)(2,1)S(1)}, u32[]{:S(2)}, u32[]{:S(2)}) %collective-permute-start.1) | collective-permute-done | bytes 131104 | tf_op jit(solution)/shard_map/ppermute | solution.py:243
  66.3 0.7 copy-done.5
  67.0 2.5 %collective-permute-start.2 = (bf16[8,136,256]{2,1,0:T(8,128)(2,1)S(1)}, bf16[8,136,256]{2,1,0:T(8,128)(2,1)S(1)}, u32[]{:S(2)}, u32[]{:S(2)}) collective-permute-start(bf16[8,136,256]{2,1,0:T(8,128)(2,1)S(1)} %all-to-all-done.1.refs_3_), channel_id=1, source_target_pairs={{0,64},{64,128},{128,192},{192,256},{256,320},{320,384},{384,448},... | collective-permute-start | bytes 1671176 | tf_op jit(solution)/shard_map/ppermute | solution.py:262
  69.5 4.0 %collective-permute-start.3 = (bf16[8,136,256]{2,1,0:T(8,128)(2,1)S(1)}, bf16[8,136,256]{2,1,0:T(8,128)(2,1)S(1)}, u32[]{:S(2)}, u32[]{:S(2)}) collective-permute-start(bf16[8,136,256]{2,1,0:T(8,128)(2,1)S(1)} %all-to-all-done.1.refs_3_), channel_id=1, source_target_pairs={{0,448},{64,0},{128,64},{192,128},{256,192},{320,256},{384,320},{4... | collective-permute-start | bytes 1671176 | tf_op jit(solution)/shard_map/ppermute | solution.py:265
  73.5 8.4 %collective-permute-done.2.refs_3_ = bf16[8,136,256]{2,1,0:T(8,128)(2,1)S(1)} collective-permute-done((bf16[8,136,256]{2,1,0:T(8,128)(2,1)S(1)}, bf16[8,136,256]{2,1,0:T(8,128)(2,1)S(1)}, u32[]{:S(2)}, u32[]{:S(2)}) %collective-permute-start.2) | collective-permute-done | bytes 557088 | tf_op jit(solution)/shard_map/ppermute | solution.py:262
  81.9 1.9 collective-permute-start.4
  83.8 4.6 %collective-permute-start.5 = (bf16[8,136,256]{2,1,0:T(8,128)(2,1)S(1)}, bf16[8,136,256]{2,1,0:T(8,128)(2,1)}, u32[]{:S(2)}, u32[]{:S(2)}) collective-permute-start(bf16[8,136,256]{2,1,0:T(8,128)(2,1)S(1)} %collective-permute-done.3.refs_4_), channel_id=1, source_target_pairs={{0,448},{64,0},{128,64},{192,128},{256,192},{320,256},{384,320},{4... | collective-permute-start | bytes 1671176 | tf_op jit(solution)/shard_map/ppermute | solution.py:265
  88.4 7.6 %collective-permute-done.4.refs_3_ = bf16[8,136,256]{2,1,0:T(8,128)(2,1)S(1)} collective-permute-done((bf16[8,136,256]{2,1,0:T(8,128)(2,1)S(1)}, bf16[8,136,256]{2,1,0:T(8,128)(2,1)S(1)}, u32[]{:S(2)}, u32[]{:S(2)}) %collective-permute-start.4) | collective-permute-done | bytes 557088 | tf_op jit(solution)/shard_map/ppermute | solution.py:262
  96.0 1.9 collective-permute-start.6
  97.9 4.6 %collective-permute-start.7 = (bf16[8,136,256]{2,1,0:T(8,128)(2,1)}, bf16[8,136,256]{2,1,0:T(8,128)(2,1)}, u32[]{:S(2)}, u32[]{:S(2)}) collective-permute-start(bf16[8,136,256]{2,1,0:T(8,128)(2,1)} %collective-permute-done.5.refs_4_), channel_id=1, source_target_pairs={{0,448},{64,0},{128,64},{192,128},{256,192},{320,256},{384,320},{4... | collective-permute-start | bytes 1671176 | tf_op jit(solution)/shard_map/ppermute | solution.py:265
  102.5 6.8 %collective-permute-done.6.refs_3_ = bf16[8,136,256]{2,1,0:T(8,128)(2,1)} collective-permute-done((bf16[8,136,256]{2,1,0:T(8,128)(2,1)S(1)}, bf16[8,136,256]{2,1,0:T(8,128)(2,1)}, u32[]{:S(2)}, u32[]{:S(2)}) %collective-permute-start.6) | collective-permute-done | bytes 557088 | tf_op jit(solution)/shard_map/ppermute | solution.py:262
  109.3 1.9 collective-permute-start.8
  111.3 0.1 broadcast_in_dim.15
  111.4 0.1 stack.112.refs_0_
  111.5 0.1 stack.119.refs_0_
  111.6 0.1 stack.116.refs_0_
  111.7 0.1 stack.117.refs_0_
  111.8 0.1 stack.118.refs_0_
  111.9 0.1 stack.106.refs_0_
  111.9 1.0 select_bitcast_fusion.1
  113.1 6.5 %shard_map.73 = (f32[1,2,256,256]{3,2,1,0:T(8,128)S(1)}, f32[1,2,64,256]{3,2,1,0:T(8,128)S(1)}, f32[1,8,128]{2,1,0:T(8,128)S(1)}) custom-call(s32[8]{0:T(128)S(1)} %stack.112.refs_0_, bf16[2,256,256]{2,1,0:T(8,128)(2,1)S(1)} %pad_maximum_fusion.refs_1_, f32[8,128]{1,0:T(8,128)S(1)} %broadcast_in_dim.16.refs_2_, bf16[8,136,256]{2,1,0:T(8,128)(2,1)S(1)} %all-to-all-done.1.refs_3_), custom_call_target="tpu_custom_call" | custom-call | tf_op jit(solution)/shard_map/pallas_call | solution.py:144
  119.5 10.3 %shard_map.74 = (f32[2,2,256,256]{3,2,1,0:T(8,128)S(1)}, f32[2,2,64,256]{3,2,1,0:T(8,128)S(1)}, f32[2,8,128]{2,1,0:T(8,128)S(1)}) custom-call(s32[8]{0:T(128)S(1)} %stack.116.refs_0_, bf16[2,256,256]{2,1,0:T(8,128)(2,1)S(1)} %pad_maximum_fusion.refs_1_, f32[8,128]{1,0:T(8,128)S(1)} %broadcast_in_dim.16.refs_2_, ...), custom_call_target="tpu_custom_call" | custom-call | tf_op jit(solution)/shard_map/pallas_call | solution.py:144
  129.9 11.0 %shard_map.75 = (f32[2,2,256,256]{3,2,1,0:T(8,128)S(1)}, f32[2,2,64,256]{3,2,1,0:T(8,128)S(1)}, f32[2,8,128]{2,1,0:T(8,128)S(1)}) custom-call(s32[8]{0:T(128)S(1)} %stack.117.refs_0_, bf16[2,256,256]{2,1,0:T(8,128)(2,1)S(1)} %pad_maximum_fusion.refs_1_, f32[8,128]{1,0:T(8,128)S(1)} %broadcast_in_dim.16.refs_2_, ...), custom_call_target="tpu_custom_call" | custom-call | tf_op jit(solution)/shard_map/pallas_call | solution.py:144
  140.9 11.0 %shard_map.76 = (f32[2,2,256,256]{3,2,1,0:T(8,128)S(1)}, f32[2,2,64,256]{3,2,1,0:T(8,128)S(1)}, f32[2,8,128]{2,1,0:T(8,128)S(1)}) custom-call(s32[8]{0:T(128)S(1)} %stack.118.refs_0_, bf16[2,256,256]{2,1,0:T(8,128)(2,1)S(1)} %pad_maximum_fusion.refs_1_, f32[8,128]{1,0:T(8,128)S(1)} %broadcast_in_dim.16.refs_2_, ...), custom_call_target="tpu_custom_call" | custom-call | tf_op jit(solution)/shard_map/pallas_call | solution.py:144
  151.9 6.0 %shard_map.77 = (f32[1,2,256,256]{3,2,1,0:T(8,128)S(1)}, f32[1,2,64,256]{3,2,1,0:T(8,128)S(1)}, f32[1,8,128]{2,1,0:T(8,128)S(1)}) custom-call(s32[8]{0:T(128)S(1)} %stack.119.refs_0_, bf16[2,256,256]{2,1,0:T(8,128)(2,1)S(1)} %pad_maximum_fusion.refs_1_, f32[8,128]{1,0:T(8,128)S(1)} %broadcast_in_dim.16.refs_2_, ...), custom_call_target="tpu_custom_call" | custom-call | tf_op jit(solution)/shard_map/pallas_call | solution.py:144
  157.8 1.1 merge.1
  158.9 0.7 copy-done.1
  159.6 6.8 %collective-permute-start.9 = (f32[264,256]{1,0:T(8,128)S(1)}, f32[264,256]{1,0:T(8,128)S(1)}, u32[]{:S(2)}, u32[]{:S(2)}) collective-permute-start(f32[264,256]{1,0:T(8,128)S(1)} %get-tuple-element.42), channel_id=1, source_target_pairs={{0,4},{4,0},{1,5},{5,1},{2,6},{6,2},{3,7},{7,3},{8,12},{12,8},{9,1... | collective-permute-start | bytes 811016 | tf_op jit(solution)/shard_map/ppermute | solution.py:275
  166.5 1.2 collective-permute-done.9.got
  167.6 0.7 copy-done.3
  168.3 1.7 finish.1
  170.1 5.2 %collective-permute-start.10 = (bf16[256,256]{1,0:T(8,128)(2,1)}, bf16[256,256]{1,0:T(8,128)(2,1)S(1)}, u32[]{:S(2)}, u32[]{:S(2)}) collective-permute-start(bf16[256,256]{1,0:T(8,128)(2,1)} %finish.1), channel_id=1, source_target_pairs={{4,508},{12,500},{20,492},{28,484},{36,476},{44,468},{52,460},{60,... | collective-permute-start | bytes 393224 | tf_op jit(solution)/shard_map/ppermute | solution.py:278
  175.2 5.5 %collective-permute-done.10 = bf16[256,256]{1,0:T(8,128)(2,1)S(1)} collective-permute-done((bf16[256,256]{1,0:T(8,128)(2,1)}, bf16[256,256]{1,0:T(8,128)(2,1)S(1)}, u32[]{:S(2)}, u32[]{:S(2)}) %collective-permute-start.10) | collective-permute-done | bytes 131104 | tf_op jit(solution)/shard_map/ppermute | solution.py:278
  180.8 0.5 convolution_convert_fusion
  181.3 12.2 %all_to_all.15 = bf16[4,64,2048]{2,1,0:T(8,128)(2,1)S(1)} all-to-all(bf16[4,64,2048]{2,1,0:T(8,128)(2,1)S(1)} %bitcast.22), channel_id=1, replica_groups=mesh['sp_0'=8,'sp_1'=8,'sp_2'=2,'tp'=4] {'tp'}, dimensions={0} | all-to-all | bytes 2097152 | tf_op jit(solution)/shard_map/all_to_all | solution.py:219
  193.4 0.9 reduce_sum.12
  (27 shorter events, 0.2 us)
Async XLA Ops:
  0.0 180.8 %copy-start = (bf16[256,2048]{1,0:T(8,128)(2,1)S(1)}, bf16[256,2048]{1,0:T(8,128)(2,1)}, u32[]{:S(2)}) copy-start(bf16[256,2048]{1,0:T(8,128)(2,1)} %param.13) | copy-start | bytes 3145732
  2.2 5.0 %copy-start.4 = (bf16[2048,64]{0,1:T(8,128)(2,1)S(1)}, bf16[2048,64]{0,1:T(8,128)(2,1)}, u32[]{:S(2)}) copy-start(bf16[2048,64]{0,1:T(8,128)(2,1)} %param.10) | copy-start | bytes 786436
  2.2 14.7 %all-to-all-start = ((bf16[4,64,2048]{2,1,0:T(8,128)(2,1)}), bf16[4,64,2048]{2,1,0:T(8,128)(2,1)S(1)}, u32[]{:S(2)}, u32[]{:S(2)}) async-start(bf16[4,64,2048]{2,1,0:T(8,128)(2,1)} %broadcast_in_dim.13), calls=%async_computation | async-start | bytes 2097152 | tf_op jit(solution)/shard_map/all_to_all | solution.py:231
  7.1 1.5 copy-start.6
  19.7 9.5 %collective-permute-start = (bf16[260,256]{1,0:T(8,128)(2,1)S(1)}, bf16[260,256]{1,0:T(8,128)(2,1)S(1)}, u32[]{:S(2)}, u32[]{:S(2)}) collective-permute-start(bf16[260,256]{1,0:T(8,128)(2,1)S(1)} %slice.28), channel_id=1, source_target_pairs={{0,4},{4,0},{1,5},{5,1},{2,6},{6,2},{3,7},{7,3},{8,12},{12,8},{9,1... | collective-permute-start | bytes 399368 | tf_op jit(solution)/shard_map/ppermute | solution.py:236
  29.3 7.4 %copy-start.2 = (bf16[260,256]{1,0:T(8,128)(2,1)}, bf16[260,256]{1,0:T(8,128)(2,1)S(1)}, u32[]{:S(2)}) copy-start(bf16[260,256]{1,0:T(8,128)(2,1)S(1)} %collective-permute-done) | copy-start | bytes 399364
  29.3 82.0 %copy-start.7 = (f32[4]{0:T(128)S(1)}, f32[4]{0:T(128)}, u32[]{:S(2)}) copy-start(f32[4]{0:T(128)} %param.12) | copy-start | bytes 52
  30.2 36.8 %all-to-all-start.1 = ((bf16[8,136,256]{2,1,0:T(8,128)(2,1)}), bf16[8,136,256]{2,1,0:T(8,128)(2,1)S(1)}, u32[]{:S(2)}, u32[]{:S(2)}) async-start(bf16[8,136,256]{2,1,0:T(8,128)(2,1)} %broadcast_in_dim.14), calls=%async_computation.1 | async-start | bytes 1114112 | tf_op jit(solution)/shard_map/all_to_all | solution.py:245
  36.7 29.6 %collective-permute-start.1 = (bf16[256,256]{1,0:T(8,128)(2,1)S(1)}, bf16[256,256]{1,0:T(8,128)(2,1)S(1)}, u32[]{:S(2)}, u32[]{:S(2)}) collective-permute-start(bf16[256,256]{1,0:T(8,128)(2,1)S(1)} %broadcast_select_fusion.1), channel_id=1, source_target_pairs={{0,504},{4,508},{8,496},{12,500},{16,488},{20,492},{24,480},{28,48... | collective-permute-start | bytes 393224 | tf_op jit(solution)/shard_map/ppermute | solution.py:243
  66.3 0.7 copy-start.5
  67.0 14.9 %collective-permute-start.2 = (bf16[8,136,256]{2,1,0:T(8,128)(2,1)S(1)}, bf16[8,136,256]{2,1,0:T(8,128)(2,1)S(1)}, u32[]{:S(2)}, u32[]{:S(2)}) collective-permute-start(bf16[8,136,256]{2,1,0:T(8,128)(2,1)S(1)} %all-to-all-done.1.refs_3_), channel_id=1, source_target_pairs={{0,64},{64,128},{128,192},{192,256},{256,320},{320,384},{384,448},... | collective-permute-start | bytes 1671176 | tf_op jit(solution)/shard_map/ppermute | solution.py:262
  69.5 14.3 %collective-permute-start.3 = (bf16[8,136,256]{2,1,0:T(8,128)(2,1)S(1)}, bf16[8,136,256]{2,1,0:T(8,128)(2,1)S(1)}, u32[]{:S(2)}, u32[]{:S(2)}) collective-permute-start(bf16[8,136,256]{2,1,0:T(8,128)(2,1)S(1)} %all-to-all-done.1.refs_3_), channel_id=1, source_target_pairs={{0,448},{64,0},{128,64},{192,128},{256,192},{320,256},{384,320},{4... | collective-permute-start | bytes 1671176 | tf_op jit(solution)/shard_map/ppermute | solution.py:265
  81.9 14.1 %collective-permute-start.4 = (bf16[8,136,256]{2,1,0:T(8,128)(2,1)S(1)}, bf16[8,136,256]{2,1,0:T(8,128)(2,1)S(1)}, u32[]{:S(2)}, u32[]{:S(2)}) collective-permute-start(bf16[8,136,256]{2,1,0:T(8,128)(2,1)S(1)} %collective-permute-done.2.refs_3_), channel_id=1, source_target_pairs={{0,64},{64,128},{128,192},{192,256},{256,320},{320,384},{384,448},... | collective-permute-start | bytes 1671176 | tf_op jit(solution)/shard_map/ppermute | solution.py:262
  83.8 14.1 %collective-permute-start.5 = (bf16[8,136,256]{2,1,0:T(8,128)(2,1)S(1)}, bf16[8,136,256]{2,1,0:T(8,128)(2,1)}, u32[]{:S(2)}, u32[]{:S(2)}) collective-permute-start(bf16[8,136,256]{2,1,0:T(8,128)(2,1)S(1)} %collective-permute-done.3.refs_4_), channel_id=1, source_target_pairs={{0,448},{64,0},{128,64},{192,128},{256,192},{320,256},{384,320},{4... | collective-permute-start | bytes 1671176 | tf_op jit(solution)/shard_map/ppermute | solution.py:265
  96.0 13.3 %collective-permute-start.6 = (bf16[8,136,256]{2,1,0:T(8,128)(2,1)S(1)}, bf16[8,136,256]{2,1,0:T(8,128)(2,1)}, u32[]{:S(2)}, u32[]{:S(2)}) collective-permute-start(bf16[8,136,256]{2,1,0:T(8,128)(2,1)S(1)} %collective-permute-done.4.refs_3_), channel_id=1, source_target_pairs={{0,64},{64,128},{128,192},{192,256},{256,320},{320,384},{384,448},... | collective-permute-start | bytes 1671176 | tf_op jit(solution)/shard_map/ppermute | solution.py:262
  97.9 43.0 %collective-permute-start.7 = (bf16[8,136,256]{2,1,0:T(8,128)(2,1)}, bf16[8,136,256]{2,1,0:T(8,128)(2,1)}, u32[]{:S(2)}, u32[]{:S(2)}) collective-permute-start(bf16[8,136,256]{2,1,0:T(8,128)(2,1)} %collective-permute-done.5.refs_4_), channel_id=1, source_target_pairs={{0,448},{64,0},{128,64},{192,128},{256,192},{320,256},{384,320},{4... | collective-permute-start | bytes 1671176 | tf_op jit(solution)/shard_map/ppermute | solution.py:265
  109.3 42.6 %collective-permute-start.8 = (bf16[8,136,256]{2,1,0:T(8,128)(2,1)}, bf16[8,136,256]{2,1,0:T(8,128)(2,1)}, u32[]{:S(2)}, u32[]{:S(2)}) collective-permute-start(bf16[8,136,256]{2,1,0:T(8,128)(2,1)} %collective-permute-done.6.refs_3_), channel_id=1, source_target_pairs={{0,64},{64,128},{128,192},{192,256},{256,320},{320,384},{384,448},... | collective-permute-start | bytes 1671176 | tf_op jit(solution)/shard_map/ppermute | solution.py:262
  158.9 0.7 copy-start.1
  159.6 8.0 %collective-permute-start.9 = (f32[264,256]{1,0:T(8,128)S(1)}, f32[264,256]{1,0:T(8,128)S(1)}, u32[]{:S(2)}, u32[]{:S(2)}) collective-permute-start(f32[264,256]{1,0:T(8,128)S(1)} %get-tuple-element.42), channel_id=1, source_target_pairs={{0,4},{4,0},{1,5},{5,1},{2,6},{6,2},{3,7},{7,3},{8,12},{12,8},{9,1... | collective-permute-start | bytes 811016 | tf_op jit(solution)/shard_map/ppermute | solution.py:275
  167.6 0.7 copy-start.3
  170.1 10.7 %collective-permute-start.10 = (bf16[256,256]{1,0:T(8,128)(2,1)}, bf16[256,256]{1,0:T(8,128)(2,1)S(1)}, u32[]{:S(2)}, u32[]{:S(2)}) collective-permute-start(bf16[256,256]{1,0:T(8,128)(2,1)} %finish.1), channel_id=1, source_target_pairs={{4,508},{12,500},{20,492},{28,484},{36,476},{44,468},{52,460},{60,... | collective-permute-start | bytes 393224 | tf_op jit(solution)/shard_map/ppermute | solution.py:278

commit v3 on v2

v3 whole, which is shorter than its diff:
```python
import functools
import jax, jax.numpy as jnp
from jax import lax
from jax.experimental import pallas as pl
from jax.experimental.pallas import tpu as pltpu
from jax.sharding import Mesh
from jax.sharding import PartitionSpec as P

f32, bf16 = jnp.float32, jnp.bfloat16
HEAD = 64
NEG = -1e30
LOW = -1e20
PIECES = 4


def split3(x):
    a = x.astype(bf16).astype(f32)
    r = x - a
    b = r.astype(bf16).astype(f32)
    return a, b, r - b


def log_sigmoid(u):
    x = jnp.exp(-jnp.abs(u))
    series = x * (1 - x * (1 / 2 - x * (1 / 3 - x * (1 / 4 - x * (1 / 5 - x * (1 / 6 - x * (1 / 7)))))))
    return jnp.minimum(u, 0.0) - jnp.where(x < 0.0625, series, jnp.log(1 + x))


def dot(a, b):
    return jnp.dot(a, b, preferred_element_type=f32)


def vmem(count):
    return [pl.BlockSpec(memory_space=pltpu.VMEM)] * count


def scalars():
    return pl.BlockSpec(memory_space=pltpu.SMEM)


def pack_kernel(info, mine, theirs, bias, payload, total, even, odd):
    first = info[0] == 0
    own, other = mine[256:260].astype(f32), theirs[256:260].astype(f32)
    gates = jnp.concatenate([jnp.where(first, own, other), jnp.where(first, other, own)], axis=0)
    payload[0:128] = mine[260:388]
    payload[128:136] = gates.astype(bf16)
    logs = jnp.sum(log_sigmoid(gates + bias[:, :1]), axis=1, keepdims=True)
    both = logs[:4] + logs[4:]
    total[...] = jnp.broadcast_to(jnp.concatenate([both, both], axis=0), total.shape)

    @pl.when(first)
    def _():
        even[...] = mine[0:256]
        odd[...] = theirs[0:256]

    @pl.when(jnp.logical_not(first))
    def _():
        even[...] = theirs[0:256]
        odd[...] = mine[0:256]


def pack(info, mine, theirs, bias8):
    blk = mine.shape[1]
    return pl.pallas_call(
        pack_kernel,
        out_shape=(jax.ShapeDtypeStruct((136, blk), bf16), jax.ShapeDtypeStruct((8, 128), f32),
                   jax.ShapeDtypeStruct((256, blk), bf16), jax.ShapeDtypeStruct((256, blk), bf16)),
        in_specs=[scalars(), *vmem(3)], out_specs=tuple(vmem(4)), name="pack",
    )(info, mine, theirs, bias8)


def prepare_kernel(info, column, totals, even, crossed, bias, chunk, rhs, *, rows, cols, blk):
    core, col = info[0], info[1]
    n = rows * 8
    gates = column[:, 128:136, :].astype(f32) + bias[...][None, :, :1]
    logs = log_sigmoid(gates).reshape(n, blk)
    tri = (lax.broadcasted_iota(jnp.int32, (blk, blk), 0) <= lax.broadcasted_iota(jnp.int32, (blk, blk), 1)).astype(bf16)
    inner = sum(dot(p.astype(bf16), tri) for p in split3(logs)).reshape(rows, 8, blk)
    index = lax.broadcasted_iota(jnp.int32, (rows * cols, 8, 128), 0)
    values = totals[...]
    for i in range(rows):
        base = jnp.sum(jnp.where(index < cols * i + col, values, 0.0), axis=0)[:4, :1]
        here = inner[i]
        own = jnp.where(core == 0, here[:4], here[4:] + here[:4, blk - 1:]) + base
        chunk[i, 64:80] = jnp.concatenate([*split3(-own), jnp.zeros((4, blk), f32)], axis=0).astype(bf16)
        chunk[i, 0:64] = column[i, 0:64, :]
        chunk[i, 80:144] = column[i, 64:128, :]
    row16 = lax.broadcasted_iota(jnp.int32, (16, blk), 0)
    swap = info[2] == 1
    for side in range(2):
        for h in range(4):
            s = slice(h * HEAD, (h + 1) * HEAD)
            a, b = even[s].astype(f32), crossed[s].astype(f32)
            q = jnp.where(swap, b, a) if side == 0 else jnp.where(swap, a, b)
            mark = jnp.where((row16 < 12) & ((row16 & 3) == h), 1.0, 0.0)
            rhs[side * 4 + h] = jnp.concatenate([q * 0.125, mark, jnp.zeros((48, blk), f32)], axis=0).astype(bf16)


def prepare(info, column, totals, even, crossed, bias8, cols):
    rows, _, blk = column.shape
    return pl.pallas_call(
        functools.partial(prepare_kernel, rows=rows, cols=cols, blk=blk),
        out_shape=(jax.ShapeDtypeStruct((rows, 144, blk), bf16), jax.ShapeDtypeStruct((8, 128, blk), bf16)),
        in_specs=[scalars(), *vmem(5)], out_specs=tuple(vmem(2)), name="prepare",
    )(info, column, totals, even, crossed, bias8)


def attend_kernel(*refs, count, rows, cols, blk):
    info, rhs = refs[:2]
    chunks = refs[2:2 + count]
    acc, stat = refs[2 + count:4 + count]
    keys, scores, tops = refs[4 + count:]
    core = info[0]
    acc[...] = jnp.zeros_like(acc)
    for side in range(2):
        stat[side, 0:32] = jnp.zeros((32, blk), f32)
        stat[side, 32:64] = jnp.full((32, blk), LOW, f32)
    for n in range(count):
        kv = chunks[n]
        col = info[3 + n]
        ahead = [jnp.clip((info[1 + side] - col + cols - 1) // cols, 0, rows) for side in range(2)]
        full = [a // 2 for a in ahead]
        diag = [(info[1 + side] - col) % cols == 0 for side in range(2)]
        part = [diag[side] | (ahead[side] % 2 == 1) for side in range(2)]
        steps = full[0] + full[1]

        def place(it):
            side = (it >= full[0]).astype(jnp.int32)
            return side, jnp.clip(it - side * full[0], 0, rows // 2 - 1)

        def load_keys(slot, jj):
            for e in range(2):
                keys[slot, e * blk:(e + 1) * blk] = kv[2 * jj + e, 0:128, :].T

        def fused(nxt, cur, allowed=None):
            if cur is not None:
                slot, jj, side, h = cur
                old = stat[side, 32 + 8 * h:40 + 8 * h]
                new = jnp.maximum(old, jnp.max(tops[slot], axis=0, keepdims=True))
                scale = jnp.exp(old - new)
                mass = stat[side, 8 * h:8 * h + 8] * scale
                out = jnp.zeros((64, blk), f32)
            top = None
            size = blk // PIECES
            for e in range(2):
                ps = []
                for g in range(PIECES):
                    at = e * blk + g * size
                    if nxt is not None:
                        s = dot(keys[nxt[1], at:at + size], rhs[nxt[2] * 4 + nxt[3]])
                        if allowed is not None:
                            s = jnp.where(allowed[at:at + size], s, NEG)
                        scores[nxt[0], at:at + size] = s
                        t = jnp.max(s.reshape(size // 8, 8, blk), axis=0)
                        top = t if top is None else jnp.maximum(top, t)
                    if cur is not None:
                        p = jnp.exp(scores[slot, at:at + size].reshape(size // 8, 8, blk) - new[None])
                        mass = mass + jnp.sum(p, axis=0)
                        ps.append(p.reshape(size, blk).astype(bf16))
                if cur is not None:
                    out = out + dot(kv[2 * jj + e, 80:144, :], jnp.concatenate(ps, axis=0))
            if nxt is not None:
                tops[nxt[0]] = top
            if cur is not None:
                stat[side, 8 * h:8 * h + 8] = mass
                stat[side, 32 + 8 * h:40 + 8 * h] = new
                a = acc[side, h * HEAD:(h + 1) * HEAD].reshape(8, 8, blk) * scale[None]
                acc[side, h * HEAD:(h + 1) * HEAD] = a.reshape(64, blk) + out

        @pl.when(steps > 0)
        def _():
            side, jj = place(0)
            load_keys(0, jj)
            fused((0, 0, side, 0), None)

            def body(it, carry):
                slot = it & 1
                side, jj = place(it)
                side_next, jj_next = place(jnp.minimum(it + 1, steps - 1))
                load_keys(1 - slot, jj_next)
                for h in range(4):
                    nxt = ((h + 1) & 1, slot, side, h + 1) if h < 3 else (0, 1 - slot, side_next, 0)
                    fused(nxt, (h & 1, jj, side, h))
                return carry

            lax.fori_loop(0, steps, body, 0)

        def edge(side, carry):
            @pl.when(jnp.where(side == 0, part[0], part[1]))
            def _():
                chip = jnp.where(side == 0, info[1], info[2])
                jj = jnp.clip(jnp.where(side == 0, full[0], full[1]), 0, rows // 2 - 1)
                par = jnp.where(side == 0, info[5], 1 - info[5])
                qpos = (2 * chip + par) * blk + lax.broadcasted_iota(jnp.int32, (2 * blk, blk), 1)
                row = lax.broadcasted_iota(jnp.int32, (2 * blk, blk), 0)
                upper = (row >= blk).astype(jnp.int32)
                kpos = row + upper * ((2 * cols - 1) * blk) + ((2 * jj * cols + col) * 2 + core) * blk
                allowed = kpos <= qpos
                load_keys(0, jj)
                fused((0, 0, side, 0), None, allowed)
                for h in range(4):
                    fused(((h + 1) & 1, 0, side, h + 1) if h < 3 else None, (h & 1, jj, side, h), allowed)

            return carry

        lax.fori_loop(0, 2, edge, 0)


def attend(info, rhs, chunks, cols):
    rows, _, blk = chunks[0].shape
    return pl.pallas_call(
        functools.partial(attend_kernel, count=len(chunks), rows=rows, cols=cols, blk=blk),
        out_shape=(jax.ShapeDtypeStruct((2, 256, blk), f32), jax.ShapeDtypeStruct((2, 64, blk), f32)),
        in_specs=[scalars(), *vmem(1 + len(chunks))], out_specs=tuple(vmem(2)),
        scratch_shapes=[pltpu.VMEM((2, 2 * blk, 128), bf16), pltpu.VMEM((2, 2 * blk, blk), f32), pltpu.VMEM((2, 8, blk), f32)],
        compiler_params=pltpu.CompilerParams(vmem_limit_bytes=24 * 1024 * 1024), name="attend",
    )(info, rhs, *chunks)


def merge_kernel(*refs, count):
    info, accs, stats = refs[0], refs[1:1 + count], refs[1 + count:1 + 2 * count]
    keep, give = refs[1 + 2 * count:]
    for which in range(2):
        dst, side = (keep, give)[which], info[which]
        for h in range(4):
            tops = [s[side, 32 + 8 * h:40 + 8 * h] for s in stats]
            top = functools.reduce(jnp.maximum, tops)
            w = [jnp.exp(t - top) for t in tops]
            mass = sum(s[side, 8 * h:8 * h + 8] * w[j] for j, s in enumerate(stats))
            dst[256 + h:257 + h] = top[:1]
            dst[260 + h:261 + h] = jnp.sum(mass, axis=0, keepdims=True)
            parts = [a[side, h * HEAD:(h + 1) * HEAD].reshape(8, 8, 256) * w[j][None] for j, a in enumerate(accs)]
            dst[h * HEAD:(h + 1) * HEAD] = functools.reduce(jnp.add, parts).reshape(HEAD, 256)


def merge(info, parts):
    shape = jax.ShapeDtypeStruct((264, 256), f32)
    return pl.pallas_call(
        functools.partial(merge_kernel, count=len(parts)), out_shape=(shape, shape),
        in_specs=[scalars(), *vmem(2 * len(parts))], out_specs=tuple(vmem(2)), name="merge",
    )(info, *[p[0] for p in parts], *[p[1] for p in parts])


def finish_kernel(keep, got, out):
    peak = jnp.maximum(keep[256:260], got[256:260])
    wa, wb = jnp.exp(keep[256:260] - peak), jnp.exp(got[256:260] - peak)
    mass = keep[260:264] * wa + got[260:264] * wb
    for h in range(4):
        s = slice(h * HEAD, (h + 1) * HEAD)
        out[s] = ((keep[s] * wa[h:h + 1] + got[s] * wb[h:h + 1]) / mass[h:h + 1]).astype(bf16)


def finish(keep, got):
    return pl.pallas_call(finish_kernel, out_shape=jax.ShapeDtypeStruct((256, 256), bf16), in_specs=vmem(2), out_specs=vmem(1)[0],
                          name="finish")(keep, got)


SP = ("sp_0", "sp_1", "sp_2")
SP_TP = ("sp_0", "sp_1", "sp_2", "tp")


def ring(count, step):
    return [(i, (i + step) % count) for i in range(count)]


def sum_at_owner(value):
    pieces = value.reshape(4, value.shape[0] // 4, value.shape[1])
    arrived = lax.all_to_all(pieces, "tp", split_axis=0, concat_axis=0, tiled=True)
    return arrived.astype(f32).sum(axis=0)


def shards(tokens, w_query, w_key, w_value, w_gate, gate_bias, w_output):
    rows, cols = lax.axis_size("sp_0"), lax.axis_size("sp_1")
    chips = rows * cols
    core, col = lax.axis_index("sp_2"), lax.axis_index("sp_1")
    chip = lax.axis_index("sp_0") * cols + col
    other = chips - 1 - chip
    behind = (chip > other).astype(jnp.int32)
    low, high = jnp.minimum(chip, other), jnp.maximum(chip, other)
    bias8 = jnp.broadcast_to(jnp.tile(gate_bias, 2)[:, None], (8, 128))

    def scalar_row(*values):
        return jnp.stack([jnp.asarray(v, jnp.int32) for v in values])

    copies = jnp.broadcast_to(tokens, (4, *tokens.shape))
    here = lax.all_to_all(copies, "tp", split_axis=0, concat_axis=0, tiled=True)
    here = here.reshape(-1, tokens.shape[1])
    joined = jnp.concatenate([w_query, w_gate, w_key, w_value], axis=1)
    projected = lax.dot_general(joined, here, (((0,), (1,)), ((), ())), preferred_element_type=f32).astype(bf16)
    swapped = lax.ppermute(projected[:260], "sp_2", [(0, 1), (1, 0)])
    payload, total, even, odd = pack(scalar_row(core), projected, swapped, bias8)
    far = [(2 * c + e, 2 * (chips - 1 - c) + e) for c in range(chips) for e in range(2)]
    crossed = lax.ppermute(odd, SP, far)
    column = lax.all_to_all(jnp.broadcast_to(payload, (rows, *payload.shape)), "sp_0", split_axis=0, concat_axis=0, tiled=True)
    totals = lax.all_to_all(jnp.broadcast_to(total, (chips, *total.shape)), ("sp_0", "sp_1"), split_axis=0, concat_axis=0, tiled=True)
    own, rhs = prepare(scalar_row(core, col, behind), column, totals, even, crossed, bias8, cols)

    parts = []
    up, down = own, own
    pending, where = [own], [col]
    for step in range(1, cols // 2 + 1):
        up = lax.ppermute(up, "sp_1", ring(cols, 1))
        following, places = [up], [(col - step) % cols]
        if 2 * step < cols:
            down = lax.ppermute(down, "sp_1", ring(cols, -1))
            following.append(down)
            places.append((col + step) % cols)
        parts.append(attend(scalar_row(core, low, high, where[0], where[-1], behind), rhs, pending, cols))
        pending, where = following, places
    parts.append(attend(scalar_row(core, low, high, where[0], where[-1], behind), rhs, pending, cols))
    mine = jnp.where(behind == 1, 1 - core, core)
    keep, give = merge(scalar_row(mine, 1 - mine), parts)
    got = lax.ppermute(give, "sp_2", [(0, 1), (1, 0)])
    attended = finish(keep, got)
    back = [(2 * c + 1, 2 * (chips - 1 - c) + 1) for c in range(chips)]
    returned = lax.ppermute(attended, SP, back)
    attended = jnp.where(core == 0, attended, returned)
    partial = lax.dot_general(attended, w_output, (((0,), (0,)), ((), ())), preferred_element_type=f32).astype(bf16)
    return sum_at_owner(partial).astype(bf16)


def solution(mesh):
    finer = Mesh(mesh.devices.reshape(8, 8, 2, mesh.shape["tp"]), SP_TP)
    placed = (P(SP_TP, None), P(None, "tp"), P(None, "tp"), P(None, "tp"), P(None, "tp"), P("tp"), P("tp", None))

    return jax.shard_map(shards, mesh=finer, in_specs=placed, out_specs=P(SP_TP, None), check_vma=False)
```

time: 195 us -> 227 us (1.16)
  the two profiles are of different devices: /device:TPU:1 before, /device:TPU:65 now
where the time goes in v3:
time: 227 us; the launch traced here: 226 us
  waiting for transfers between devices  61.3 us (27%)
  Pallas kernels  51.6 us (23%)
  starting transfers between devices  50.2 us (22%)
  blocking collectives  39.9 us (18%)
  local copies, waits for them, and re-layouts  17.2 us (8%)
  matrix products  3.3 us (1%)
    pallas_call x5, Pallas kernels, attend(): pl.pallas_call(functools.partial(attend_kernel, count=len(chunks), rows=r...  42.3 us
    all_to_all x1, blocking collectives, shards(): lax.all_to_all(jnp.broadcast_to(total, (chips, *total.shape)), ('sp_0', '...  27.8 us
    ppermute x4, waiting for transfers between devices, shards(): up = lax.ppermute(up, 'sp_1', ring(cols, 1))  25.5 us
    ppermute x3, starting transfers between devices, shards(): down = lax.ppermute(down, 'sp_1', ring(cols, -1))  13.7 us
    all_to_all x1, blocking collectives, sum_at_owner(): lax.all_to_all(pieces, 'tp', split_axis=0, concat_axis=0, tiled=True)  12.2 us
    all_to_all x1, waiting for transfers between devices, shards(): here = lax.all_to_all(copies, 'tp', split_axis=0, concat_axis=0, tiled=True)  11.6 us
    unnamed x49, local copies, waits for them, and re-layouts  11.4 us
    all_to_all x1, waiting for transfers between devices, shards(): lax.all_to_all(jnp.broadcast_to(payload, (rows, *payload.shape)), 'sp_0',...  9.45 us
  transfers between devices with their start and end apart: 13, of which 9 were waited for; matrix products, arithmetic and copies ran while one was open for 2% of the time, Pallas kernels for 16%

profile of v3, /device:TPU:65, one launch (start us, length us, event | category | flops | bytes accessed | tf_op | source)
XLA Modules:
  0.0 226.2 jit_solution(3140346664988955616)
XLA Ops:
  0.0 2.1 broadcast_in_dim.16
  2.2 4.1 %all-to-all-start = ((bf16[4,64,2048]{2,1,0:T(8,128)(2,1)}), bf16[4,64,2048]{2,1,0:T(8,128)(2,1)S(1)}, u32[]{:S(2)}, u32[]{:S(2)}) async-start(bf16[4,64,2048]{2,1,0:T(8,128)(2,1)} %broadcast_in_dim.16), calls=%async_computation | async-start | bytes 2097152 | tf_op jit(solution)/shard_map/all_to_all | solution.py:286
  6.6 1.3 copy.10
  7.9 1.1 copy.8
  9.0 11.6 %all-to-all-done = bf16[4,64,2048]{2,1,0:T(8,128)(2,1)S(1)} async-done(((bf16[4,64,2048]{2,1,0:T(8,128)(2,1)}), bf16[4,64,2048]{2,1,0:T(8,128)(2,1)S(1)}, u32[]{:S(2)}, u32[]{:S(2)}) %all-to-all-start) | async-done | bytes 1048608 | tf_op jit(solution)/shard_map/all_to_all | solution.py:286
  20.5 2.8 %fusion.8.mine = bf16[388,256]{1,0:T(8,128)(2,1)S(1)} fusion(bf16[256,2048]{1,0:T(8,128)(2,1)S(1)} %bitcast.19, bf16[2048,64]{1,0:T(8,128)(2,1)S(1)} %copy.10, bf16[2048,64]{1,0:T(8,128)(2,1)S(1)} %copy.9, bf16[2048,4]{1,0:T(8,128)(2,1)} %copy.8, bf16[2048,256]{1,0:T(8,128)(2,1)} %param.8), kind=kOutput, calls=%fused_computation.9 | convolution fusion | flops 413303808 | bytes 2836480 | tf_op jit(solution)/shard_map/dot_general | solution.py:289
  23.4 3.7 %collective-permute-start = (bf16[260,256]{1,0:T(8,128)(2,1)S(1)}, bf16[260,256]{1,0:T(8,128)(2,1)S(1)}, u32[]{:S(2)}, u32[]{:S(2)}) collective-permute-start(bf16[260,256]{1,0:T(8,128)(2,1)S(1)} %slice.4), channel_id=1, source_target_pairs={{0,4},{4,0},{1,5},{5,1},{2,6},{6,2},{3,7},{7,3},{8,12},{12,8},{9,1... | collective-permute-start | bytes 399368 | tf_op jit(solution)/shard_map/ppermute | solution.py:290
  27.2 0.9 collective-permute-done.theirs
  28.8 2.0 pack.1
  30.8 0.7 broadcast_in_dim.20
  31.5 27.8 %all_to_all.20.totals = f32[64,8,128]{2,1,0:T(8,128)} all-to-all(f32[64,8,128]{2,1,0:T(8,128)S(1)} %broadcast_in_dim.20), channel_id=1, replica_groups=mesh['sp_0'=8,'sp_1'=8,'sp_2'=2,'tp'=4] {'sp_0','sp_1'}, dimensions={0} | all-to-all | bytes 524288 | tf_op jit(solution)/shard_map/all_to_all | solution.py:295
  59.3 1.7 broadcast_in_dim.19
  61.0 4.6 %all-to-all-start.1 = ((bf16[8,136,256]{2,1,0:T(8,128)(2,1)}), bf16[8,136,256]{2,1,0:T(8,128)(2,1)S(1)}, u32[]{:S(2)}, u32[]{:S(2)}) async-start(bf16[8,136,256]{2,1,0:T(8,128)(2,1)} %broadcast_in_dim.19), calls=%async_computation.1 | async-start | bytes 1114112 | tf_op jit(solution)/shard_map/all_to_all | solution.py:294
  65.5 5.4 %collective-permute-start.1 = (bf16[256,256]{1,0:T(8,128)(2,1)S(1)}, bf16[256,256]{1,0:T(8,128)(2,1)S(1)}, u32[]{:S(2)}, u32[]{:S(2)}) collective-permute-start(bf16[256,256]{1,0:T(8,128)(2,1)S(1)} %copy-done.21), channel_id=1, source_target_pairs={{0,504},{4,508},{8,496},{12,500},{16,488},{20,492},{24,480},{28,48... | collective-permute-start | bytes 393224 | tf_op jit(solution)/shard_map/ppermute | solution.py:293
  71.6 5.9 %collective-permute-done.1.crossed = bf16[256,256]{1,0:T(8,128)(2,1)S(1)} collective-permute-done((bf16[256,256]{1,0:T(8,128)(2,1)S(1)}, bf16[256,256]{1,0:T(8,128)(2,1)S(1)}, u32[]{:S(2)}, u32[]{:S(2)}) %collective-permute-start.1) | collective-permute-done | bytes 131104 | tf_op jit(solution)/shard_map/ppermute | solution.py:293
  77.5 9.4 %all-to-all-done.1.column = bf16[8,136,256]{2,1,0:T(8,128)(2,1)S(1)} async-done(((bf16[8,136,256]{2,1,0:T(8,128)(2,1)}), bf16[8,136,256]{2,1,0:T(8,128)(2,1)S(1)}, u32[]{:S(2)}, u32[]{:S(2)}) %all-to-all-start.1) | async-done | bytes 557088 | tf_op jit(solution)/shard_map/all_to_all | solution.py:294
  87.0 0.8 copy-done.14
  87.8 2.8 %prepare.1 = (bf16[8,144,256]{2,1,0:T(8,128)(2,1)}, bf16[8,128,256]{2,1,0:T(8,128)(2,1)}) custom-call(s32[3]{0:T(128)} %pad_add_fusion.1.info, bf16[8,136,256]{2,1,0:T(8,128)(2,1)} %copy-done.14, f32[64,8,128]{2,1,0:T(8,128)} %all_to_all.20.totals, bf16[256,256]{1,0:T(8,128)(2,1)} %get-tuple-element.25.even, bf16[256,256]{1,0:T(8,128)(2,1)} %copy-done.19, ...), custom_call_target="tpu_custom_call" | custom-call | tf_op jit(solution)/shard_map/prepare/pallas_call | solution.py:101
  90.5 1.9 collective-permute-start.2
  92.4 4.6 %collective-permute-start.3 = (bf16[8,144,256]{2,1,0:T(8,128)(2,1)}, bf16[8,144,256]{2,1,0:T(8,128)(2,1)S(1)}, u32[]{:S(2)}, u32[]{:S(2)}) collective-permute-start(bf16[8,144,256]{2,1,0:T(8,128)(2,1)} %get-tuple-element.28.refs_2_), channel_id=1, source_target_pairs={{0,56},{8,0},{16,8},{24,16},{32,24},{40,32},{48,40},{56,48},{1,57}... | collective-permute-start | bytes 1769480 | tf_op jit(solution)/shard_map/ppermute | solution.py:305
  97.0 9.5 %collective-permute-done.2.refs_2_ = bf16[8,144,256]{2,1,0:T(8,128)(2,1)S(1)} collective-permute-done((bf16[8,144,256]{2,1,0:T(8,128)(2,1)}, bf16[8,144,256]{2,1,0:T(8,128)(2,1)S(1)}, u32[]{:S(2)}, u32[]{:S(2)}) %collective-permute-start.2) | collective-permute-done | bytes 589856 | tf_op jit(solution)/shard_map/ppermute | solution.py:302
  106.5 1.9 collective-permute-start.4
  108.4 4.6 %collective-permute-start.5 = (bf16[8,144,256]{2,1,0:T(8,128)(2,1)S(1)}, bf16[8,144,256]{2,1,0:T(8,128)(2,1)}, u32[]{:S(2)}, u32[]{:S(2)}) collective-permute-start(bf16[8,144,256]{2,1,0:T(8,128)(2,1)S(1)} %collective-permute-done.3.refs_3_), channel_id=1, source_target_pairs={{0,56},{8,0},{16,8},{24,16},{32,24},{40,32},{48,40},{56,48},{1,57}... | collective-permute-start | bytes 1769480 | tf_op jit(solution)/shard_map/ppermute | solution.py:305
  113.0 8.4 %collective-permute-done.4.refs_2_ = bf16[8,144,256]{2,1,0:T(8,128)(2,1)S(1)} collective-permute-done((bf16[8,144,256]{2,1,0:T(8,128)(2,1)S(1)}, bf16[8,144,256]{2,1,0:T(8,128)(2,1)S(1)}, u32[]{:S(2)}, u32[]{:S(2)}) %collective-permute-start.4) | collective-permute-done | bytes 589856 | tf_op jit(solution)/shard_map/ppermute | solution.py:302
  121.5 1.9 collective-permute-start.6
  123.4 4.6 %collective-permute-start.7 = (bf16[8,144,256]{2,1,0:T(8,128)(2,1)}, bf16[8,144,256]{2,1,0:T(8,128)(2,1)}, u32[]{:S(2)}, u32[]{:S(2)}) collective-permute-start(bf16[8,144,256]{2,1,0:T(8,128)(2,1)} %collective-permute-done.5.refs_3_), channel_id=1, source_target_pairs={{0,56},{8,0},{16,8},{24,16},{32,24},{40,32},{48,40},{56,48},{1,57}... | collective-permute-start | bytes 1769480 | tf_op jit(solution)/shard_map/ppermute | solution.py:305
  128.0 7.6 %collective-permute-done.6.refs_2_ = bf16[8,144,256]{2,1,0:T(8,128)(2,1)S(1)} collective-permute-done((bf16[8,144,256]{2,1,0:T(8,128)(2,1)S(1)}, bf16[8,144,256]{2,1,0:T(8,128)(2,1)S(1)}, u32[]{:S(2)}, u32[]{:S(2)}) %collective-permute-start.6) | collective-permute-done | bytes 589856 | tf_op jit(solution)/shard_map/ppermute | solution.py:302
  135.5 1.9 collective-permute-start.8
  138.6 1.0 copy-done.1
  139.7 1.1 copy-done.3
  140.7 5.2 %attend.5 = (f32[2,256,256]{2,1,0:T(8,128)S(1)}, f32[2,64,256]{2,1,0:T(8,128)S(1)}) custom-call(s32[6]{0:T(128)S(1)} %stack.93.refs_0_, bf16[8,128,256]{2,1,0:T(8,128)(2,1)S(1)} %copy-done.1, bf16[8,144,256]{2,1,0:T(8,128)(2,1)S(1)} %copy-done.3), custom_call_target="tpu_custom_call" | custom-call | tf_op jit(solution)/shard_map/attend/pallas_call | solution.py:211
  146.0 0.8 copy-done.4
  147.5 9.9 %attend.6 = (f32[2,256,256]{2,1,0:T(8,128)S(1)}, f32[2,64,256]{2,1,0:T(8,128)S(1)}) custom-call(s32[6]{0:T(128)S(1)} %stack.97.refs_0_, bf16[8,128,256]{2,1,0:T(8,128)(2,1)S(1)} %copy-done.2, bf16[8,144,256]{2,1,0:T(8,128)(2,1)S(1)} %collective-permute-done.2.refs_2_, bf16[8,144,256]{2,1,0:T(8,128)(2,1)S(1)} %collective-permute-done.3.refs_3_), custom_call_target="tpu_custom_call" | custom-call | tf_op jit(solution)/shard_map/attend/pallas_call | solution.py:211
  157.4 10.9 %attend.7 = (f32[2,256,256]{2,1,0:T(8,128)S(1)}, f32[2,64,256]{2,1,0:T(8,128)S(1)}) custom-call(s32[6]{0:T(128)S(1)} %stack.100.refs_0_, bf16[8,128,256]{2,1,0:T(8,128)(2,1)S(1)} %copy-done.2, bf16[8,144,256]{2,1,0:T(8,128)(2,1)S(1)} %collective-permute-done.4.refs_2_, bf16[8,144,256]{2,1,0:T(8,128)(2,1)} %collective-permute-done.5.refs_3_), custom_call_target="tpu_custom_call" | custom-call | tf_op jit(solution)/shard_map/attend/pallas_call | solution.py:211
  168.3 0.8 copy-done.6
  169.7 10.4 %attend.8 = (f32[2,256,256]{2,1,0:T(8,128)S(1)}, f32[2,64,256]{2,1,0:T(8,128)S(1)}) custom-call(s32[6]{0:T(128)S(1)} %stack.103.refs_0_, bf16[8,128,256]{2,1,0:T(8,128)(2,1)S(1)} %copy-done.2, bf16[8,144,256]{2,1,0:T(8,128)(2,1)S(1)} %collective-permute-done.6.refs_2_, bf16[8,144,256]{2,1,0:T(8,128)(2,1)} %collective-permute-done.7.refs_3_), custom_call_target="tpu_custom_call" | custom-call | tf_op jit(solution)/shard_map/attend/pallas_call | solution.py:211
  180.2 0.8 copy-done.7
  181.0 5.8 %attend.9 = (f32[2,256,256]{2,1,0:T(8,128)S(1)}, f32[2,64,256]{2,1,0:T(8,128)S(1)}) custom-call(s32[6]{0:T(128)S(1)} %stack.105.refs_0_, bf16[8,128,256]{2,1,0:T(8,128)(2,1)S(1)} %copy-done.2, bf16[8,144,256]{2,1,0:T(8,128)(2,1)} %collective-permute-done.8.refs_2_), custom_call_target="tpu_custom_call" | custom-call | tf_op jit(solution)/shard_map/attend/pallas_call | solution.py:211
  186.8 0.8 copy-done.8
  188.3 2.8 %merge.1 = (f32[264,256]{1,0:T(8,128)}, f32[264,256]{1,0:T(8,128)}) custom-call(s32[2]{0:T(128)} %pad_add_fusion.refs_0_, f32[2,256,256]{2,1,0:T(8,128)} %copy-done.4, f32[2,256,256]{2,1,0:T(8,128)} %copy-done.5, f32[2,256,256]{2,1,0:T(8,128)} %copy-done.6, f32[2,256,256]{2,1,0:T(8,128)} %copy-done.7, f32[2,256,256]{2,1,0:T(8,128)} %copy-done.8, ...), custom_call_target="tpu_custom_call" | custom-call | tf_op jit(solution)/shard_map/merge/pallas_call | solution.py:238
  191.1 6.7 %collective-permute-start.9 = (f32[264,256]{1,0:T(8,128)}, f32[264,256]{1,0:T(8,128)S(1)}, u32[]{:S(2)}, u32[]{:S(2)}) collective-permute-start(f32[264,256]{1,0:T(8,128)} %get-tuple-element.40), channel_id=1, source_target_pairs={{0,4},{4,0},{1,5},{5,1},{2,6},{6,2},{3,7},{7,3},{8,12},{12,8},{9,1... | collective-permute-start | bytes 811016 | tf_op jit(solution)/shard_map/ppermute | solution.py:313
  197.8 1.4 collective-permute-done.9.got
  199.2 0.7 copy-done.16
  199.9 1.7 finish.1
  201.6 4.3 %collective-permute-start.10 = (bf16[256,256]{1,0:T(8,128)(2,1)}, bf16[256,256]{1,0:T(8,128)(2,1)S(1)}, u32[]{:S(2)}, u32[]{:S(2)}) collective-permute-start(bf16[256,256]{1,0:T(8,128)(2,1)} %finish.1), channel_id=1, source_target_pairs={{4,508},{12,500},{20,492},{28,484},{36,476},{44,468},{52,460},{60,... | collective-permute-start | bytes 393224 | tf_op jit(solution)/shard_map/ppermute | solution.py:316
  206.0 6.7 %collective-permute-done.10 = bf16[256,256]{1,0:T(8,128)(2,1)S(1)} collective-permute-done((bf16[256,256]{1,0:T(8,128)(2,1)}, bf16[256,256]{1,0:T(8,128)(2,1)S(1)}, u32[]{:S(2)}, u32[]{:S(2)}) %collective-permute-start.10) | collective-permute-done | bytes 131104 | tf_op jit(solution)/shard_map/ppermute | solution.py:316
  213.1 12.2 %all_to_all.21 = bf16[4,64,2048]{2,1,0:T(8,128)(2,1)S(1)} all-to-all(bf16[4,64,2048]{2,1,0:T(8,128)(2,1)S(1)} %bitcast.18), channel_id=1, replica_groups=mesh['sp_0'=8,'sp_1'=8,'sp_2'=2,'tp'=4] {'tp'}, dimensions={0} | all-to-all | bytes 2097152 | tf_op jit(solution)/shard_map/all_to_all | solution.py:268
  225.3 0.9 reduce_sum.12
  (55 shorter events, 5.3 us)
Async XLA Ops:
  0.0 212.6 %copy-start = (bf16[256,2048]{1,0:T(8,128)(2,1)S(1)}, bf16[256,2048]{1,0:T(8,128)(2,1)}, u32[]{:S(2)}) copy-start(bf16[256,2048]{1,0:T(8,128)(2,1)} %param.13) | copy-start | bytes 3145732
  2.2 4.1 %copy-start.17 = (bf16[2048,64]{0,1:T(8,128)(2,1)S(1)}, bf16[2048,64]{0,1:T(8,128)(2,1)}, u32[]{:S(2)}) copy-start(bf16[2048,64]{0,1:T(8,128)(2,1)} %param.9) | copy-start | bytes 786436
  2.2 18.4 %all-to-all-start = ((bf16[4,64,2048]{2,1,0:T(8,128)(2,1)}), bf16[4,64,2048]{2,1,0:T(8,128)(2,1)S(1)}, u32[]{:S(2)}, u32[]{:S(2)}) async-start(bf16[4,64,2048]{2,1,0:T(8,128)(2,1)} %broadcast_in_dim.16), calls=%async_computation | async-start | bytes 2097152 | tf_op jit(solution)/shard_map/all_to_all | solution.py:286
  6.3 1.6 copy-start.20
  20.5 6.6 %copy-start.22 = (f32[4]{0:T(128)S(1)}, f32[4]{0:T(128)}, u32[]{:S(2)}) copy-start(f32[4]{0:T(128)} %param.12) | copy-start | bytes 52
  23.4 5.4 %copy-start.15 = (bf16[388,256]{1,0:T(8,128)(2,1)}, bf16[388,256]{1,0:T(8,128)(2,1)S(1)}, u32[]{:S(2)}) copy-start(bf16[388,256]{1,0:T(8,128)(2,1)S(1)} %fusion.8.mine) | copy-start | bytes 595972
  23.4 4.7 %collective-permute-start = (bf16[260,256]{1,0:T(8,128)(2,1)S(1)}, bf16[260,256]{1,0:T(8,128)(2,1)S(1)}, u32[]{:S(2)}, u32[]{:S(2)}) collective-permute-start(bf16[260,256]{1,0:T(8,128)(2,1)S(1)} %slice.4), channel_id=1, source_target_pairs={{0,4},{4,0},{1,5},{5,1},{2,6},{6,2},{3,7},{7,3},{8,12},{12,8},{9,1... | collective-permute-start | bytes 399368 | tf_op jit(solution)/shard_map/ppermute | solution.py:290
  28.1 0.7 copy-start.18
  31.5 34.1 %copy-start.21 = (bf16[256,256]{1,0:T(8,128)(2,1)S(1)}, bf16[256,256]{1,0:T(8,128)(2,1)}, u32[]{:S(2)}) copy-start(bf16[256,256]{1,0:T(8,128)(2,1)} %get-tuple-element.26) | copy-start | bytes 393220
  61.0 26.0 %all-to-all-start.1 = ((bf16[8,136,256]{2,1,0:T(8,128)(2,1)}), bf16[8,136,256]{2,1,0:T(8,128)(2,1)S(1)}, u32[]{:S(2)}, u32[]{:S(2)}) async-start(bf16[8,136,256]{2,1,0:T(8,128)(2,1)} %broadcast_in_dim.19), calls=%async_computation.1 | async-start | bytes 1114112 | tf_op jit(solution)/shard_map/all_to_all | solution.py:294
  65.5 12.0 %collective-permute-start.1 = (bf16[256,256]{1,0:T(8,128)(2,1)S(1)}, bf16[256,256]{1,0:T(8,128)(2,1)S(1)}, u32[]{:S(2)}, u32[]{:S(2)}) collective-permute-start(bf16[256,256]{1,0:T(8,128)(2,1)S(1)} %copy-done.21), channel_id=1, source_target_pairs={{0,504},{4,508},{8,496},{12,500},{16,488},{20,492},{24,480},{28,48... | collective-permute-start | bytes 393224 | tf_op jit(solution)/shard_map/ppermute | solution.py:293
  77.5 9.5 %copy-start.19 = (bf16[256,256]{1,0:T(8,128)(2,1)}, bf16[256,256]{1,0:T(8,128)(2,1)S(1)}, u32[]{:S(2)}) copy-start(bf16[256,256]{1,0:T(8,128)(2,1)S(1)} %collective-permute-done.1.crossed) | copy-start | bytes 393220
  87.0 0.8 copy-start.14
  90.5 16.0 %collective-permute-start.2 = (bf16[8,144,256]{2,1,0:T(8,128)(2,1)}, bf16[8,144,256]{2,1,0:T(8,128)(2,1)S(1)}, u32[]{:S(2)}, u32[]{:S(2)}) collective-permute-start(bf16[8,144,256]{2,1,0:T(8,128)(2,1)} %get-tuple-element.28.refs_2_), channel_id=1, source_target_pairs={{0,8},{8,16},{16,24},{24,32},{32,40},{40,48},{48,56},{56,0},{1,9},... | collective-permute-start | bytes 1769480 | tf_op jit(solution)/shard_map/ppermute | solution.py:302
  92.4 16.0 %collective-permute-start.3 = (bf16[8,144,256]{2,1,0:T(8,128)(2,1)}, bf16[8,144,256]{2,1,0:T(8,128)(2,1)S(1)}, u32[]{:S(2)}, u32[]{:S(2)}) collective-permute-start(bf16[8,144,256]{2,1,0:T(8,128)(2,1)} %get-tuple-element.28.refs_2_), channel_id=1, source_target_pairs={{0,56},{8,0},{16,8},{24,16},{32,24},{40,32},{48,40},{56,48},{1,57}... | collective-permute-start | bytes 1769480 | tf_op jit(solution)/shard_map/ppermute | solution.py:305
  106.5 14.9 %collective-permute-start.4 = (bf16[8,144,256]{2,1,0:T(8,128)(2,1)S(1)}, bf16[8,144,256]{2,1,0:T(8,128)(2,1)S(1)}, u32[]{:S(2)}, u32[]{:S(2)}) collective-permute-start(bf16[8,144,256]{2,1,0:T(8,128)(2,1)S(1)} %collective-permute-done.2.refs_2_), channel_id=1, source_target_pairs={{0,8},{8,16},{16,24},{24,32},{32,40},{40,48},{48,56},{56,0},{1,9},... | collective-permute-start | bytes 1769480 | tf_op jit(solution)/shard_map/ppermute | solution.py:302
  108.4 14.9 %collective-permute-start.5 = (bf16[8,144,256]{2,1,0:T(8,128)(2,1)S(1)}, bf16[8,144,256]{2,1,0:T(8,128)(2,1)}, u32[]{:S(2)}, u32[]{:S(2)}) collective-permute-start(bf16[8,144,256]{2,1,0:T(8,128)(2,1)S(1)} %collective-permute-done.3.refs_3_), channel_id=1, source_target_pairs={{0,56},{8,0},{16,8},{24,16},{32,24},{40,32},{48,40},{56,48},{1,57}... | collective-permute-start | bytes 1769480 | tf_op jit(solution)/shard_map/ppermute | solution.py:305
  121.5 14.1 %collective-permute-start.6 = (bf16[8,144,256]{2,1,0:T(8,128)(2,1)S(1)}, bf16[8,144,256]{2,1,0:T(8,128)(2,1)S(1)}, u32[]{:S(2)}, u32[]{:S(2)}) collective-permute-start(bf16[8,144,256]{2,1,0:T(8,128)(2,1)S(1)} %collective-permute-done.4.refs_2_), channel_id=1, source_target_pairs={{0,8},{8,16},{16,24},{24,32},{32,40},{40,48},{48,56},{56,0},{1,9},... | collective-permute-start | bytes 1769480 | tf_op jit(solution)/shard_map/ppermute | solution.py:302
  123.4 46.3 %collective-permute-start.7 = (bf16[8,144,256]{2,1,0:T(8,128)(2,1)}, bf16[8,144,256]{2,1,0:T(8,128)(2,1)}, u32[]{:S(2)}, u32[]{:S(2)}) collective-permute-start(bf16[8,144,256]{2,1,0:T(8,128)(2,1)} %collective-permute-done.5.refs_3_), channel_id=1, source_target_pairs={{0,56},{8,0},{16,8},{24,16},{32,24},{40,32},{48,40},{56,48},{1,57}... | collective-permute-start | bytes 1769480 | tf_op jit(solution)/shard_map/ppermute | solution.py:305
  135.5 45.5 %collective-permute-start.8 = (bf16[8,144,256]{2,1,0:T(8,128)(2,1)S(1)}, bf16[8,144,256]{2,1,0:T(8,128)(2,1)}, u32[]{:S(2)}, u32[]{:S(2)}) collective-permute-start(bf16[8,144,256]{2,1,0:T(8,128)(2,1)S(1)} %collective-permute-done.6.refs_2_), channel_id=1, source_target_pairs={{0,8},{8,16},{16,24},{24,32},{32,40},{40,48},{48,56},{56,0},{1,9},... | collective-permute-start | bytes 1769480 | tf_op jit(solution)/shard_map/ppermute | solution.py:302
  138.6 1.0 copy-start.1
  139.7 1.1 copy-start.3
  140.7 6.7 %copy-start.2 = (bf16[8,128,256]{2,1,0:T(8,128)(2,1)S(1)}, bf16[8,128,256]{2,1,0:T(8,128)(2,1)}, u32[]{:S(2)}) copy-start(bf16[8,128,256]{2,1,0:T(8,128)(2,1)} %get-tuple-element.27.refs_1_) | copy-start | bytes 1572868
  146.0 0.8 copy-start.4
  146.8 0.7 copy-start.9
  157.4 22.8 %copy-start.5 = (f32[2,256,256]{2,1,0:T(8,128)}, f32[2,256,256]{2,1,0:T(8,128)S(1)}, u32[]{:S(2)}) copy-start(f32[2,256,256]{2,1,0:T(8,128)S(1)} %get-tuple-element.30.refs_2_) | copy-start | bytes 1572868
  157.4 22.8 %copy-start.10 = (f32[2,64,256]{2,1,0:T(8,128)}, f32[2,64,256]{2,1,0:T(8,128)S(1)}, u32[]{:S(2)}) copy-start(f32[2,64,256]{2,1,0:T(8,128)S(1)} %get-tuple-element.35.refs_7_) | copy-start | bytes 393220
  168.3 0.8 copy-start.6
  169.1 0.6 copy-start.11
  180.2 0.8 copy-start.7
  181.0 5.8 %copy-start.12 = (f32[2,64,256]{2,1,0:T(8,128)}, f32[2,64,256]{2,1,0:T(8,128)S(1)}, u32[]{:S(2)}) copy-start(f32[2,64,256]{2,1,0:T(8,128)S(1)} %get-tuple-element.37.refs_9_) | copy-start | bytes 393220
  186.8 0.8 copy-start.8
  187.6 0.7 copy-start.13
  191.1 8.0 %collective-permute-start.9 = (f32[264,256]{1,0:T(8,128)}, f32[264,256]{1,0:T(8,128)S(1)}, u32[]{:S(2)}, u32[]{:S(2)}) collective-permute-start(f32[264,256]{1,0:T(8,128)} %get-tuple-element.40), channel_id=1, source_target_pairs={{0,4},{4,0},{1,5},{5,1},{2,6},{6,2},{3,7},{7,3},{8,12},{12,8},{9,1... | collective-permute-start | bytes 811016 | tf_op jit(solution)/shard_map/ppermute | solution.py:313
  199.2 0.7 copy-start.16
  201.6 11.0 %collective-permute-start.10 = (bf16[256,256]{1,0:T(8,128)(2,1)}, bf16[256,256]{1,0:T(8,128)(2,1)S(1)}, u32[]{:S(2)}, u32[]{:S(2)}) collective-permute-start(bf16[256,256]{1,0:T(8,128)(2,1)} %finish.1), channel_id=1, source_target_pairs={{4,508},{12,500},{20,492},{28,484},{36,476},{44,468},{52,460},{60,... | collective-permute-start | bytes 393224 | tf_op jit(solution)/shard_map/ppermute | solution.py:316

commit v4 on v3

--- a/solution.py
+++ b/solution.py
@@ -11,6 +11,7 @@
 NEG = -1e30
 LOW = -1e20
 PIECES = 4
+SMALL = pltpu.CompilerParams(vmem_limit_bytes=8 * 1024 * 1024)
 
 
 def split3(x):
@@ -38,15 +39,13 @@
     return pl.BlockSpec(memory_space=pltpu.SMEM)
 
 
-def pack_kernel(info, mine, theirs, bias, payload, total, even, odd):
+def sums_kernel(info, mine, theirs, bias, total, even, odd):
     first = info[0] == 0
     own, other = mine[256:260].astype(f32), theirs[256:260].astype(f32)
     gates = jnp.concatenate([jnp.where(first, own, other), jnp.where(first, other, own)], axis=0)
-    payload[0:128] = mine[260:388]
-    payload[128:136] = gates.astype(bf16)
     logs = jnp.sum(log_sigmoid(gates + bias[:, :1]), axis=1, keepdims=True)
     both = logs[:4] + logs[4:]
-    total[...] = jnp.broadcast_to(jnp.concatenate([both, both], axis=0), total.shape)
+    total[...] = jnp.broadcast_to(jnp.concatenate([both, logs[:4]], axis=0), total.shape)
 
     @pl.when(first)
     def _():
@@ -59,29 +58,50 @@
         odd[...] = mine[0:256]
 
 
-def pack(info, mine, theirs, bias8):
+def sums(info, mine, theirs, bias8):
     blk = mine.shape[1]
-    return pl.pallas_call(
-        pack_kernel,
-        out_shape=(jax.ShapeDtypeStruct((136, blk), bf16), jax.ShapeDtypeStruct((8, 128), f32),
-                   jax.ShapeDtypeStruct((256, blk), bf16), jax.ShapeDtypeStruct((256, blk), bf16)),
-        in_specs=[scalars(), *vmem(3)], out_specs=tuple(vmem(4)), name="pack",
+    half = jax.ShapeDtypeStruct((256, blk), bf16)
+    return pl.pallas_call(
+        sums_kernel, out_shape=(jax.ShapeDtypeStruct((8, 128), f32), half, half),
+        in_specs=[scalars(), *vmem(3)], out_specs=tuple(vmem(3)), compiler_params=SMALL, name="sums",
     )(info, mine, theirs, bias8)
 
 
-def prepare_kernel(info, column, totals, even, crossed, bias, chunk, rhs, *, rows, cols, blk):
+def pack_kernel(mine, total, row, payload, *, cols):
+    payload[0:128] = mine[260:388]
+    lane = lax.broadcasted_iota(jnp.int32, (4, 128), 1)
+    held = jnp.zeros((4, 128), f32)
+    for j in range(cols + 1):
+        values = row[j, 0:4] if j < cols else total[4:8]
+        for p, part in enumerate(split3(values)):
+            held = jnp.where(lane == 16 * p + j, part, held)
+    held = jnp.concatenate([held, jnp.zeros((4, 128), f32)], axis=1)
+    payload[128:136] = jnp.concatenate([mine[256:260].astype(f32), held], axis=0).astype(bf16)
+
+
+def pack(mine, total, row):
+    blk = mine.shape[1]
+    return pl.pallas_call(
+        functools.partial(pack_kernel, cols=row.shape[0]), out_shape=jax.ShapeDtypeStruct((136, blk), bf16),
+        in_specs=vmem(3), out_specs=vmem(1)[0], compiler_params=SMALL, name="pack",
+    )(mine, total, row)
+
+
+def prepare_kernel(info, column, even, crossed, bias, chunk, rhs, *, rows, cols, blk):
     core, col = info[0], info[1]
-    n = rows * 8
-    gates = column[:, 128:136, :].astype(f32) + bias[...][None, :, :1]
-    logs = log_sigmoid(gates).reshape(n, blk)
+    last = column[:, 128:136, :].astype(f32)
+    logs = log_sigmoid(last + bias[...][None, :, :1]).reshape(rows * 8, blk)
     tri = (lax.broadcasted_iota(jnp.int32, (blk, blk), 0) <= lax.broadcasted_iota(jnp.int32, (blk, blk), 1)).astype(bf16)
     inner = sum(dot(p.astype(bf16), tri) for p in split3(logs)).reshape(rows, 8, blk)
-    index = lax.broadcasted_iota(jnp.int32, (rows * cols, 8, 128), 0)
-    values = totals[...]
+    lane = lax.broadcasted_iota(jnp.int32, (rows, 8, blk), 2)
+    which = lane & 15
+    used = lane < 48
+    whole = jnp.sum(jnp.where(used & (which < cols), last, 0.0), axis=2, keepdims=True)
+    early = jnp.sum(jnp.where(used & ((which < col) | ((which == cols) & (core == 1))), last, 0.0), axis=2, keepdims=True)
+    before = jnp.zeros((4, 1), f32)
     for i in range(rows):
-        base = jnp.sum(jnp.where(index < cols * i + col, values, 0.0), axis=0)[:4, :1]
-        here = inner[i]
-        own = jnp.where(core == 0, here[:4], here[4:] + here[:4, blk - 1:]) + base
+        own = inner[i, :4] + (before + early[i, 4:])
+        before = before + whole[i, 4:]
         chunk[i, 64:80] = jnp.concatenate([*split3(-own), jnp.zeros((4, blk), f32)], axis=0).astype(bf16)
         chunk[i, 0:64] = column[i, 0:64, :]
         chunk[i, 80:144] = column[i, 64:128, :]
@@ -92,17 +112,17 @@
             s = slice(h * HEAD, (h + 1) * HEAD)
             a, b = even[s].astype(f32), crossed[s].astype(f32)
             q = jnp.where(swap, b, a) if side == 0 else jnp.where(swap, a, b)
-            mark = jnp.where((row16 < 12) & ((row16 & 3) == h), 1.0, 0.0)
+            mark = jnp.where((row16 == 12) | ((row16 < 12) & ((row16 & 3) == h)), 1.0, 0.0)
             rhs[side * 4 + h] = jnp.concatenate([q * 0.125, mark, jnp.zeros((48, blk), f32)], axis=0).astype(bf16)
 
 
-def prepare(info, column, totals, even, crossed, bias8, cols):
+def prepare(info, column, even, crossed, bias8, cols):
     rows, _, blk = column.shape
     return pl.pallas_call(
         functools.partial(prepare_kernel, rows=rows, cols=cols, blk=blk),
         out_shape=(jax.ShapeDtypeStruct((rows, 144, blk), bf16), jax.ShapeDtypeStruct((8, 128, blk), bf16)),
-        in_specs=[scalars(), *vmem(5)], out_specs=tuple(vmem(2)), name="prepare",
-    )(info, column, totals, even, crossed, bias8)
+        in_specs=[scalars(), *vmem(4)], out_specs=tuple(vmem(2)), compiler_params=pltpu.CompilerParams(vmem_limit_bytes=16 * 1024 * 1024), name="prepare",
+    )(info, column, even, crossed, bias8)
 
 
 def attend_kernel(*refs, count, rows, cols, blk):
@@ -111,6 +131,8 @@
     acc, stat = refs[2 + count:4 + count]
     keys, scores, tops = refs[4 + count:]
     core = info[0]
+    size = blk // PIECES
+    row16 = lax.broadcasted_iota(jnp.int32, (16, blk), 0)
     acc[...] = jnp.zeros_like(acc)
     for side in range(2):
         stat[side, 0:32] = jnp.zeros((32, blk), f32)
@@ -119,18 +141,19 @@
         kv = chunks[n]
         col = info[3 + n]
         ahead = [jnp.clip((info[1 + side] - col + cols - 1) // cols, 0, rows) for side in range(2)]
-        full = [a // 2 for a in ahead]
         diag = [(info[1 + side] - col) % cols == 0 for side in range(2)]
-        part = [diag[side] | (ahead[side] % 2 == 1) for side in range(2)]
+        full = [jnp.where(diag[side], ahead[side], ahead[side] + 1) // 2 for side in range(2)]
         steps = full[0] + full[1]
 
         def place(it):
             side = (it >= full[0]).astype(jnp.int32)
             return side, jnp.clip(it - side * full[0], 0, rows // 2 - 1)
 
-        def load_keys(slot, jj):
+        def load_keys(slot, jj, count):
             for e in range(2):
-                keys[slot, e * blk:(e + 1) * blk] = kv[2 * jj + e, 0:128, :].T
+                marks = kv[2 * jj + e, 64:80, :].astype(f32)
+                marks = jnp.where((row16 == 12) & (2 * jj + e >= count), NEG, marks).astype(bf16)
+                keys[slot, e * blk:(e + 1) * blk] = jnp.concatenate([kv[2 * jj + e, 0:64, :], marks, kv[2 * jj + e, 80:128, :]], axis=0).T
 
         def fused(nxt, cur, allowed=None):
             if cur is not None:
@@ -141,7 +164,6 @@
                 mass = stat[side, 8 * h:8 * h + 8] * scale
                 out = jnp.zeros((64, blk), f32)
             top = None
-            size = blk // PIECES
             for e in range(2):
                 ps = []
                 for g in range(PIECES):
@@ -170,14 +192,14 @@
         @pl.when(steps > 0)
         def _():
             side, jj = place(0)
-            load_keys(0, jj)
+            load_keys(0, jj, jnp.where(side == 0, ahead[0], ahead[1]))
             fused((0, 0, side, 0), None)
 
             def body(it, carry):
                 slot = it & 1
                 side, jj = place(it)
                 side_next, jj_next = place(jnp.minimum(it + 1, steps - 1))
-                load_keys(1 - slot, jj_next)
+                load_keys(1 - slot, jj_next, jnp.where(side_next == 0, ahead[0], ahead[1]))
                 for h in range(4):
                     nxt = ((h + 1) & 1, slot, side, h + 1) if h < 3 else (0, 1 - slot, side_next, 0)
                     fused(nxt, (h & 1, jj, side, h))
@@ -186,7 +208,7 @@
             lax.fori_loop(0, steps, body, 0)
 
         def edge(side, carry):
-            @pl.when(jnp.where(side == 0, part[0], part[1]))
+            @pl.when(jnp.where(side == 0, diag[0], diag[1]))
             def _():
                 chip = jnp.where(side == 0, info[1], info[2])
                 jj = jnp.clip(jnp.where(side == 0, full[0], full[1]), 0, rows // 2 - 1)
@@ -196,7 +218,7 @@
                 upper = (row >= blk).astype(jnp.int32)
                 kpos = row + upper * ((2 * cols - 1) * blk) + ((2 * jj * cols + col) * 2 + core) * blk
                 allowed = kpos <= qpos
-                load_keys(0, jj)
+                load_keys(0, jj, rows)
                 fused((0, 0, side, 0), None, allowed)
                 for h in range(4):
                     fused(((h + 1) & 1, 0, side, h + 1) if h < 3 else None, (h & 1, jj, side, h), allowed)
@@ -213,7 +235,7 @@
         out_shape=(jax.ShapeDtypeStruct((2, 256, blk), f32), jax.ShapeDtypeStruct((2, 64, blk), f32)),
         in_specs=[scalars(), *vmem(1 + len(chunks))], out_specs=tuple(vmem(2)),
         scratch_shapes=[pltpu.VMEM((2, 2 * blk, 128), bf16), pltpu.VMEM((2, 2 * blk, blk), f32), pltpu.VMEM((2, 8, blk), f32)],
-        compiler_params=pltpu.CompilerParams(vmem_limit_bytes=24 * 1024 * 1024), name="attend",
+        compiler_params=pltpu.CompilerParams(vmem_limit_bytes=16 * 1024 * 1024), name="attend",
     )(info, rhs, *chunks)
 
 
@@ -237,7 +259,8 @@
     shape = jax.ShapeDtypeStruct((264, 256), f32)
     return pl.pallas_call(
         functools.partial(merge_kernel, count=len(parts)), out_shape=(shape, shape),
-        in_specs=[scalars(), *vmem(2 * len(parts))], out_specs=tuple(vmem(2)), name="merge",
+        in_specs=[scalars(), *vmem(2 * len(parts))], out_specs=tuple(vmem(2)),
+        compiler_params=pltpu.CompilerParams(vmem_limit_bytes=16 * 1024 * 1024), name="merge",
     )(info, *[p[0] for p in parts], *[p[1] for p in parts])
 
 
@@ -252,7 +275,7 @@
 
 def finish(keep, got):
     return pl.pallas_call(finish_kernel, out_shape=jax.ShapeDtypeStruct((256, 256), bf16), in_specs=vmem(2), out_specs=vmem(1)[0],
-                          name="finish")(keep, got)
+                          compiler_params=SMALL, name="finish")(keep, got)
 
 
 SP = ("sp_0", "sp_1", "sp_2")
@@ -288,12 +311,13 @@
     joined = jnp.concatenate([w_query, w_gate, w_key, w_value], axis=1)
     projected = lax.dot_general(joined, here, (((0,), (1,)), ((), ())), preferred_element_type=f32).astype(bf16)
     swapped = lax.ppermute(projected[:260], "sp_2", [(0, 1), (1, 0)])
-    payload, total, even, odd = pack(scalar_row(core), projected, swapped, bias8)
+    total, even, odd = sums(scalar_row(core), projected, swapped, bias8)
     far = [(2 * c + e, 2 * (chips - 1 - c) + e) for c in range(chips) for e in range(2)]
     crossed = lax.ppermute(odd, SP, far)
+    row = lax.all_to_all(jnp.broadcast_to(total, (cols, *total.shape)), "sp_1", split_axis=0, concat_axis=0, tiled=True)
+    payload = pack(projected, total, row)
     column = lax.all_to_all(jnp.broadcast_to(payload, (rows, *payload.shape)), "sp_0", split_axis=0, concat_axis=0, tiled=True)
-    totals = lax.all_to_all(jnp.broadcast_to(total, (chips, *total.shape)), ("sp_0", "sp_1"), split_axis=0, concat_axis=0, tiled=True)
-    own, rhs = prepare(scalar_row(core, col, behind), column, totals, even, crossed, bias8, cols)
+    own, rhs = prepare(scalar_row(core, col, behind), column, even, crossed, bias8, cols)
 
     parts = []
     up, down = own, own

time: 227 us -> 198 us (0.87)
  blocking collectives: 39.9 us -> 25.7 us
  local copies, waits for them, and re-layouts: 17.2 us -> 8.13 us
  Pallas kernels: 51.6 us -> 42.6 us
  starting transfers between devices: 50.2 us -> 56.1 us
    all_to_all x1, blocking collectives: 27.8 us -> 13.5 us  [shards(): lax.all_to_all(jnp.broadcast_to(total, (cols, *total.shape)), 'sp_1', spl...]
    unnamed x49 -> x15, local copies, waits for them, and re-layouts: 11.4 us -> 4.52 us
    all_to_all x1, starting transfers between devices: 4.56 us -> 9.4 us  [shards(): lax.all_to_all(jnp.broadcast_to(payload, (rows, *payload.shape)), 'sp_0',...]
  transfers between devices with their start and end apart: 13 -> 13, of which waited for: 9 -> 9; matrix products, arithmetic and copies ran while one was open for 2% -> 2% of each run, Pallas kernels for 16% -> 18%
where the time goes in v4:
time: 198 us; the launch traced here: 197 us
  waiting for transfers between devices  59.5 us (30%)
  starting transfers between devices  56.1 us (28%)
  Pallas kernels  42.6 us (22%)
  blocking collectives  25.7 us (13%)
  local copies, waits for them, and re-layouts  8.13 us (4%)
  matrix products  3.3 us (2%)
    pallas_call x5, Pallas kernels, attend(): pl.pallas_call(functools.partial(attend_kernel, count=len(chunks), rows=r...  40.5 us
    ppermute x4, waiting for transfers between devices, shards(): up = lax.ppermute(up, 'sp_1', ring(cols, 1))  24.6 us
    ppermute x3, starting transfers between devices, shards(): down = lax.ppermute(down, 'sp_1', ring(cols, -1))  13.7 us
    all_to_all x1, blocking collectives, shards(): lax.all_to_all(jnp.broadcast_to(total, (cols, *total.shape)), 'sp_1', spl...  13.5 us
    all_to_all x1, blocking collectives, sum_at_owner(): lax.all_to_all(pieces, 'tp', split_axis=0, concat_axis=0, tiled=True)  12.2 us
    all_to_all x1, waiting for transfers between devices, shards(): here = lax.all_to_all(copies, 'tp', split_axis=0, concat_axis=0, tiled=True)  11.6 us
    all_to_all x1, starting transfers between devices, shards(): lax.all_to_all(jnp.broadcast_to(payload, (rows, *payload.shape)), 'sp_0',...  9.4 us
    all_to_all x1, waiting for transfers between devices, shards(): lax.all_to_all(jnp.broadcast_to(payload, (rows, *payload.shape)), 'sp_0',...  8.46 us
  transfers between devices with their start and end apart: 13, of which 9 were waited for; matrix products, arithmetic and copies ran while one was open for 2% of the time, Pallas kernels for 18%

profile of v4, /device:TPU:65, one launch (start us, length us, event | category | flops | bytes accessed | tf_op | source)
XLA Modules:
  0.0 196.8 jit_solution(6425342068718421349)
XLA Ops:
  0.0 2.2 %broadcast_in_dim.16 = bf16[4,64,2048]{2,1,0:T(8,128)(2,1)} broadcast(bf16[64,2048]{1,0:T(8,128)(2,1)} %param.7), dimensions={1,2} | broadcast | bytes 1310720 | tf_op jit(solution)/shard_map/broadcast_in_dim | solution.py:308
  2.2 4.1 %all-to-all-start = ((bf16[4,64,2048]{2,1,0:T(8,128)(2,1)}), bf16[4,64,2048]{2,1,0:T(8,128)(2,1)S(1)}, u32[]{:S(2)}, u32[]{:S(2)}) async-start(bf16[4,64,2048]{2,1,0:T(8,128)(2,1)} %broadcast_in_dim.16), calls=%async_computation | async-start | bytes 2097152 | tf_op jit(solution)/shard_map/all_to_all | solution.py:309
  6.3 0.3 copy.9
  6.6 1.2 copy.10
  7.9 1.1 copy.8
  9.0 11.6 %all-to-all-done = bf16[4,64,2048]{2,1,0:T(8,128)(2,1)S(1)} async-done(((bf16[4,64,2048]{2,1,0:T(8,128)(2,1)}), bf16[4,64,2048]{2,1,0:T(8,128)(2,1)S(1)}, u32[]{:S(2)}, u32[]{:S(2)}) %all-to-all-start) | async-done | bytes 1048608 | tf_op jit(solution)/shard_map/all_to_all | solution.py:309
  20.6 2.8 %fusion.8.mine = bf16[388,256]{1,0:T(8,128)(2,1)S(1)} fusion(bf16[256,2048]{1,0:T(8,128)(2,1)S(1)} %bitcast.19, bf16[2048,64]{1,0:T(8,128)(2,1)S(1)} %copy.10, bf16[2048,64]{1,0:T(8,128)(2,1)S(1)} %copy.9, bf16[2048,4]{1,0:T(8,128)(2,1)} %copy.8, bf16[2048,256]{1,0:T(8,128)(2,1)} %param.8), kind=kOutput, calls=%fused_computation.9 | convolution fusion | flops 413303808 | bytes 2836480 | tf_op jit(solution)/shard_map/dot_general | solution.py:312
  23.4 3.7 %collective-permute-start = (bf16[260,256]{1,0:T(8,128)(2,1)S(1)}, bf16[260,256]{1,0:T(8,128)(2,1)S(1)}, u32[]{:S(2)}, u32[]{:S(2)}) collective-permute-start(bf16[260,256]{1,0:T(8,128)(2,1)S(1)} %slice.4), channel_id=1, source_target_pairs={{0,4},{4,0},{1,5},{5,1},{2,6},{6,2},{3,7},{7,3},{8,12},{12,8},{9,1... | collective-permute-start | bytes 399368 | tf_op jit(solution)/shard_map/ppermute | solution.py:313
  27.2 0.1 broadcast_in_dim.17
  27.3 0.9 collective-permute-done.theirs
  28.2 0.3 sums.1
  28.5 13.5 %all_to_all.20.row = f32[8,8,128]{2,1,0:T(8,128)S(1)} all-to-all(f32[8,8,128]{2,1,0:T(8,128)S(1)} %broadcast_in_dim.19), channel_id=1, replica_groups=mesh['sp_0'=8,'sp_1'=8,'sp_2'=2,'tp'=4] {'sp_1'}, dimensions={0} | all-to-all | bytes 65536 | tf_op jit(solution)/shard_map/all_to_all | solution.py:317
  42.0 0.9 broadcast_in_dim.20
  42.9 9.4 %all-to-all-start.2 = ((bf16[8,136,256]{2,1,0:T(8,128)(2,1)}), bf16[8,136,256]{2,1,0:T(8,128)(2,1)S(1)}, u32[]{:S(2)}, u32[]{:S(2)}) async-start(bf16[8,136,256]{2,1,0:T(8,128)(2,1)} %broadcast_in_dim.20), calls=%async_computation.2 | async-start | bytes 1114112 | tf_op jit(solution)/shard_map/all_to_all | solution.py:319
  52.3 5.2 %collective-permute-start.1 = (bf16[256,256]{1,0:T(8,128)(2,1)S(1)}, bf16[256,256]{1,0:T(8,128)(2,1)S(1)}, u32[]{:S(2)}, u32[]{:S(2)}) collective-permute-start(bf16[256,256]{1,0:T(8,128)(2,1)S(1)} %get-tuple-element.24), channel_id=1, source_target_pairs={{0,504},{4,508},{8,496},{12,500},{16,488},{20,492},{24,480},{28,48... | collective-permute-start | bytes 393224 | tf_op jit(solution)/shard_map/ppermute | solution.py:316
  57.5 7.7 %collective-permute-done.1.crossed = bf16[256,256]{1,0:T(8,128)(2,1)S(1)} collective-permute-done((bf16[256,256]{1,0:T(8,128)(2,1)S(1)}, bf16[256,256]{1,0:T(8,128)(2,1)S(1)}, u32[]{:S(2)}, u32[]{:S(2)}) %collective-permute-start.1) | collective-permute-done | bytes 131104 | tf_op jit(solution)/shard_map/ppermute | solution.py:316
  65.2 8.5 %all-to-all-done.2.column = bf16[8,136,256]{2,1,0:T(8,128)(2,1)S(1)} async-done(((bf16[8,136,256]{2,1,0:T(8,128)(2,1)}), bf16[8,136,256]{2,1,0:T(8,128)(2,1)S(1)}, u32[]{:S(2)}, u32[]{:S(2)}) %all-to-all-start.2) | async-done | bytes 557088 | tf_op jit(solution)/shard_map/all_to_all | solution.py:319
  73.7 0.9 prepare.1
  74.6 1.9 collective-permute-start.2
  76.5 4.6 %collective-permute-start.3 = (bf16[8,144,256]{2,1,0:T(8,128)(2,1)S(1)}, bf16[8,144,256]{2,1,0:T(8,128)(2,1)S(1)}, u32[]{:S(2)}, u32[]{:S(2)}) collective-permute-start(bf16[8,144,256]{2,1,0:T(8,128)(2,1)S(1)} %get-tuple-element.26.refs_2_), channel_id=1, source_target_pairs={{0,56},{8,0},{16,8},{24,16},{32,24},{40,32},{48,40},{56,48},{1,57}... | collective-permute-start | bytes 1769480 | tf_op jit(solution)/shard_map/ppermute | solution.py:329
  81.1 0.8 copy-done.1
  81.9 8.5 %collective-permute-done.2.refs_2_ = bf16[8,144,256]{2,1,0:T(8,128)(2,1)S(1)} collective-permute-done((bf16[8,144,256]{2,1,0:T(8,128)(2,1)S(1)}, bf16[8,144,256]{2,1,0:T(8,128)(2,1)S(1)}, u32[]{:S(2)}, u32[]{:S(2)}) %collective-permute-start.2) | collective-permute-done | bytes 589856 | tf_op jit(solution)/shard_map/ppermute | solution.py:326
  90.4 1.9 collective-permute-start.4
  92.3 4.6 %collective-permute-start.5 = (bf16[8,144,256]{2,1,0:T(8,128)(2,1)S(1)}, bf16[8,144,256]{2,1,0:T(8,128)(2,1)}, u32[]{:S(2)}, u32[]{:S(2)}) collective-permute-start(bf16[8,144,256]{2,1,0:T(8,128)(2,1)S(1)} %collective-permute-done.3.refs_3_), channel_id=1, source_target_pairs={{0,56},{8,0},{16,8},{24,16},{32,24},{40,32},{48,40},{56,48},{1,57}... | collective-permute-start | bytes 1769480 | tf_op jit(solution)/shard_map/ppermute | solution.py:329
  96.9 8.4 %collective-permute-done.4.refs_2_ = bf16[8,144,256]{2,1,0:T(8,128)(2,1)S(1)} collective-permute-done((bf16[8,144,256]{2,1,0:T(8,128)(2,1)S(1)}, bf16[8,144,256]{2,1,0:T(8,128)(2,1)S(1)}, u32[]{:S(2)}, u32[]{:S(2)}) %collective-permute-start.4) | collective-permute-done | bytes 589856 | tf_op jit(solution)/shard_map/ppermute | solution.py:326
  105.3 1.9 collective-permute-start.6
  107.2 4.6 %collective-permute-start.7 = (bf16[8,144,256]{2,1,0:T(8,128)(2,1)}, bf16[8,144,256]{2,1,0:T(8,128)(2,1)}, u32[]{:S(2)}, u32[]{:S(2)}) collective-permute-start(bf16[8,144,256]{2,1,0:T(8,128)(2,1)} %collective-permute-done.5.refs_3_), channel_id=1, source_target_pairs={{0,56},{8,0},{16,8},{24,16},{32,24},{40,32},{48,40},{56,48},{1,57}... | collective-permute-start | bytes 1769480 | tf_op jit(solution)/shard_map/ppermute | solution.py:329
  111.8 7.7 %collective-permute-done.6.refs_2_ = bf16[8,144,256]{2,1,0:T(8,128)(2,1)} collective-permute-done((bf16[8,144,256]{2,1,0:T(8,128)(2,1)S(1)}, bf16[8,144,256]{2,1,0:T(8,128)(2,1)}, u32[]{:S(2)}, u32[]{:S(2)}) %collective-permute-start.6) | collective-permute-done | bytes 589856 | tf_op jit(solution)/shard_map/ppermute | solution.py:326
  119.5 1.9 collective-permute-start.8
  121.5 0.1 stack.93.refs_0_
  121.6 0.1 stack.105.refs_0_
  121.7 0.1 stack.103.refs_0_
  121.8 0.1 stack.100.refs_0_
  121.9 0.1 stack.97.refs_0_
  122.0 1.1 copy-done.2
  123.1 5.1 %attend.5 = (f32[2,256,256]{2,1,0:T(8,128)S(1)}, f32[2,64,256]{2,1,0:T(8,128)S(1)}) custom-call(s32[6]{0:T(128)S(1)} %stack.93.refs_0_, bf16[8,128,256]{2,1,0:T(8,128)(2,1)S(1)} %get-tuple-element.25.refs_1_, bf16[8,144,256]{2,1,0:T(8,128)(2,1)S(1)} %copy-done.2), custom_call_target="tpu_custom_call" | custom-call | tf_op jit(solution)/shard_map/attend/pallas_call | solution.py:233
  128.2 9.5 %attend.6 = (f32[2,256,256]{2,1,0:T(8,128)S(1)}, f32[2,64,256]{2,1,0:T(8,128)S(1)}) custom-call(s32[6]{0:T(128)S(1)} %stack.97.refs_0_, bf16[8,128,256]{2,1,0:T(8,128)(2,1)S(1)} %get-tuple-element.25.refs_1_, bf16[8,144,256]{2,1,0:T(8,128)(2,1)S(1)} %collective-permute-done.2.refs_2_, bf16[8,144,256]{2,1,0:T(8,128)(2,1)S(1)} %collective-permute-done.3.refs_3_), custom_call_target="tpu_custom_call" | custom-call | tf_op jit(solution)/shard_map/attend/pallas_call | solution.py:233
  137.8 10.2 %attend.7 = (f32[2,256,256]{2,1,0:T(8,128)S(1)}, f32[2,64,256]{2,1,0:T(8,128)S(1)}) custom-call(s32[6]{0:T(128)S(1)} %stack.100.refs_0_, bf16[8,128,256]{2,1,0:T(8,128)(2,1)S(1)} %get-tuple-element.25.refs_1_, bf16[8,144,256]{2,1,0:T(8,128)(2,1)S(1)} %collective-permute-done.4.refs_2_, bf16[8,144,256]{2,1,0:T(8,128)(2,1)} %collective-permute-done.5.refs_3_), custom_call_target="tpu_custom_call" | custom-call | tf_op jit(solution)/shard_map/attend/pallas_call | solution.py:233
  147.9 10.2 %attend.8 = (f32[2,256,256]{2,1,0:T(8,128)S(1)}, f32[2,64,256]{2,1,0:T(8,128)S(1)}) custom-call(s32[6]{0:T(128)S(1)} %stack.103.refs_0_, bf16[8,128,256]{2,1,0:T(8,128)(2,1)S(1)} %get-tuple-element.25.refs_1_, bf16[8,144,256]{2,1,0:T(8,128)(2,1)} %collective-permute-done.6.refs_2_, bf16[8,144,256]{2,1,0:T(8,128)(2,1)} %collective-permute-done.7.refs_3_), custom_call_target="tpu_custom_call" | custom-call | tf_op jit(solution)/shard_map/attend/pallas_call | solution.py:233
  158.1 5.5 %attend.9 = (f32[2,256,256]{2,1,0:T(8,128)S(1)}, f32[2,64,256]{2,1,0:T(8,128)S(1)}) custom-call(s32[6]{0:T(128)S(1)} %stack.105.refs_0_, bf16[8,128,256]{2,1,0:T(8,128)(2,1)S(1)} %get-tuple-element.25.refs_1_, bf16[8,144,256]{2,1,0:T(8,128)(2,1)} %collective-permute-done.8.refs_2_), custom_call_target="tpu_custom_call" | custom-call | tf_op jit(solution)/shard_map/attend/pallas_call | solution.py:233
  163.7 0.8 merge.1
  164.5 6.7 %collective-permute-start.9 = (f32[264,256]{1,0:T(8,128)S(1)}, f32[264,256]{1,0:T(8,128)S(1)}, u32[]{:S(2)}, u32[]{:S(2)}) collective-permute-start(f32[264,256]{1,0:T(8,128)S(1)} %get-tuple-element.38), channel_id=1, source_target_pairs={{0,4},{4,0},{1,5},{5,1},{2,6},{6,2},{3,7},{7,3},{8,12},{12,8},{9,1... | collective-permute-start | bytes 811016 | tf_op jit(solution)/shard_map/ppermute | solution.py:337
  171.2 1.2 collective-permute-done.9.got
  172.4 5.6 %collective-permute-start.10 = (bf16[256,256]{1,0:T(8,128)(2,1)S(1)}, bf16[256,256]{1,0:T(8,128)(2,1)S(1)}, u32[]{:S(2)}, u32[]{:S(2)}) collective-permute-start(bf16[256,256]{1,0:T(8,128)(2,1)S(1)} %finish.1), channel_id=1, source_target_pairs={{4,508},{12,500},{20,492},{28,484},{36,476},{44,468},{52,460},{60,... | collective-permute-start | bytes 393224 | tf_op jit(solution)/shard_map/ppermute | solution.py:340
  178.1 5.2 %collective-permute-done.10 = bf16[256,256]{1,0:T(8,128)(2,1)S(1)} collective-permute-done((bf16[256,256]{1,0:T(8,128)(2,1)S(1)}, bf16[256,256]{1,0:T(8,128)(2,1)S(1)}, u32[]{:S(2)}, u32[]{:S(2)}) %collective-permute-start.10) | collective-permute-done | bytes 131104 | tf_op jit(solution)/shard_map/ppermute | solution.py:340
  183.2 0.5 convolution_convert_fusion
  183.7 12.2 %all_to_all.21 = bf16[4,64,2048]{2,1,0:T(8,128)(2,1)S(1)} all-to-all(bf16[4,64,2048]{2,1,0:T(8,128)(2,1)S(1)} %bitcast.18), channel_id=1, replica_groups=mesh['sp_0'=8,'sp_1'=8,'sp_2'=2,'tp'=4] {'tp'}, dimensions={0} | all-to-all | bytes 2097152 | tf_op jit(solution)/shard_map/all_to_all | solution.py:291
  195.9 0.9 reduce_sum.12
  (22 shorter events, 0.4 us)
Async XLA Ops:
  0.0 183.2 %copy-start = (bf16[256,2048]{1,0:T(8,128)(2,1)S(1)}, bf16[256,2048]{1,0:T(8,128)(2,1)}, u32[]{:S(2)}) copy-start(bf16[256,2048]{1,0:T(8,128)(2,1)} %param.13) | copy-start | bytes 3145732
  2.2 4.1 %copy-start.3 = (bf16[2048,64]{0,1:T(8,128)(2,1)S(1)}, bf16[2048,64]{0,1:T(8,128)(2,1)}, u32[]{:S(2)}) copy-start(bf16[2048,64]{0,1:T(8,128)(2,1)} %param.9) | copy-start | bytes 786436
  2.2 18.4 %all-to-all-start = ((bf16[4,64,2048]{2,1,0:T(8,128)(2,1)}), bf16[4,64,2048]{2,1,0:T(8,128)(2,1)S(1)}, u32[]{:S(2)}, u32[]{:S(2)}) async-start(bf16[4,64,2048]{2,1,0:T(8,128)(2,1)} %broadcast_in_dim.16), calls=%async_computation | async-start | bytes 2097152 | tf_op jit(solution)/shard_map/all_to_all | solution.py:309
  6.3 1.5 copy-start.4
  20.6 6.6 %copy-start.5 = (f32[4]{0:T(128)S(1)}, f32[4]{0:T(128)}, u32[]{:S(2)}) copy-start(f32[4]{0:T(128)} %param.12) | copy-start | bytes 52
  23.4 4.7 %collective-permute-start = (bf16[260,256]{1,0:T(8,128)(2,1)S(1)}, bf16[260,256]{1,0:T(8,128)(2,1)S(1)}, u32[]{:S(2)}, u32[]{:S(2)}) collective-permute-start(bf16[260,256]{1,0:T(8,128)(2,1)S(1)} %slice.4), channel_id=1, source_target_pairs={{0,4},{4,0},{1,5},{5,1},{2,6},{6,2},{3,7},{7,3},{8,12},{12,8},{9,1... | collective-permute-start | bytes 399368 | tf_op jit(solution)/shard_map/ppermute | solution.py:313
  42.9 30.8 %all-to-all-start.2 = ((bf16[8,136,256]{2,1,0:T(8,128)(2,1)}), bf16[8,136,256]{2,1,0:T(8,128)(2,1)S(1)}, u32[]{:S(2)}, u32[]{:S(2)}) async-start(bf16[8,136,256]{2,1,0:T(8,128)(2,1)} %broadcast_in_dim.20), calls=%async_computation.2 | async-start | bytes 1114112 | tf_op jit(solution)/shard_map/all_to_all | solution.py:319
  52.3 12.9 %collective-permute-start.1 = (bf16[256,256]{1,0:T(8,128)(2,1)S(1)}, bf16[256,256]{1,0:T(8,128)(2,1)S(1)}, u32[]{:S(2)}, u32[]{:S(2)}) collective-permute-start(bf16[256,256]{1,0:T(8,128)(2,1)S(1)} %get-tuple-element.24), channel_id=1, source_target_pairs={{0,504},{4,508},{8,496},{12,500},{16,488},{20,492},{24,480},{28,48... | collective-permute-start | bytes 393224 | tf_op jit(solution)/shard_map/ppermute | solution.py:316
  74.6 15.8 %collective-permute-start.2 = (bf16[8,144,256]{2,1,0:T(8,128)(2,1)S(1)}, bf16[8,144,256]{2,1,0:T(8,128)(2,1)S(1)}, u32[]{:S(2)}, u32[]{:S(2)}) collective-permute-start(bf16[8,144,256]{2,1,0:T(8,128)(2,1)S(1)} %get-tuple-element.26.refs_2_), channel_id=1, source_target_pairs={{0,8},{8,16},{16,24},{24,32},{32,40},{40,48},{48,56},{56,0},{1,9},... | collective-permute-start | bytes 1769480 | tf_op jit(solution)/shard_map/ppermute | solution.py:326
  76.5 15.8 %collective-permute-start.3 = (bf16[8,144,256]{2,1,0:T(8,128)(2,1)S(1)}, bf16[8,144,256]{2,1,0:T(8,128)(2,1)S(1)}, u32[]{:S(2)}, u32[]{:S(2)}) collective-permute-start(bf16[8,144,256]{2,1,0:T(8,128)(2,1)S(1)} %get-tuple-element.26.refs_2_), channel_id=1, source_target_pairs={{0,56},{8,0},{16,8},{24,16},{32,24},{40,32},{48,40},{56,48},{1,57}... | collective-permute-start | bytes 1769480 | tf_op jit(solution)/shard_map/ppermute | solution.py:329
  81.1 0.8 copy-start.1
  90.4 14.9 %collective-permute-start.4 = (bf16[8,144,256]{2,1,0:T(8,128)(2,1)S(1)}, bf16[8,144,256]{2,1,0:T(8,128)(2,1)S(1)}, u32[]{:S(2)}, u32[]{:S(2)}) collective-permute-start(bf16[8,144,256]{2,1,0:T(8,128)(2,1)S(1)} %collective-permute-done.2.refs_2_), channel_id=1, source_target_pairs={{0,8},{8,16},{16,24},{24,32},{32,40},{40,48},{48,56},{56,0},{1,9},... | collective-permute-start | bytes 1769480 | tf_op jit(solution)/shard_map/ppermute | solution.py:326
  92.3 14.9 %collective-permute-start.5 = (bf16[8,144,256]{2,1,0:T(8,128)(2,1)S(1)}, bf16[8,144,256]{2,1,0:T(8,128)(2,1)}, u32[]{:S(2)}, u32[]{:S(2)}) collective-permute-start(bf16[8,144,256]{2,1,0:T(8,128)(2,1)S(1)} %collective-permute-done.3.refs_3_), channel_id=1, source_target_pairs={{0,56},{8,0},{16,8},{24,16},{32,24},{40,32},{48,40},{56,48},{1,57}... | collective-permute-start | bytes 1769480 | tf_op jit(solution)/shard_map/ppermute | solution.py:329
  105.3 14.2 %collective-permute-start.6 = (bf16[8,144,256]{2,1,0:T(8,128)(2,1)S(1)}, bf16[8,144,256]{2,1,0:T(8,128)(2,1)}, u32[]{:S(2)}, u32[]{:S(2)}) collective-permute-start(bf16[8,144,256]{2,1,0:T(8,128)(2,1)S(1)} %collective-permute-done.4.refs_2_), channel_id=1, source_target_pairs={{0,8},{8,16},{16,24},{24,32},{32,40},{40,48},{48,56},{56,0},{1,9},... | collective-permute-start | bytes 1769480 | tf_op jit(solution)/shard_map/ppermute | solution.py:326
  107.2 40.7 %collective-permute-start.7 = (bf16[8,144,256]{2,1,0:T(8,128)(2,1)}, bf16[8,144,256]{2,1,0:T(8,128)(2,1)}, u32[]{:S(2)}, u32[]{:S(2)}) collective-permute-start(bf16[8,144,256]{2,1,0:T(8,128)(2,1)} %collective-permute-done.5.refs_3_), channel_id=1, source_target_pairs={{0,56},{8,0},{16,8},{24,16},{32,24},{40,32},{48,40},{56,48},{1,57}... | collective-permute-start | bytes 1769480 | tf_op jit(solution)/shard_map/ppermute | solution.py:329
  119.5 38.6 %collective-permute-start.8 = (bf16[8,144,256]{2,1,0:T(8,128)(2,1)}, bf16[8,144,256]{2,1,0:T(8,128)(2,1)}, u32[]{:S(2)}, u32[]{:S(2)}) collective-permute-start(bf16[8,144,256]{2,1,0:T(8,128)(2,1)} %collective-permute-done.6.refs_2_), channel_id=1, source_target_pairs={{0,8},{8,16},{16,24},{24,32},{32,40},{40,48},{48,56},{56,0},{1,9},... | collective-permute-start | bytes 1769480 | tf_op jit(solution)/shard_map/ppermute | solution.py:326
  122.0 1.1 copy-start.2
  164.5 7.8 %collective-permute-start.9 = (f32[264,256]{1,0:T(8,128)S(1)}, f32[264,256]{1,0:T(8,128)S(1)}, u32[]{:S(2)}, u32[]{:S(2)}) collective-permute-start(f32[264,256]{1,0:T(8,128)S(1)} %get-tuple-element.38), channel_id=1, source_target_pairs={{0,4},{4,0},{1,5},{5,1},{2,6},{6,2},{3,7},{7,3},{8,12},{12,8},{9,1... | collective-permute-start | bytes 811016 | tf_op jit(solution)/shard_map/ppermute | solution.py:337
  172.4 10.8 %collective-permute-start.10 = (bf16[256,256]{1,0:T(8,128)(2,1)S(1)}, bf16[256,256]{1,0:T(8,128)(2,1)S(1)}, u32[]{:S(2)}, u32[]{:S(2)}) collective-permute-start(bf16[256,256]{1,0:T(8,128)(2,1)S(1)} %finish.1), channel_id=1, source_target_pairs={{4,508},{12,500},{20,492},{28,484},{36,476},{44,468},{52,460},{60,... | collective-permute-start | bytes 393224 | tf_op jit(solution)/shard_map/ppermute | solution.py:340

commit v5 on v4

--- a/solution.py
+++ b/solution.py
@@ -11,6 +11,7 @@
 NEG = -1e30
 LOW = -1e20
 PIECES = 4
+LOADAT = 3
 SMALL = pltpu.CompilerParams(vmem_limit_bytes=8 * 1024 * 1024)
 
 
@@ -88,7 +89,7 @@
 
 
 def prepare_kernel(info, column, even, crossed, bias, chunk, rhs, *, rows, cols, blk):
-    core, col = info[0], info[1]
+    core, col = info[0], info[3]
     last = column[:, 128:136, :].astype(f32)
     logs = log_sigmoid(last + bias[...][None, :, :1]).reshape(rows * 8, blk)
     tri = (lax.broadcasted_iota(jnp.int32, (blk, blk), 0) <= lax.broadcasted_iota(jnp.int32, (blk, blk), 1)).astype(bf16)
@@ -106,7 +107,7 @@
         chunk[i, 0:64] = column[i, 0:64, :]
         chunk[i, 80:144] = column[i, 64:128, :]
     row16 = lax.broadcasted_iota(jnp.int32, (16, blk), 0)
-    swap = info[2] == 1
+    swap = info[4] == 1
     for side in range(2):
         for h in range(4):
             s = slice(h * HEAD, (h + 1) * HEAD)
@@ -125,7 +126,8 @@
     )(info, column, even, crossed, bias8)
 
 
-def attend_kernel(*refs, count, rows, cols, blk):
+def attend_kernel(*refs, steps_away, rows, cols, blk):
+    count = len(steps_away)
     info, rhs = refs[:2]
     chunks = refs[2:2 + count]
     acc, stat = refs[2 + count:4 + count]
@@ -139,7 +141,7 @@
         stat[side, 32:64] = jnp.full((32, blk), LOW, f32)
     for n in range(count):
         kv = chunks[n]
-        col = info[3 + n]
+        col = lax.rem(info[3] + (steps_away[n] + cols), cols)
         ahead = [jnp.clip((info[1 + side] - col + cols - 1) // cols, 0, rows) for side in range(2)]
         diag = [(info[1 + side] - col) % cols == 0 for side in range(2)]
         full = [jnp.where(diag[side], ahead[side], ahead[side] + 1) // 2 for side in range(2)]
@@ -199,8 +201,9 @@
                 slot = it & 1
                 side, jj = place(it)
                 side_next, jj_next = place(jnp.minimum(it + 1, steps - 1))
-                load_keys(1 - slot, jj_next, jnp.where(side_next == 0, ahead[0], ahead[1]))
                 for h in range(4):
+                    if h == LOADAT:
+                        load_keys(1 - slot, jj_next, jnp.where(side_next == 0, ahead[0], ahead[1]))
                     nxt = ((h + 1) & 1, slot, side, h + 1) if h < 3 else (0, 1 - slot, side_next, 0)
                     fused(nxt, (h & 1, jj, side, h))
                 return carry
@@ -212,7 +215,7 @@
             def _():
                 chip = jnp.where(side == 0, info[1], info[2])
                 jj = jnp.clip(jnp.where(side == 0, full[0], full[1]), 0, rows // 2 - 1)
-                par = jnp.where(side == 0, info[5], 1 - info[5])
+                par = jnp.where(side == 0, info[4], 1 - info[4])
                 qpos = (2 * chip + par) * blk + lax.broadcasted_iota(jnp.int32, (2 * blk, blk), 1)
                 row = lax.broadcasted_iota(jnp.int32, (2 * blk, blk), 0)
                 upper = (row >= blk).astype(jnp.int32)
@@ -228,10 +231,10 @@
         lax.fori_loop(0, 2, edge, 0)
 
 
-def attend(info, rhs, chunks, cols):
+def attend(info, rhs, chunks, steps_away, cols):
     rows, _, blk = chunks[0].shape
     return pl.pallas_call(
-        functools.partial(attend_kernel, count=len(chunks), rows=rows, cols=cols, blk=blk),
+        functools.partial(attend_kernel, steps_away=steps_away, rows=rows, cols=cols, blk=blk),
         out_shape=(jax.ShapeDtypeStruct((2, 256, blk), f32), jax.ShapeDtypeStruct((2, 64, blk), f32)),
         in_specs=[scalars(), *vmem(1 + len(chunks))], out_specs=tuple(vmem(2)),
         scratch_shapes=[pltpu.VMEM((2, 2 * blk, 128), bf16), pltpu.VMEM((2, 2 * blk, blk), f32), pltpu.VMEM((2, 8, blk), f32)],
@@ -243,7 +246,7 @@
     info, accs, stats = refs[0], refs[1:1 + count], refs[1 + count:1 + 2 * count]
     keep, give = refs[1 + 2 * count:]
     for which in range(2):
-        dst, side = (keep, give)[which], info[which]
+        dst, side = (keep, give)[which], info[5] if which == 0 else 1 - info[5]
         for h in range(4):
             tops = [s[side, 32 + 8 * h:40 + 8 * h] for s in stats]
             top = functools.reduce(jnp.maximum, tops)
@@ -268,9 +271,11 @@
     peak = jnp.maximum(keep[256:260], got[256:260])
     wa, wb = jnp.exp(keep[256:260] - peak), jnp.exp(got[256:260] - peak)
     mass = keep[260:264] * wa + got[260:264] * wb
+    heads = []
     for h in range(4):
         s = slice(h * HEAD, (h + 1) * HEAD)
-        out[s] = ((keep[s] * wa[h:h + 1] + got[s] * wb[h:h + 1]) / mass[h:h + 1]).astype(bf16)
+        heads.append((keep[s] * wa[h:h + 1] + got[s] * wb[h:h + 1]) / mass[h:h + 1])
+    out[...] = jnp.concatenate(heads, axis=0).T.astype(bf16)
 
 
 def finish(keep, got):
@@ -278,18 +283,29 @@
                           compiler_params=SMALL, name="finish")(keep, got)
 
 
+def project_kernel(info, heads, *refs, shifts):
+    weights, out = refs[:-1], refs[-1]
+    total = None
+    for k, shift in enumerate(shifts):
+        part = dot(heads[lax.rem(info[6] + (4 - shift), 4)], weights[k][...]).astype(bf16).astype(f32)
+        total = part if total is None else total + part
+    out[...] = total.astype(bf16)
+
+
+def project(info, heads, weights, shifts):
+    shape = jax.ShapeDtypeStruct((heads.shape[1], weights[0].shape[1]), bf16)
+    return pl.pallas_call(
+        functools.partial(project_kernel, shifts=shifts), out_shape=shape, in_specs=[scalars(), *vmem(1 + len(weights))],
+        out_specs=vmem(1)[0], compiler_params=pltpu.CompilerParams(vmem_limit_bytes=16 * 1024 * 1024), name="project",
+    )(info, heads, *weights)
+
+
 SP = ("sp_0", "sp_1", "sp_2")
 SP_TP = ("sp_0", "sp_1", "sp_2", "tp")
 
 
 def ring(count, step):
     return [(i, (i + step) % count) for i in range(count)]
-
-
-def sum_at_owner(value):
-    pieces = value.reshape(4, value.shape[0] // 4, value.shape[1])
-    arrived = lax.all_to_all(pieces, "tp", split_axis=0, concat_axis=0, tiled=True)
-    return arrived.astype(f32).sum(axis=0)
 
 
 def shards(tokens, w_query, w_key, w_value, w_gate, gate_bias, w_output):
@@ -300,10 +316,9 @@
     other = chips - 1 - chip
     behind = (chip > other).astype(jnp.int32)
     low, high = jnp.minimum(chip, other), jnp.maximum(chip, other)
+    mine = jnp.where(behind == 1, 1 - core, core)
+    info = jnp.stack([jnp.asarray(v, jnp.int32) for v in (core, low, high, col, behind, mine, lax.axis_index("tp"))])
     bias8 = jnp.broadcast_to(jnp.tile(gate_bias, 2)[:, None], (8, 128))
-
-    def scalar_row(*values):
-        return jnp.stack([jnp.asarray(v, jnp.int32) for v in values])
 
     copies = jnp.broadcast_to(tokens, (4, *tokens.shape))
     here = lax.all_to_all(copies, "tp", split_axis=0, concat_axis=0, tiled=True)
@@ -311,36 +326,38 @@
     joined = jnp.concatenate([w_query, w_gate, w_key, w_value], axis=1)
     projected = lax.dot_general(joined, here, (((0,), (1,)), ((), ())), preferred_element_type=f32).astype(bf16)
     swapped = lax.ppermute(projected[:260], "sp_2", [(0, 1), (1, 0)])
-    total, even, odd = sums(scalar_row(core), projected, swapped, bias8)
+    total, even, odd = sums(info, projected, swapped, bias8)
     far = [(2 * c + e, 2 * (chips - 1 - c) + e) for c in range(chips) for e in range(2)]
     crossed = lax.ppermute(odd, SP, far)
     row = lax.all_to_all(jnp.broadcast_to(total, (cols, *total.shape)), "sp_1", split_axis=0, concat_axis=0, tiled=True)
     payload = pack(projected, total, row)
     column = lax.all_to_all(jnp.broadcast_to(payload, (rows, *payload.shape)), "sp_0", split_axis=0, concat_axis=0, tiled=True)
-    own, rhs = prepare(scalar_row(core, col, behind), column, even, crossed, bias8, cols)
+    shifts, weights = (0, 1, 3, 2), [w_output]
+    for shift in shifts[1:]:
+        weights.append(lax.ppermute(w_output, "tp", ring(4, shift)))
+    own, rhs = prepare(info, column, even, crossed, bias8, cols)
 
     parts = []
     up, down = own, own
-    pending, where = [own], [col]
+    pending, where = [own], (0,)
     for step in range(1, cols // 2 + 1):
         up = lax.ppermute(up, "sp_1", ring(cols, 1))
-        following, places = [up], [(col - step) % cols]
+        following, places = [up], (-step,)
         if 2 * step < cols:
             down = lax.ppermute(down, "sp_1", ring(cols, -1))
             following.append(down)
-            places.append((col + step) % cols)
-        parts.append(attend(scalar_row(core, low, high, where[0], where[-1], behind), rhs, pending, cols))
+            places = (-step, step)
+        parts.append(attend(info, rhs, pending, where, cols))
         pending, where = following, places
-    parts.append(attend(scalar_row(core, low, high, where[0], where[-1], behind), rhs, pending, cols))
-    mine = jnp.where(behind == 1, 1 - core, core)
-    keep, give = merge(scalar_row(mine, 1 - mine), parts)
+    parts.append(attend(info, rhs, pending, where, cols))
+    keep, give = merge(info, parts)
     got = lax.ppermute(give, "sp_2", [(0, 1), (1, 0)])
     attended = finish(keep, got)
     back = [(2 * c + 1, 2 * (chips - 1 - c) + 1) for c in range(chips)]
     returned = lax.ppermute(attended, SP, back)
     attended = jnp.where(core == 0, attended, returned)
-    partial = lax.dot_general(attended, w_output, (((0,), (0,)), ((), ())), preferred_element_type=f32).astype(bf16)
-    return sum_at_owner(partial).astype(bf16)
+    heads = lax.all_to_all(attended.reshape(4, -1, attended.shape[1]), "tp", split_axis=0, concat_axis=0, tiled=True)
+    return project(info, heads, weights, shifts)
 
 
 def solution(mesh):

time: 198 us -> 201 us (1.015)
  starting transfers between devices: 56.1 us -> 68.5 us
  blocking collectives: 25.7 us -> 13.5 us
  waiting for transfers between devices: 59.5 us -> 66.6 us
  local copies, waits for them, and re-layouts: 8.13 us -> 4.22 us
    all_to_all x1 -> x0, blocking collectives: 12.2 us -> none  [sum_at_owner(): lax.all_to_all(pieces, 'tp', split_axis=0, concat_axis=0, tiled=True)]
    ppermute x0 -> x3, starting transfers between devices: none -> 7.81 us  [shards(): weights.append(lax.ppermute(w_output, 'tp', ring(4, shift)))]
    all_to_all x0 -> x1, waiting for transfers between devices: none -> 4.81 us  [shards(): lax.all_to_all(attended.reshape(4, -1, attended.shape[1]), 'tp', split_ax...]
    all_to_all x0 -> x1, starting transfers between devices: none -> 3.9 us  [shards(): lax.all_to_all(attended.reshape(4, -1, attended.shape[1]), 'tp', split_ax...]
    unnamed x15 -> x13, local copies, waits for them, and re-layouts: 4.52 us -> 1.07 us
    pallas_call x5 -> x6, Pallas kernels: 40.5 us -> 41.1 us  [the longest x5 38 us: attend(): pl.pallas_call(functools.partial(attend_kernel, steps_away=steps_away, ro...]
  transfers between devices with their start and end apart: 13 -> 17, of which waited for: 9 -> 10; matrix products, arithmetic and copies ran while one was open for 2% -> 1% of each run, Pallas kernels for 18% -> 19%
where the time goes in v5:
time: 201 us; the launch traced here: 200 us
  starting transfers between devices  68.5 us (34%)
  waiting for transfers between devices  66.6 us (33%)
  Pallas kernels  43.7 us (22%)
  blocking collectives  13.5 us (7%)
  local copies, waits for them, and re-layouts  4.22 us (2%)
  matrix products  2.68 us (1%)
    pallas_call x5, Pallas kernels, attend(): pl.pallas_call(functools.partial(attend_kernel, steps_away=steps_away, ro...  38 us
    ppermute x4, waiting for transfers between devices, shards(): up = lax.ppermute(up, 'sp_1', ring(cols, 1))  25.3 us
    ppermute x3, starting transfers between devices, shards(): down = lax.ppermute(down, 'sp_1', ring(cols, -1))  13.7 us
    all_to_all x1, blocking collectives, shards(): lax.all_to_all(jnp.broadcast_to(total, (cols, *total.shape)), 'sp_1', spl...  13.5 us
    all_to_all x1, waiting for transfers between devices, shards(): here = lax.all_to_all(copies, 'tp', split_axis=0, concat_axis=0, tiled=True)  13.2 us
    all_to_all x1, starting transfers between devices, shards(): lax.all_to_all(jnp.broadcast_to(payload, (rows, *payload.shape)), 'sp_0',...  9.54 us
    all_to_all x1, waiting for transfers between devices, shards(): lax.all_to_all(jnp.broadcast_to(payload, (rows, *payload.shape)), 'sp_0',...  8.46 us
    ppermute x3, starting transfers between devices, shards(): weights.append(lax.ppermute(w_output, 'tp', ring(4, shift)))  7.81 us
  transfers between devices with their start and end apart: 17, of which 10 were waited for; matrix products, arithmetic and copies ran while one was open for 1% of the time, Pallas kernels for 19%

profile of v5, /device:TPU:65, one launch (start us, length us, event | category | flops | bytes accessed | tf_op | source)
XLA Modules:
  0.0 200.2 jit_solution(11354666549238226154)
XLA Ops:
  0.0 2.0 %broadcast_in_dim.16 = bf16[4,64,2048]{2,1,0:T(8,128)(2,1)} broadcast(bf16[64,2048]{1,0:T(8,128)(2,1)} %param.7), dimensions={1,2} | broadcast | bytes 1310720 | tf_op jit(solution)/shard_map/broadcast_in_dim | solution.py:323
  2.1 4.1 %all-to-all-start = ((bf16[4,64,2048]{2,1,0:T(8,128)(2,1)}), bf16[4,64,2048]{2,1,0:T(8,128)(2,1)S(1)}, u32[]{:S(2)}, u32[]{:S(2)}) async-start(bf16[4,64,2048]{2,1,0:T(8,128)(2,1)} %broadcast_in_dim.16), calls=%async_computation | async-start | bytes 2097152 | tf_op jit(solution)/shard_map/all_to_all | solution.py:324
  6.2 0.3 copy.9
  6.5 0.3 copy.10
  6.8 0.1 copy-done.3
  6.9 0.4 copy.8
  7.3 13.2 %all-to-all-done = bf16[4,64,2048]{2,1,0:T(8,128)(2,1)S(1)} async-done(((bf16[4,64,2048]{2,1,0:T(8,128)(2,1)}), bf16[4,64,2048]{2,1,0:T(8,128)(2,1)S(1)}, u32[]{:S(2)}, u32[]{:S(2)}) %all-to-all-start) | async-done | bytes 1048608 | tf_op jit(solution)/shard_map/all_to_all | solution.py:324
  20.4 2.7 %fusion.8.mine = bf16[388,256]{1,0:T(8,128)(2,1)S(1)} fusion(bf16[256,2048]{1,0:T(8,128)(2,1)S(1)} %bitcast.10, bf16[2048,64]{1,0:T(8,128)(2,1)S(1)} %copy.10, bf16[2048,64]{1,0:T(8,128)(2,1)S(1)} %copy.9, bf16[2048,4]{1,0:T(8,128)(2,1)S(1)} %copy.8, bf16[2048,256]{1,0:T(8,128)(2,1)} %param.8), kind=kOutput, calls=%fused_computation.8 | convolution fusion | flops 413303808 | bytes 2836480 | tf_op jit(solution)/shard_map/dot_general | solution.py:327
  23.1 3.7 %collective-permute-start = (bf16[260,256]{1,0:T(8,128)(2,1)S(1)}, bf16[260,256]{1,0:T(8,128)(2,1)S(1)}, u32[]{:S(2)}, u32[]{:S(2)}) collective-permute-start(bf16[260,256]{1,0:T(8,128)(2,1)S(1)} %slice.4), channel_id=1, source_target_pairs={{0,4},{4,0},{1,5},{5,1},{2,6},{6,2},{3,7},{7,3},{8,12},{12,8},{9,1... | collective-permute-start | bytes 399368 | tf_op jit(solution)/shard_map/ppermute | solution.py:328
  26.9 0.1 broadcast_in_dim.17
  27.0 0.1 stack.31.info.refs_0_
  27.1 0.8 collective-permute-done.theirs
  27.9 0.8 sums.1
  28.7 13.5 %all_to_all.20.row = f32[8,8,128]{2,1,0:T(8,128)S(1)} all-to-all(f32[8,8,128]{2,1,0:T(8,128)S(1)} %broadcast_in_dim.19), channel_id=1, replica_groups=mesh['sp_0'=8,'sp_1'=8,'sp_2'=2,'tp'=4] {'sp_1'}, dimensions={0} | all-to-all | bytes 65536 | tf_op jit(solution)/shard_map/all_to_all | solution.py:332
  42.3 0.8 broadcast_in_dim.20
  43.1 9.5 %all-to-all-start.2 = ((bf16[8,136,256]{2,1,0:T(8,128)(2,1)}), bf16[8,136,256]{2,1,0:T(8,128)(2,1)S(1)}, u32[]{:S(2)}, u32[]{:S(2)}) async-start(bf16[8,136,256]{2,1,0:T(8,128)(2,1)} %broadcast_in_dim.20), calls=%async_computation.2 | async-start | bytes 1114112 | tf_op jit(solution)/shard_map/all_to_all | solution.py:334
  52.6 5.2 %collective-permute-start.1 = (bf16[256,256]{1,0:T(8,128)(2,1)S(1)}, bf16[256,256]{1,0:T(8,128)(2,1)S(1)}, u32[]{:S(2)}, u32[]{:S(2)}) collective-permute-start(bf16[256,256]{1,0:T(8,128)(2,1)S(1)} %get-tuple-element.24), channel_id=1, source_target_pairs={{0,504},{4,508},{8,496},{12,500},{16,488},{20,492},{24,480},{28,48... | collective-permute-start | bytes 393224 | tf_op jit(solution)/shard_map/ppermute | solution.py:331
  57.8 7.8 %collective-permute-done.1.crossed = bf16[256,256]{1,0:T(8,128)(2,1)S(1)} collective-permute-done((bf16[256,256]{1,0:T(8,128)(2,1)S(1)}, bf16[256,256]{1,0:T(8,128)(2,1)S(1)}, u32[]{:S(2)}, u32[]{:S(2)}) %collective-permute-start.1) | collective-permute-done | bytes 131104 | tf_op jit(solution)/shard_map/ppermute | solution.py:331
  65.6 8.5 %all-to-all-done.2.column = bf16[8,136,256]{2,1,0:T(8,128)(2,1)S(1)} async-done(((bf16[8,136,256]{2,1,0:T(8,128)(2,1)}), bf16[8,136,256]{2,1,0:T(8,128)(2,1)S(1)}, u32[]{:S(2)}, u32[]{:S(2)}) %all-to-all-start.2) | async-done | bytes 557088 | tf_op jit(solution)/shard_map/all_to_all | solution.py:334
  74.1 0.9 prepare.1
  75.0 1.9 collective-permute-start.2
  76.9 4.6 %collective-permute-start.3 = (bf16[8,144,256]{2,1,0:T(8,128)(2,1)S(1)}, bf16[8,144,256]{2,1,0:T(8,128)(2,1)S(1)}, u32[]{:S(2)}, u32[]{:S(2)}) collective-permute-start(bf16[8,144,256]{2,1,0:T(8,128)(2,1)S(1)} %get-tuple-element.26.refs_2_), channel_id=1, source_target_pairs={{0,56},{8,0},{16,8},{24,16},{32,24},{40,32},{48,40},{56,48},{1,57}... | collective-permute-start | bytes 1769480 | tf_op jit(solution)/shard_map/ppermute | solution.py:347
  81.5 9.3 %collective-permute-done.2.refs_2_ = bf16[8,144,256]{2,1,0:T(8,128)(2,1)S(1)} collective-permute-done((bf16[8,144,256]{2,1,0:T(8,128)(2,1)S(1)}, bf16[8,144,256]{2,1,0:T(8,128)(2,1)S(1)}, u32[]{:S(2)}, u32[]{:S(2)}) %collective-permute-start.2) | collective-permute-done | bytes 589856 | tf_op jit(solution)/shard_map/ppermute | solution.py:344
  90.8 1.9 collective-permute-start.4
  92.7 4.6 %collective-permute-start.5 = (bf16[8,144,256]{2,1,0:T(8,128)(2,1)S(1)}, bf16[8,144,256]{2,1,0:T(8,128)(2,1)S(1)}, u32[]{:S(2)}, u32[]{:S(2)}) collective-permute-start(bf16[8,144,256]{2,1,0:T(8,128)(2,1)S(1)} %collective-permute-done.3.refs_3_), channel_id=1, source_target_pairs={{0,56},{8,0},{16,8},{24,16},{32,24},{40,32},{48,40},{56,48},{1,57}... | collective-permute-start | bytes 1769480 | tf_op jit(solution)/shard_map/ppermute | solution.py:347
  97.3 8.4 %collective-permute-done.4.refs_2_ = bf16[8,144,256]{2,1,0:T(8,128)(2,1)S(1)} collective-permute-done((bf16[8,144,256]{2,1,0:T(8,128)(2,1)S(1)}, bf16[8,144,256]{2,1,0:T(8,128)(2,1)S(1)}, u32[]{:S(2)}, u32[]{:S(2)}) %collective-permute-start.4) | collective-permute-done | bytes 589856 | tf_op jit(solution)/shard_map/ppermute | solution.py:344
  105.7 1.9 collective-permute-start.6
  107.6 4.6 %collective-permute-start.7 = (bf16[8,144,256]{2,1,0:T(8,128)(2,1)S(1)}, bf16[8,144,256]{2,1,0:T(8,128)(2,1)S(1)}, u32[]{:S(2)}, u32[]{:S(2)}) collective-permute-start(bf16[8,144,256]{2,1,0:T(8,128)(2,1)S(1)} %collective-permute-done.5.refs_3_), channel_id=1, source_target_pairs={{0,56},{8,0},{16,8},{24,16},{32,24},{40,32},{48,40},{56,48},{1,57}... | collective-permute-start | bytes 1769480 | tf_op jit(solution)/shard_map/ppermute | solution.py:347
  112.2 7.6 %collective-permute-done.6.refs_2_ = bf16[8,144,256]{2,1,0:T(8,128)(2,1)S(1)} collective-permute-done((bf16[8,144,256]{2,1,0:T(8,128)(2,1)S(1)}, bf16[8,144,256]{2,1,0:T(8,128)(2,1)S(1)}, u32[]{:S(2)}, u32[]{:S(2)}) %collective-permute-start.6) | collective-permute-done | bytes 589856 | tf_op jit(solution)/shard_map/ppermute | solution.py:344
  119.8 1.9 collective-permute-start.8
  121.7 2.8 %collective-permute-start.12 = (bf16[256,2048]{1,0:T(8,128)(2,1)S(1)}, bf16[256,2048]{1,0:T(8,128)(2,1)S(1)}, u32[]{:S(2)}, u32[]{:S(2)}) collective-permute-start(bf16[256,2048]{1,0:T(8,128)(2,1)S(1)} %copy-done), channel_id=1, source_target_pairs={{0,3},{1,0},{2,1},{3,2},{4,7},{5,4},{6,5},{7,6},{8,11},{9,8},{10,9... | collective-permute-start | bytes 3145736 | tf_op jit(solution)/shard_map/ppermute | solution.py:337
  124.5 2.5 %collective-permute-start.11 = (bf16[256,2048]{1,0:T(8,128)(2,1)S(1)}, bf16[256,2048]{1,0:T(8,128)(2,1)}, u32[]{:S(2)}, u32[]{:S(2)}) collective-permute-start(bf16[256,2048]{1,0:T(8,128)(2,1)S(1)} %copy-done), channel_id=1, source_target_pairs={{0,1},{1,2},{2,3},{3,0},{4,5},{5,6},{6,7},{7,4},{8,9},{9,10},{10,1... | collective-permute-start | bytes 3145736 | tf_op jit(solution)/shard_map/ppermute | solution.py:337
  127.0 2.5 %collective-permute-start.13 = (bf16[256,2048]{1,0:T(8,128)(2,1)S(1)}, bf16[256,2048]{1,0:T(8,128)(2,1)}, u32[]{:S(2)}, u32[]{:S(2)}) collective-permute-start(bf16[256,2048]{1,0:T(8,128)(2,1)S(1)} %copy-done), channel_id=1, source_target_pairs={{0,2},{1,3},{2,0},{3,1},{4,6},{5,7},{6,4},{7,5},{8,10},{9,11},{10,... | collective-permute-start | bytes 3145736 | tf_op jit(solution)/shard_map/ppermute | solution.py:337
  129.5 5.1 %attend.5 = (f32[2,256,256]{2,1,0:T(8,128)S(1)}, f32[2,64,256]{2,1,0:T(8,128)S(1)}) custom-call(s32[7]{0:T(128)S(1)} %stack.31.info.refs_0_, bf16[8,128,256]{2,1,0:T(8,128)(2,1)S(1)} %get-tuple-element.25.refs_1_, bf16[8,144,256]{2,1,0:T(8,128)(2,1)S(1)} %get-tuple-element.26.refs_2_), custom_call_target="tpu_custom_call" | custom-call | tf_op jit(solution)/shard_map/attend/pallas_call | solution.py:236
  134.6 9.4 %attend.6 = (f32[2,256,256]{2,1,0:T(8,128)S(1)}, f32[2,64,256]{2,1,0:T(8,128)S(1)}) custom-call(s32[7]{0:T(128)S(1)} %stack.31.info.refs_0_, bf16[8,128,256]{2,1,0:T(8,128)(2,1)S(1)} %get-tuple-element.25.refs_1_, bf16[8,144,256]{2,1,0:T(8,128)(2,1)S(1)} %collective-permute-done.2.refs_2_, bf16[8,144,256]{2,1,0:T(8,128)(2,1)S(1)} %collective-permute-done.3.refs_3_), custom_call_target="tpu_custom_call" | custom-call | tf_op jit(solution)/shard_map/attend/pallas_call | solution.py:236
  144.0 9.4 %attend.7 = (f32[2,256,256]{2,1,0:T(8,128)S(1)}, f32[2,64,256]{2,1,0:T(8,128)S(1)}) custom-call(s32[7]{0:T(128)S(1)} %stack.31.info.refs_0_, bf16[8,128,256]{2,1,0:T(8,128)(2,1)S(1)} %get-tuple-element.25.refs_1_, bf16[8,144,256]{2,1,0:T(8,128)(2,1)S(1)} %collective-permute-done.4.refs_2_, bf16[8,144,256]{2,1,0:T(8,128)(2,1)S(1)} %collective-permute-done.5.refs_3_), custom_call_target="tpu_custom_call" | custom-call | tf_op jit(solution)/shard_map/attend/pallas_call | solution.py:236
  153.4 9.2 %attend.8 = (f32[2,256,256]{2,1,0:T(8,128)S(1)}, f32[2,64,256]{2,1,0:T(8,128)S(1)}) custom-call(s32[7]{0:T(128)S(1)} %stack.31.info.refs_0_, bf16[8,128,256]{2,1,0:T(8,128)(2,1)S(1)} %get-tuple-element.25.refs_1_, bf16[8,144,256]{2,1,0:T(8,128)(2,1)S(1)} %collective-permute-done.6.refs_2_, bf16[8,144,256]{2,1,0:T(8,128)(2,1)S(1)} %collective-permute-done.7.refs_3_), custom_call_target="tpu_custom_call" | custom-call | tf_op jit(solution)/shard_map/attend/pallas_call | solution.py:236
  162.7 4.9 %attend.9 = (f32[2,256,256]{2,1,0:T(8,128)S(1)}, f32[2,64,256]{2,1,0:T(8,128)S(1)}) custom-call(s32[7]{0:T(128)S(1)} %stack.31.info.refs_0_, bf16[8,128,256]{2,1,0:T(8,128)(2,1)S(1)} %get-tuple-element.25.refs_1_, bf16[8,144,256]{2,1,0:T(8,128)(2,1)S(1)} %collective-permute-done.8.refs_2_), custom_call_target="tpu_custom_call" | custom-call | tf_op jit(solution)/shard_map/attend/pallas_call | solution.py:236
  167.6 0.8 merge.1
  168.4 7.2 %collective-permute-start.9 = (f32[264,256]{1,0:T(8,128)S(1)}, f32[264,256]{1,0:T(8,128)S(1)}, u32[]{:S(2)}, u32[]{:S(2)}) collective-permute-start(f32[264,256]{1,0:T(8,128)S(1)} %get-tuple-element.38), channel_id=1, source_target_pairs={{0,4},{4,0},{1,5},{5,1},{2,6},{6,2},{3,7},{7,3},{8,12},{12,8},{9,1... | collective-permute-start | bytes 811016 | tf_op jit(solution)/shard_map/ppermute | solution.py:354
  175.6 1.2 collective-permute-done.9.got
  176.7 0.1 finish.1
  176.9 5.7 %collective-permute-start.10 = (bf16[256,256]{1,0:T(8,128)(2,1)S(1)}, bf16[256,256]{1,0:T(8,128)(2,1)S(1)}, u32[]{:S(2)}, u32[]{:S(2)}) collective-permute-start(bf16[256,256]{1,0:T(8,128)(2,1)S(1)} %finish.1), channel_id=1, source_target_pairs={{4,508},{12,500},{20,492},{28,484},{36,476},{44,468},{52,460},{60,... | collective-permute-start | bytes 393224 | tf_op jit(solution)/shard_map/ppermute | solution.py:357
  182.5 5.2 %collective-permute-done.10 = bf16[256,256]{1,0:T(8,128)(2,1)S(1)} collective-permute-done((bf16[256,256]{1,0:T(8,128)(2,1)S(1)}, bf16[256,256]{1,0:T(8,128)(2,1)S(1)}, u32[]{:S(2)}, u32[]{:S(2)}) %collective-permute-start.10) | collective-permute-done | bytes 131104 | tf_op jit(solution)/shard_map/ppermute | solution.py:357
  187.7 0.7 broadcast_select_fusion
  188.4 3.9 %all-to-all-start.3 = ((bf16[4,64,256]{2,1,0:T(8,128)(2,1)}), bf16[4,64,256]{2,1,0:T(8,128)(2,1)S(1)}, u32[]{:S(2)}, u32[]{:S(2)}) async-start(bf16[4,64,256]{2,1,0:T(8,128)(2,1)} %bitcast.8), calls=%async_computation.3 | async-start | bytes 262144 | tf_op jit(solution)/shard_map/all_to_all | solution.py:359
  192.3 4.8 %all-to-all-done.3.heads = bf16[4,64,256]{2,1,0:T(8,128)(2,1)S(1)} async-done(((bf16[4,64,256]{2,1,0:T(8,128)(2,1)}), bf16[4,64,256]{2,1,0:T(8,128)(2,1)S(1)}, u32[]{:S(2)}, u32[]{:S(2)}) %all-to-all-start.3) | async-done | bytes 131104 | tf_op jit(solution)/shard_map/all_to_all | solution.py:359
  197.1 3.1 %project.1 = bf16[64,2048]{1,0:T(8,128)(2,1)} custom-call(s32[7]{0:T(128)S(1)} %stack.31.info.refs_0_, bf16[4,64,256]{2,1,0:T(8,128)(2,1)S(1)} %all-to-all-done.3.heads, bf16[256,2048]{1,0:T(8,128)(2,1)S(1)} %copy-done, bf16[256,2048]{1,0:T(8,128)(2,1)} %collective-permute-done.11.refs_1_, bf16[256,2048]{1,0:T(8,128)(2,1)S(1)} %collective-permute-done.12.refs_2_, ...), custom_call_target="tpu_custom_call" | custom-call | tf_op jit(solution)/shard_map/project/pallas_call | solution.py:297
  (21 shorter events, 0.2 us)
Async XLA Ops:
  2.0 4.2 %copy-start.1 = (bf16[2048,64]{0,1:T(8,128)(2,1)S(1)}, bf16[2048,64]{0,1:T(8,128)(2,1)}, u32[]{:S(2)}) copy-start(bf16[2048,64]{0,1:T(8,128)(2,1)} %param.9) | copy-start | bytes 786436
  2.0 4.4 %copy-start.2 = (bf16[2048,64]{0,1:T(8,128)(2,1)S(1)}, bf16[2048,64]{0,1:T(8,128)(2,1)}, u32[]{:S(2)}) copy-start(bf16[2048,64]{0,1:T(8,128)(2,1)} %param.10) | copy-start | bytes 786436
  2.1 18.4 %all-to-all-start = ((bf16[4,64,2048]{2,1,0:T(8,128)(2,1)}), bf16[4,64,2048]{2,1,0:T(8,128)(2,1)S(1)}, u32[]{:S(2)}, u32[]{:S(2)}) async-start(bf16[4,64,2048]{2,1,0:T(8,128)(2,1)} %broadcast_in_dim.16), calls=%async_computation | async-start | bytes 2097152 | tf_op jit(solution)/shard_map/all_to_all | solution.py:324
  6.2 0.7 copy-start.3
  20.4 6.5 %copy-start.4 = (f32[4]{0:T(128)S(1)}, f32[4]{0:T(128)}, u32[]{:S(2)}) copy-start(f32[4]{0:T(128)} %param.12) | copy-start | bytes 52
  23.1 4.7 %collective-permute-start = (bf16[260,256]{1,0:T(8,128)(2,1)S(1)}, bf16[260,256]{1,0:T(8,128)(2,1)S(1)}, u32[]{:S(2)}, u32[]{:S(2)}) collective-permute-start(bf16[260,256]{1,0:T(8,128)(2,1)S(1)} %slice.4), channel_id=1, source_target_pairs={{0,4},{4,0},{1,5},{5,1},{2,6},{6,2},{3,7},{7,3},{8,12},{12,8},{9,1... | collective-permute-start | bytes 399368 | tf_op jit(solution)/shard_map/ppermute | solution.py:328
  43.1 78.6 %copy-start = (bf16[256,2048]{1,0:T(8,128)(2,1)S(1)}, bf16[256,2048]{1,0:T(8,128)(2,1)}, u32[]{:S(2)}) copy-start(bf16[256,2048]{1,0:T(8,128)(2,1)} %refs_0_.1) | copy-start | bytes 3145732
  43.1 30.9 %all-to-all-start.2 = ((bf16[8,136,256]{2,1,0:T(8,128)(2,1)}), bf16[8,136,256]{2,1,0:T(8,128)(2,1)S(1)}, u32[]{:S(2)}, u32[]{:S(2)}) async-start(bf16[8,136,256]{2,1,0:T(8,128)(2,1)} %broadcast_in_dim.20), calls=%async_computation.2 | async-start | bytes 1114112 | tf_op jit(solution)/shard_map/all_to_all | solution.py:334
  52.6 12.9 %collective-permute-start.1 = (bf16[256,256]{1,0:T(8,128)(2,1)S(1)}, bf16[256,256]{1,0:T(8,128)(2,1)S(1)}, u32[]{:S(2)}, u32[]{:S(2)}) collective-permute-start(bf16[256,256]{1,0:T(8,128)(2,1)S(1)} %get-tuple-element.24), channel_id=1, source_target_pairs={{0,504},{4,508},{8,496},{12,500},{16,488},{20,492},{24,480},{28,48... | collective-permute-start | bytes 393224 | tf_op jit(solution)/shard_map/ppermute | solution.py:331
  75.0 15.8 %collective-permute-start.2 = (bf16[8,144,256]{2,1,0:T(8,128)(2,1)S(1)}, bf16[8,144,256]{2,1,0:T(8,128)(2,1)S(1)}, u32[]{:S(2)}, u32[]{:S(2)}) collective-permute-start(bf16[8,144,256]{2,1,0:T(8,128)(2,1)S(1)} %get-tuple-element.26.refs_2_), channel_id=1, source_target_pairs={{0,8},{8,16},{16,24},{24,32},{32,40},{40,48},{48,56},{56,0},{1,9},... | collective-permute-start | bytes 1769480 | tf_op jit(solution)/shard_map/ppermute | solution.py:344
  76.9 15.8 %collective-permute-start.3 = (bf16[8,144,256]{2,1,0:T(8,128)(2,1)S(1)}, bf16[8,144,256]{2,1,0:T(8,128)(2,1)S(1)}, u32[]{:S(2)}, u32[]{:S(2)}) collective-permute-start(bf16[8,144,256]{2,1,0:T(8,128)(2,1)S(1)} %get-tuple-element.26.refs_2_), channel_id=1, source_target_pairs={{0,56},{8,0},{16,8},{24,16},{32,24},{40,32},{48,40},{56,48},{1,57}... | collective-permute-start | bytes 1769480 | tf_op jit(solution)/shard_map/ppermute | solution.py:347
  90.8 14.9 %collective-permute-start.4 = (bf16[8,144,256]{2,1,0:T(8,128)(2,1)S(1)}, bf16[8,144,256]{2,1,0:T(8,128)(2,1)S(1)}, u32[]{:S(2)}, u32[]{:S(2)}) collective-permute-start(bf16[8,144,256]{2,1,0:T(8,128)(2,1)S(1)} %collective-permute-done.2.refs_2_), channel_id=1, source_target_pairs={{0,8},{8,16},{16,24},{24,32},{32,40},{40,48},{48,56},{56,0},{1,9},... | collective-permute-start | bytes 1769480 | tf_op jit(solution)/shard_map/ppermute | solution.py:344
  92.7 14.9 %collective-permute-start.5 = (bf16[8,144,256]{2,1,0:T(8,128)(2,1)S(1)}, bf16[8,144,256]{2,1,0:T(8,128)(2,1)S(1)}, u32[]{:S(2)}, u32[]{:S(2)}) collective-permute-start(bf16[8,144,256]{2,1,0:T(8,128)(2,1)S(1)} %collective-permute-done.3.refs_3_), channel_id=1, source_target_pairs={{0,56},{8,0},{16,8},{24,16},{32,24},{40,32},{48,40},{56,48},{1,57}... | collective-permute-start | bytes 1769480 | tf_op jit(solution)/shard_map/ppermute | solution.py:347
  105.7 14.1 %collective-permute-start.6 = (bf16[8,144,256]{2,1,0:T(8,128)(2,1)S(1)}, bf16[8,144,256]{2,1,0:T(8,128)(2,1)S(1)}, u32[]{:S(2)}, u32[]{:S(2)}) collective-permute-start(bf16[8,144,256]{2,1,0:T(8,128)(2,1)S(1)} %collective-permute-done.4.refs_2_), channel_id=1, source_target_pairs={{0,8},{8,16},{16,24},{24,32},{32,40},{40,48},{48,56},{56,0},{1,9},... | collective-permute-start | bytes 1769480 | tf_op jit(solution)/shard_map/ppermute | solution.py:344
  107.6 45.8 %collective-permute-start.7 = (bf16[8,144,256]{2,1,0:T(8,128)(2,1)S(1)}, bf16[8,144,256]{2,1,0:T(8,128)(2,1)S(1)}, u32[]{:S(2)}, u32[]{:S(2)}) collective-permute-start(bf16[8,144,256]{2,1,0:T(8,128)(2,1)S(1)} %collective-permute-done.5.refs_3_), channel_id=1, source_target_pairs={{0,56},{8,0},{16,8},{24,16},{32,24},{40,32},{48,40},{56,48},{1,57}... | collective-permute-start | bytes 1769480 | tf_op jit(solution)/shard_map/ppermute | solution.py:347
  119.8 42.9 %collective-permute-start.8 = (bf16[8,144,256]{2,1,0:T(8,128)(2,1)S(1)}, bf16[8,144,256]{2,1,0:T(8,128)(2,1)S(1)}, u32[]{:S(2)}, u32[]{:S(2)}) collective-permute-start(bf16[8,144,256]{2,1,0:T(8,128)(2,1)S(1)} %collective-permute-done.6.refs_2_), channel_id=1, source_target_pairs={{0,8},{8,16},{16,24},{24,32},{32,40},{40,48},{48,56},{56,0},{1,9},... | collective-permute-start | bytes 1769480 | tf_op jit(solution)/shard_map/ppermute | solution.py:344
  121.7 70.6 %collective-permute-start.12 = (bf16[256,2048]{1,0:T(8,128)(2,1)S(1)}, bf16[256,2048]{1,0:T(8,128)(2,1)S(1)}, u32[]{:S(2)}, u32[]{:S(2)}) collective-permute-start(bf16[256,2048]{1,0:T(8,128)(2,1)S(1)} %copy-done), channel_id=1, source_target_pairs={{0,3},{1,0},{2,1},{3,2},{4,7},{5,4},{6,5},{7,6},{8,11},{9,8},{10,9... | collective-permute-start | bytes 3145736 | tf_op jit(solution)/shard_map/ppermute | solution.py:337
  124.5 67.8 %collective-permute-start.11 = (bf16[256,2048]{1,0:T(8,128)(2,1)S(1)}, bf16[256,2048]{1,0:T(8,128)(2,1)}, u32[]{:S(2)}, u32[]{:S(2)}) collective-permute-start(bf16[256,2048]{1,0:T(8,128)(2,1)S(1)} %copy-done), channel_id=1, source_target_pairs={{0,1},{1,2},{2,3},{3,0},{4,5},{5,6},{6,7},{7,4},{8,9},{9,10},{10,1... | collective-permute-start | bytes 3145736 | tf_op jit(solution)/shard_map/ppermute | solution.py:337
  127.0 65.3 %collective-permute-start.13 = (bf16[256,2048]{1,0:T(8,128)(2,1)S(1)}, bf16[256,2048]{1,0:T(8,128)(2,1)}, u32[]{:S(2)}, u32[]{:S(2)}) collective-permute-start(bf16[256,2048]{1,0:T(8,128)(2,1)S(1)} %copy-done), channel_id=1, source_target_pairs={{0,2},{1,3},{2,0},{3,1},{4,6},{5,7},{6,4},{7,5},{8,10},{9,11},{10,... | collective-permute-start | bytes 3145736 | tf_op jit(solution)/shard_map/ppermute | solution.py:337
  168.4 8.4 %collective-permute-start.9 = (f32[264,256]{1,0:T(8,128)S(1)}, f32[264,256]{1,0:T(8,128)S(1)}, u32[]{:S(2)}, u32[]{:S(2)}) collective-permute-start(f32[264,256]{1,0:T(8,128)S(1)} %get-tuple-element.38), channel_id=1, source_target_pairs={{0,4},{4,0},{1,5},{5,1},{2,6},{6,2},{3,7},{7,3},{8,12},{12,8},{9,1... | collective-permute-start | bytes 811016 | tf_op jit(solution)/shard_map/ppermute | solution.py:354
  176.9 10.9 %collective-permute-start.10 = (bf16[256,256]{1,0:T(8,128)(2,1)S(1)}, bf16[256,256]{1,0:T(8,128)(2,1)S(1)}, u32[]{:S(2)}, u32[]{:S(2)}) collective-permute-start(bf16[256,256]{1,0:T(8,128)(2,1)S(1)} %finish.1), channel_id=1, source_target_pairs={{4,508},{12,500},{20,492},{28,484},{36,476},{44,468},{52,460},{60,... | collective-permute-start | bytes 393224 | tf_op jit(solution)/shard_map/ppermute | solution.py:357
  188.4 8.7 %all-to-all-start.3 = ((bf16[4,64,256]{2,1,0:T(8,128)(2,1)}), bf16[4,64,256]{2,1,0:T(8,128)(2,1)S(1)}, u32[]{:S(2)}, u32[]{:S(2)}) async-start(bf16[4,64,256]{2,1,0:T(8,128)(2,1)} %bitcast.8), calls=%async_computation.3 | async-start | bytes 262144 | tf_op jit(solution)/shard_map/all_to_all | solution.py:359

commit v6 on v5

--- a/solution.py
+++ b/solution.py
@@ -139,96 +139,113 @@
     for side in range(2):
         stat[side, 0:32] = jnp.zeros((32, blk), f32)
         stat[side, 32:64] = jnp.full((32, blk), LOW, f32)
-    for n in range(count):
-        kv = chunks[n]
-        col = lax.rem(info[3] + (steps_away[n] + cols), cols)
-        ahead = [jnp.clip((info[1 + side] - col + cols - 1) // cols, 0, rows) for side in range(2)]
-        diag = [(info[1 + side] - col) % cols == 0 for side in range(2)]
-        full = [jnp.where(diag[side], ahead[side], ahead[side] + 1) // 2 for side in range(2)]
-        steps = full[0] + full[1]
-
-        def place(it):
-            side = (it >= full[0]).astype(jnp.int32)
-            return side, jnp.clip(it - side * full[0], 0, rows // 2 - 1)
-
-        def load_keys(slot, jj, count):
+    columns = [lax.rem(info[3] + (away + cols), cols) for away in steps_away]
+    ahead = [[jnp.clip((info[1 + side] - col + cols - 1) // cols, 0, rows) for col in columns] for side in range(2)]
+    own = [[(info[1 + side] - col) % cols == 0 for col in columns] for side in range(2)]
+    if count == 2:
+        tiles = rows
+        diag = [o[0] | o[1] for o in own]
+        full = [jnp.where(o[0], x[0], jnp.where(o[1], x[1], jnp.maximum(x[0], x[1]))) for o, x in zip(own, ahead)]
+    else:
+        tiles = rows // 2
+        diag = [o[0] for o in own]
+        full = [jnp.where(o[0], x[0], x[0] + 1) // 2 for o, x in zip(own, ahead)]
+    steps = full[0] + full[1]
+
+    def half(jj, e):
+        return (e, jj) if count == 2 else (0, 2 * jj + e)
+
+    def limits(side):
+        return [jnp.where(side == 0, ahead[0][n], ahead[1][n]) for n in range(count)]
+
+    def place(it):
+        side = (it >= full[0]).astype(jnp.int32)
+        return side, jnp.clip(it - side * full[0], 0, tiles - 1)
+
+    def load_keys(slot, jj, counts):
+        for e in range(2):
+            n, j = half(jj, e)
+            kv = chunks[n]
+            marks = kv[j, 64:80, :].astype(f32)
+            marks = jnp.where((row16 == 12) & (j >= counts[n]), NEG, marks).astype(bf16)
+            keys[slot, e * blk:(e + 1) * blk] = jnp.concatenate([kv[j, 0:64, :], marks, kv[j, 80:128, :]], axis=0).T
+
+    def fused(nxt, cur, allowed=None):
+        if cur is not None:
+            slot, jj, side, h = cur
+            old = stat[side, 32 + 8 * h:40 + 8 * h]
+            new = jnp.maximum(old, jnp.max(tops[slot], axis=0, keepdims=True))
+            scale = jnp.exp(old - new)
+            mass = stat[side, 8 * h:8 * h + 8] * scale
+            out = jnp.zeros((64, blk), f32)
+        top = None
+        for e in range(2):
+            ps = []
+            for g in range(PIECES):
+                at = e * blk + g * size
+                if nxt is not None:
+                    s = dot(keys[nxt[1], at:at + size], rhs[nxt[2] * 4 + nxt[3]])
+                    if allowed is not None:
+                        s = jnp.where(allowed[at:at + size], s, NEG)
+                    scores[nxt[0], at:at + size] = s
+                    t = jnp.max(s.reshape(size // 8, 8, blk), axis=0)
+                    top = t if top is None else jnp.maximum(top, t)
+                if cur is not None:
+                    p = jnp.exp(scores[slot, at:at + size].reshape(size // 8, 8, blk) - new[None])
+                    mass = mass + jnp.sum(p, axis=0)
+                    ps.append(p.reshape(size, blk).astype(bf16))
+            if cur is not None:
+                n, j = half(jj, e)
+                out = out + dot(chunks[n][j, 80:144, :], jnp.concatenate(ps, axis=0))
+        if nxt is not None:
+            tops[nxt[0]] = top
+        if cur is not None:
+            stat[side, 8 * h:8 * h + 8] = mass
+            stat[side, 32 + 8 * h:40 + 8 * h] = new
+            a = acc[side, h * HEAD:(h + 1) * HEAD].reshape(8, 8, blk) * scale[None]
+            acc[side, h * HEAD:(h + 1) * HEAD] = a.reshape(64, blk) + out
+
+    @pl.when(steps > 0)
+    def _():
+        side, jj = place(0)
+        load_keys(0, jj, limits(side))
+        fused((0, 0, side, 0), None)
+
+        def body(it, carry):
+            slot = it & 1
+            side, jj = place(it)
+            side_next, jj_next = place(jnp.minimum(it + 1, steps - 1))
+            for h in range(4):
+                if h == LOADAT:
+                    load_keys(1 - slot, jj_next, limits(side_next))
+                nxt = ((h + 1) & 1, slot, side, h + 1) if h < 3 else (0, 1 - slot, side_next, 0)
+                fused(nxt, (h & 1, jj, side, h))
+            return carry
+
+        lax.fori_loop(0, steps, body, 0)
+
+    def edge(side, carry):
+        @pl.when(jnp.where(side == 0, diag[0], diag[1]))
+        def _():
+            chip = jnp.where(side == 0, info[1], info[2])
+            jj = jnp.clip(jnp.where(side == 0, full[0], full[1]), 0, tiles - 1)
+            par = jnp.where(side == 0, info[4], 1 - info[4])
+            qpos = (2 * chip + par) * blk + lax.broadcasted_iota(jnp.int32, (2 * blk, blk), 1)
+            row = lax.broadcasted_iota(jnp.int32, (2 * blk, blk), 0)
+            starts = []
             for e in range(2):
-                marks = kv[2 * jj + e, 64:80, :].astype(f32)
-                marks = jnp.where((row16 == 12) & (2 * jj + e >= count), NEG, marks).astype(bf16)
-                keys[slot, e * blk:(e + 1) * blk] = jnp.concatenate([kv[2 * jj + e, 0:64, :], marks, kv[2 * jj + e, 80:128, :]], axis=0).T
-
-        def fused(nxt, cur, allowed=None):
-            if cur is not None:
-                slot, jj, side, h = cur
-                old = stat[side, 32 + 8 * h:40 + 8 * h]
-                new = jnp.maximum(old, jnp.max(tops[slot], axis=0, keepdims=True))
-                scale = jnp.exp(old - new)
-                mass = stat[side, 8 * h:8 * h + 8] * scale
-                out = jnp.zeros((64, blk), f32)
-            top = None
-            for e in range(2):
-                ps = []
-                for g in range(PIECES):
-                    at = e * blk + g * size
-                    if nxt is not None:
-                        s = dot(keys[nxt[1], at:at + size], rhs[nxt[2] * 4 + nxt[3]])
-                        if allowed is not None:
-                            s = jnp.where(allowed[at:at + size], s, NEG)
-                        scores[nxt[0], at:at + size] = s
-                        t = jnp.max(s.reshape(size // 8, 8, blk), axis=0)
-                        top = t if top is None else jnp.maximum(top, t)
-                    if cur is not None:
-                        p = jnp.exp(scores[slot, at:at + size].reshape(size // 8, 8, blk) - new[None])
-                        mass = mass + jnp.sum(p, axis=0)
-                        ps.append(p.reshape(size, blk).astype(bf16))
-                if cur is not None:
-                    out = out + dot(kv[2 * jj + e, 80:144, :], jnp.concatenate(ps, axis=0))
-            if nxt is not None:
-                tops[nxt[0]] = top
-            if cur is not None:
-                stat[side, 8 * h:8 * h + 8] = mass
-                stat[side, 32 + 8 * h:40 + 8 * h] = new
-                a = acc[side, h * HEAD:(h + 1) * HEAD].reshape(8, 8, blk) * scale[None]
-                acc[side, h * HEAD:(h + 1) * HEAD] = a.reshape(64, blk) + out
-
-        @pl.when(steps > 0)
-        def _():
-            side, jj = place(0)
-            load_keys(0, jj, jnp.where(side == 0, ahead[0], ahead[1]))
-            fused((0, 0, side, 0), None)
-
-            def body(it, carry):
-                slot = it & 1
-                side, jj = place(it)
-                side_next, jj_next = place(jnp.minimum(it + 1, steps - 1))
-                for h in range(4):
-                    if h == LOADAT:
-                        load_keys(1 - slot, jj_next, jnp.where(side_next == 0, ahead[0], ahead[1]))
-                    nxt = ((h + 1) & 1, slot, side, h + 1) if h < 3 else (0, 1 - slot, side_next, 0)
-                    fused(nxt, (h & 1, jj, side, h))
-                return carry
-
-            lax.fori_loop(0, steps, body, 0)
-
-        def edge(side, carry):
-            @pl.when(jnp.where(side == 0, diag[0], diag[1]))
-            def _():
-                chip = jnp.where(side == 0, info[1], info[2])
-                jj = jnp.clip(jnp.where(side == 0, full[0], full[1]), 0, rows // 2 - 1)
-                par = jnp.where(side == 0, info[4], 1 - info[4])
-                qpos = (2 * chip + par) * blk + lax.broadcasted_iota(jnp.int32, (2 * blk, blk), 1)
-                row = lax.broadcasted_iota(jnp.int32, (2 * blk, blk), 0)
-                upper = (row >= blk).astype(jnp.int32)
-                kpos = row + upper * ((2 * cols - 1) * blk) + ((2 * jj * cols + col) * 2 + core) * blk
-                allowed = kpos <= qpos
-                load_keys(0, jj, rows)
-                fused((0, 0, side, 0), None, allowed)
-                for h in range(4):
-                    fused(((h + 1) & 1, 0, side, h + 1) if h < 3 else None, (h & 1, jj, side, h), allowed)
-
-            return carry
-
-        lax.fori_loop(0, 2, edge, 0)
+                n, j = half(jj, e)
+                starts.append((2 * (j * cols + columns[n]) + core - e) * blk)
+            kpos = row + jnp.where(row >= blk, starts[1], starts[0])
+            allowed = kpos <= qpos
+            load_keys(0, jj, [rows] * count)
+            fused((0, 0, side, 0), None, allowed)
+            for h in range(4):
+                fused(((h + 1) & 1, 0, side, h + 1) if h < 3 else None, (h & 1, jj, side, h), allowed)
+
+        return carry
+
+    lax.fori_loop(0, 2, edge, 0)
 
 
 def attend(info, rhs, chunks, steps_away, cols):

time: 201 us -> 197 us (0.980)
  Pallas kernels: 43.7 us -> 37.8 us
    pallas_call x5, Pallas kernels: 38 us -> 32 us  [attend(): pl.pallas_call(functools.partial(attend_kernel, steps_away=steps_away, ro...]
  transfers between devices with their start and end apart: 17 -> 17, of which waited for: 10 -> 10; matrix products, arithmetic and copies ran while one was open for 1% -> 1% of each run, Pallas kernels for 19% -> 17%
where the time goes in v6:
time: 197 us; the launch traced here: 196 us
  starting transfers between devices  69.3 us (35%)
  waiting for transfers between devices  67.2 us (34%)
  Pallas kernels  37.8 us (19%)
  blocking collectives  13.5 us (7%)
  local copies, waits for them, and re-layouts  4.22 us (2%)
  matrix products  2.68 us (1%)
    pallas_call x5, Pallas kernels, attend(): pl.pallas_call(functools.partial(attend_kernel, steps_away=steps_away, ro...  32 us
    ppermute x4, waiting for transfers between devices, shards(): up = lax.ppermute(up, 'sp_1', ring(cols, 1))  25.3 us
    ppermute x3, starting transfers between devices, shards(): down = lax.ppermute(down, 'sp_1', ring(cols, -1))  13.7 us
    all_to_all x1, blocking collectives, shards(): lax.all_to_all(jnp.broadcast_to(total, (cols, *total.shape)), 'sp_1', spl...  13.5 us
    all_to_all x1, waiting for transfers between devices, shards(): here = lax.all_to_all(copies, 'tp', split_axis=0, concat_axis=0, tiled=True)  13.2 us
    all_to_all x1, starting transfers between devices, shards(): lax.all_to_all(jnp.broadcast_to(payload, (rows, *payload.shape)), 'sp_0',...  9.54 us
    all_to_all x1, waiting for transfers between devices, shards(): lax.all_to_all(jnp.broadcast_to(payload, (rows, *payload.shape)), 'sp_0',...  8.46 us
    ppermute x3, starting transfers between devices, shards(): weights.append(lax.ppermute(w_output, 'tp', ring(4, shift)))  7.81 us
  transfers between devices with their start and end apart: 17, of which 10 were waited for; matrix products, arithmetic and copies ran while one was open for 1% of the time, Pallas kernels for 17%

profile of v6, /device:TPU:65, one launch (start us, length us, event | category | flops | bytes accessed | tf_op | source)
XLA Modules:
  0.0 195.7 jit_solution(1914854924303333697)
XLA Ops:
  0.0 2.0 %broadcast_in_dim.16 = bf16[4,64,2048]{2,1,0:T(8,128)(2,1)} broadcast(bf16[64,2048]{1,0:T(8,128)(2,1)} %param.7), dimensions={1,2} | broadcast | bytes 1310720 | tf_op jit(solution)/shard_map/broadcast_in_dim | solution.py:340
  2.1 4.1 %all-to-all-start = ((bf16[4,64,2048]{2,1,0:T(8,128)(2,1)}), bf16[4,64,2048]{2,1,0:T(8,128)(2,1)S(1)}, u32[]{:S(2)}, u32[]{:S(2)}) async-start(bf16[4,64,2048]{2,1,0:T(8,128)(2,1)} %broadcast_in_dim.16), calls=%async_computation | async-start | bytes 2097152 | tf_op jit(solution)/shard_map/all_to_all | solution.py:341
  6.2 0.3 copy.9
  6.5 0.3 copy.10
  6.8 0.1 copy-done.3
  6.9 0.4 copy.8
  7.3 13.2 %all-to-all-done = bf16[4,64,2048]{2,1,0:T(8,128)(2,1)S(1)} async-done(((bf16[4,64,2048]{2,1,0:T(8,128)(2,1)}), bf16[4,64,2048]{2,1,0:T(8,128)(2,1)S(1)}, u32[]{:S(2)}, u32[]{:S(2)}) %all-to-all-start) | async-done | bytes 1048608 | tf_op jit(solution)/shard_map/all_to_all | solution.py:341
  20.4 2.7 %fusion.8.mine = bf16[388,256]{1,0:T(8,128)(2,1)S(1)} fusion(bf16[256,2048]{1,0:T(8,128)(2,1)S(1)} %bitcast.10, bf16[2048,64]{1,0:T(8,128)(2,1)S(1)} %copy.10, bf16[2048,64]{1,0:T(8,128)(2,1)S(1)} %copy.9, bf16[2048,4]{1,0:T(8,128)(2,1)S(1)} %copy.8, bf16[2048,256]{1,0:T(8,128)(2,1)} %param.8), kind=kOutput, calls=%fused_computation.8 | convolution fusion | flops 413303808 | bytes 2836480 | tf_op jit(solution)/shard_map/dot_general | solution.py:344
  23.1 3.7 %collective-permute-start = (bf16[260,256]{1,0:T(8,128)(2,1)S(1)}, bf16[260,256]{1,0:T(8,128)(2,1)S(1)}, u32[]{:S(2)}, u32[]{:S(2)}) collective-permute-start(bf16[260,256]{1,0:T(8,128)(2,1)S(1)} %slice.4), channel_id=1, source_target_pairs={{0,4},{4,0},{1,5},{5,1},{2,6},{6,2},{3,7},{7,3},{8,12},{12,8},{9,1... | collective-permute-start | bytes 399368 | tf_op jit(solution)/shard_map/ppermute | solution.py:345
  26.9 0.1 broadcast_in_dim.17
  27.0 0.1 stack.31.info.refs_0_
  27.1 0.8 collective-permute-done.theirs
  27.9 0.8 sums.1
  28.7 13.5 %all_to_all.20.row = f32[8,8,128]{2,1,0:T(8,128)S(1)} all-to-all(f32[8,8,128]{2,1,0:T(8,128)S(1)} %broadcast_in_dim.19), channel_id=1, replica_groups=mesh['sp_0'=8,'sp_1'=8,'sp_2'=2,'tp'=4] {'sp_1'}, dimensions={0} | all-to-all | bytes 65536 | tf_op jit(solution)/shard_map/all_to_all | solution.py:349
  42.3 0.8 broadcast_in_dim.20
  43.1 9.5 %all-to-all-start.2 = ((bf16[8,136,256]{2,1,0:T(8,128)(2,1)}), bf16[8,136,256]{2,1,0:T(8,128)(2,1)S(1)}, u32[]{:S(2)}, u32[]{:S(2)}) async-start(bf16[8,136,256]{2,1,0:T(8,128)(2,1)} %broadcast_in_dim.20), calls=%async_computation.2 | async-start | bytes 1114112 | tf_op jit(solution)/shard_map/all_to_all | solution.py:351
  52.6 5.2 %collective-permute-start.1 = (bf16[256,256]{1,0:T(8,128)(2,1)S(1)}, bf16[256,256]{1,0:T(8,128)(2,1)S(1)}, u32[]{:S(2)}, u32[]{:S(2)}) collective-permute-start(bf16[256,256]{1,0:T(8,128)(2,1)S(1)} %get-tuple-element.24), channel_id=1, source_target_pairs={{0,504},{4,508},{8,496},{12,500},{16,488},{20,492},{24,480},{28,48... | collective-permute-start | bytes 393224 | tf_op jit(solution)/shard_map/ppermute | solution.py:348
  57.8 7.8 %collective-permute-done.1.crossed = bf16[256,256]{1,0:T(8,128)(2,1)S(1)} collective-permute-done((bf16[256,256]{1,0:T(8,128)(2,1)S(1)}, bf16[256,256]{1,0:T(8,128)(2,1)S(1)}, u32[]{:S(2)}, u32[]{:S(2)}) %collective-permute-start.1) | collective-permute-done | bytes 131104 | tf_op jit(solution)/shard_map/ppermute | solution.py:348
  65.6 8.5 %all-to-all-done.2.column = bf16[8,136,256]{2,1,0:T(8,128)(2,1)S(1)} async-done(((bf16[8,136,256]{2,1,0:T(8,128)(2,1)}), bf16[8,136,256]{2,1,0:T(8,128)(2,1)S(1)}, u32[]{:S(2)}, u32[]{:S(2)}) %all-to-all-start.2) | async-done | bytes 557088 | tf_op jit(solution)/shard_map/all_to_all | solution.py:351
  74.1 0.9 prepare.1
  75.0 1.9 collective-permute-start.2
  76.9 4.6 %collective-permute-start.3 = (bf16[8,144,256]{2,1,0:T(8,128)(2,1)S(1)}, bf16[8,144,256]{2,1,0:T(8,128)(2,1)S(1)}, u32[]{:S(2)}, u32[]{:S(2)}) collective-permute-start(bf16[8,144,256]{2,1,0:T(8,128)(2,1)S(1)} %get-tuple-element.26.refs_2_), channel_id=1, source_target_pairs={{0,56},{8,0},{16,8},{24,16},{32,24},{40,32},{48,40},{56,48},{1,57}... | collective-permute-start | bytes 1769480 | tf_op jit(solution)/shard_map/ppermute | solution.py:364
  81.5 9.3 %collective-permute-done.2.refs_2_ = bf16[8,144,256]{2,1,0:T(8,128)(2,1)S(1)} collective-permute-done((bf16[8,144,256]{2,1,0:T(8,128)(2,1)S(1)}, bf16[8,144,256]{2,1,0:T(8,128)(2,1)S(1)}, u32[]{:S(2)}, u32[]{:S(2)}) %collective-permute-start.2) | collective-permute-done | bytes 589856 | tf_op jit(solution)/shard_map/ppermute | solution.py:361
  90.8 1.9 collective-permute-start.4
  92.7 4.6 %collective-permute-start.5 = (bf16[8,144,256]{2,1,0:T(8,128)(2,1)S(1)}, bf16[8,144,256]{2,1,0:T(8,128)(2,1)S(1)}, u32[]{:S(2)}, u32[]{:S(2)}) collective-permute-start(bf16[8,144,256]{2,1,0:T(8,128)(2,1)S(1)} %collective-permute-done.3.refs_3_), channel_id=1, source_target_pairs={{0,56},{8,0},{16,8},{24,16},{32,24},{40,32},{48,40},{56,48},{1,57}... | collective-permute-start | bytes 1769480 | tf_op jit(solution)/shard_map/ppermute | solution.py:364
  97.3 8.4 %collective-permute-done.4.refs_2_ = bf16[8,144,256]{2,1,0:T(8,128)(2,1)S(1)} collective-permute-done((bf16[8,144,256]{2,1,0:T(8,128)(2,1)S(1)}, bf16[8,144,256]{2,1,0:T(8,128)(2,1)S(1)}, u32[]{:S(2)}, u32[]{:S(2)}) %collective-permute-start.4) | collective-permute-done | bytes 589856 | tf_op jit(solution)/shard_map/ppermute | solution.py:361
  105.7 1.9 collective-permute-start.6
  107.6 4.6 %collective-permute-start.7 = (bf16[8,144,256]{2,1,0:T(8,128)(2,1)S(1)}, bf16[8,144,256]{2,1,0:T(8,128)(2,1)S(1)}, u32[]{:S(2)}, u32[]{:S(2)}) collective-permute-start(bf16[8,144,256]{2,1,0:T(8,128)(2,1)S(1)} %collective-permute-done.5.refs_3_), channel_id=1, source_target_pairs={{0,56},{8,0},{16,8},{24,16},{32,24},{40,32},{48,40},{56,48},{1,57}... | collective-permute-start | bytes 1769480 | tf_op jit(solution)/shard_map/ppermute | solution.py:364
  112.2 7.6 %collective-permute-done.6.refs_2_ = bf16[8,144,256]{2,1,0:T(8,128)(2,1)S(1)} collective-permute-done((bf16[8,144,256]{2,1,0:T(8,128)(2,1)S(1)}, bf16[8,144,256]{2,1,0:T(8,128)(2,1)S(1)}, u32[]{:S(2)}, u32[]{:S(2)}) %collective-permute-start.6) | collective-permute-done | bytes 589856 | tf_op jit(solution)/shard_map/ppermute | solution.py:361
  119.8 1.9 collective-permute-start.8
  121.7 2.8 %collective-permute-start.12 = (bf16[256,2048]{1,0:T(8,128)(2,1)S(1)}, bf16[256,2048]{1,0:T(8,128)(2,1)S(1)}, u32[]{:S(2)}, u32[]{:S(2)}) collective-permute-start(bf16[256,2048]{1,0:T(8,128)(2,1)S(1)} %copy-done), channel_id=1, source_target_pairs={{0,3},{1,0},{2,1},{3,2},{4,7},{5,4},{6,5},{7,6},{8,11},{9,8},{10,9... | collective-permute-start | bytes 3145736 | tf_op jit(solution)/shard_map/ppermute | solution.py:354
  124.5 2.5 %collective-permute-start.11 = (bf16[256,2048]{1,0:T(8,128)(2,1)S(1)}, bf16[256,2048]{1,0:T(8,128)(2,1)}, u32[]{:S(2)}, u32[]{:S(2)}) collective-permute-start(bf16[256,2048]{1,0:T(8,128)(2,1)S(1)} %copy-done), channel_id=1, source_target_pairs={{0,1},{1,2},{2,3},{3,0},{4,5},{5,6},{6,7},{7,4},{8,9},{9,10},{10,1... | collective-permute-start | bytes 3145736 | tf_op jit(solution)/shard_map/ppermute | solution.py:354
  127.0 2.5 %collective-permute-start.13 = (bf16[256,2048]{1,0:T(8,128)(2,1)S(1)}, bf16[256,2048]{1,0:T(8,128)(2,1)}, u32[]{:S(2)}, u32[]{:S(2)}) collective-permute-start(bf16[256,2048]{1,0:T(8,128)(2,1)S(1)} %copy-done), channel_id=1, source_target_pairs={{0,2},{1,3},{2,0},{3,1},{4,6},{5,7},{6,4},{7,5},{8,10},{9,11},{10,... | collective-permute-start | bytes 3145736 | tf_op jit(solution)/shard_map/ppermute | solution.py:354
  129.5 5.1 %attend.5 = (f32[2,256,256]{2,1,0:T(8,128)S(1)}, f32[2,64,256]{2,1,0:T(8,128)S(1)}) custom-call(s32[7]{0:T(128)S(1)} %stack.31.info.refs_0_, bf16[8,128,256]{2,1,0:T(8,128)(2,1)S(1)} %get-tuple-element.25.refs_1_, bf16[8,144,256]{2,1,0:T(8,128)(2,1)S(1)} %get-tuple-element.26.refs_2_), custom_call_target="tpu_custom_call" | custom-call | tf_op jit(solution)/shard_map/attend/pallas_call | solution.py:253
  134.6 7.5 %attend.6 = (f32[2,256,256]{2,1,0:T(8,128)S(1)}, f32[2,64,256]{2,1,0:T(8,128)S(1)}) custom-call(s32[7]{0:T(128)S(1)} %stack.31.info.refs_0_, bf16[8,128,256]{2,1,0:T(8,128)(2,1)S(1)} %get-tuple-element.25.refs_1_, bf16[8,144,256]{2,1,0:T(8,128)(2,1)S(1)} %collective-permute-done.2.refs_2_, bf16[8,144,256]{2,1,0:T(8,128)(2,1)S(1)} %collective-permute-done.3.refs_3_), custom_call_target="tpu_custom_call" | custom-call | tf_op jit(solution)/shard_map/attend/pallas_call | solution.py:253
  142.1 7.3 %attend.7 = (f32[2,256,256]{2,1,0:T(8,128)S(1)}, f32[2,64,256]{2,1,0:T(8,128)S(1)}) custom-call(s32[7]{0:T(128)S(1)} %stack.31.info.refs_0_, bf16[8,128,256]{2,1,0:T(8,128)(2,1)S(1)} %get-tuple-element.25.refs_1_, bf16[8,144,256]{2,1,0:T(8,128)(2,1)S(1)} %collective-permute-done.4.refs_2_, bf16[8,144,256]{2,1,0:T(8,128)(2,1)S(1)} %collective-permute-done.5.refs_3_), custom_call_target="tpu_custom_call" | custom-call | tf_op jit(solution)/shard_map/attend/pallas_call | solution.py:253
  149.4 7.3 %attend.8 = (f32[2,256,256]{2,1,0:T(8,128)S(1)}, f32[2,64,256]{2,1,0:T(8,128)S(1)}) custom-call(s32[7]{0:T(128)S(1)} %stack.31.info.refs_0_, bf16[8,128,256]{2,1,0:T(8,128)(2,1)S(1)} %get-tuple-element.25.refs_1_, bf16[8,144,256]{2,1,0:T(8,128)(2,1)S(1)} %collective-permute-done.6.refs_2_, bf16[8,144,256]{2,1,0:T(8,128)(2,1)S(1)} %collective-permute-done.7.refs_3_), custom_call_target="tpu_custom_call" | custom-call | tf_op jit(solution)/shard_map/attend/pallas_call | solution.py:253
  156.7 4.9 %attend.9 = (f32[2,256,256]{2,1,0:T(8,128)S(1)}, f32[2,64,256]{2,1,0:T(8,128)S(1)}) custom-call(s32[7]{0:T(128)S(1)} %stack.31.info.refs_0_, bf16[8,128,256]{2,1,0:T(8,128)(2,1)S(1)} %get-tuple-element.25.refs_1_, bf16[8,144,256]{2,1,0:T(8,128)(2,1)S(1)} %collective-permute-done.8.refs_2_), custom_call_target="tpu_custom_call" | custom-call | tf_op jit(solution)/shard_map/attend/pallas_call | solution.py:253
  161.6 0.8 merge.1
  162.5 7.2 %collective-permute-start.9 = (f32[264,256]{1,0:T(8,128)S(1)}, f32[264,256]{1,0:T(8,128)S(1)}, u32[]{:S(2)}, u32[]{:S(2)}) collective-permute-start(f32[264,256]{1,0:T(8,128)S(1)} %get-tuple-element.38), channel_id=1, source_target_pairs={{0,4},{4,0},{1,5},{5,1},{2,6},{6,2},{3,7},{7,3},{8,12},{12,8},{9,1... | collective-permute-start | bytes 811016 | tf_op jit(solution)/shard_map/ppermute | solution.py:371
  169.7 1.2 collective-permute-done.9.got
  170.8 0.1 finish.1
  171.0 6.4 %collective-permute-start.10 = (bf16[256,256]{1,0:T(8,128)(2,1)S(1)}, bf16[256,256]{1,0:T(8,128)(2,1)S(1)}, u32[]{:S(2)}, u32[]{:S(2)}) collective-permute-start(bf16[256,256]{1,0:T(8,128)(2,1)S(1)} %finish.1), channel_id=1, source_target_pairs={{4,508},{12,500},{20,492},{28,484},{36,476},{44,468},{52,460},{60,... | collective-permute-start | bytes 393224 | tf_op jit(solution)/shard_map/ppermute | solution.py:374
  177.4 5.8 %collective-permute-done.10 = bf16[256,256]{1,0:T(8,128)(2,1)S(1)} collective-permute-done((bf16[256,256]{1,0:T(8,128)(2,1)S(1)}, bf16[256,256]{1,0:T(8,128)(2,1)S(1)}, u32[]{:S(2)}, u32[]{:S(2)}) %collective-permute-start.10) | collective-permute-done | bytes 131104 | tf_op jit(solution)/shard_map/ppermute | solution.py:374
  183.2 0.7 broadcast_select_fusion
  183.9 3.9 %all-to-all-start.3 = ((bf16[4,64,256]{2,1,0:T(8,128)(2,1)}), bf16[4,64,256]{2,1,0:T(8,128)(2,1)S(1)}, u32[]{:S(2)}, u32[]{:S(2)}) async-start(bf16[4,64,256]{2,1,0:T(8,128)(2,1)} %bitcast.8), calls=%async_computation.3 | async-start | bytes 262144 | tf_op jit(solution)/shard_map/all_to_all | solution.py:376
  187.8 4.8 %all-to-all-done.3.heads = bf16[4,64,256]{2,1,0:T(8,128)(2,1)S(1)} async-done(((bf16[4,64,256]{2,1,0:T(8,128)(2,1)}), bf16[4,64,256]{2,1,0:T(8,128)(2,1)S(1)}, u32[]{:S(2)}, u32[]{:S(2)}) %all-to-all-start.3) | async-done | bytes 131104 | tf_op jit(solution)/shard_map/all_to_all | solution.py:376
  192.6 3.1 %project.1 = bf16[64,2048]{1,0:T(8,128)(2,1)} custom-call(s32[7]{0:T(128)S(1)} %stack.31.info.refs_0_, bf16[4,64,256]{2,1,0:T(8,128)(2,1)S(1)} %all-to-all-done.3.heads, bf16[256,2048]{1,0:T(8,128)(2,1)S(1)} %copy-done, bf16[256,2048]{1,0:T(8,128)(2,1)} %collective-permute-done.11.refs_1_, bf16[256,2048]{1,0:T(8,128)(2,1)S(1)} %collective-permute-done.12.refs_2_, ...), custom_call_target="tpu_custom_call" | custom-call | tf_op jit(solution)/shard_map/project/pallas_call | solution.py:314
  (21 shorter events, 0.2 us)
Async XLA Ops:
  2.0 4.2 %copy-start.1 = (bf16[2048,64]{0,1:T(8,128)(2,1)S(1)}, bf16[2048,64]{0,1:T(8,128)(2,1)}, u32[]{:S(2)}) copy-start(bf16[2048,64]{0,1:T(8,128)(2,1)} %param.9) | copy-start | bytes 786436
  2.0 4.4 %copy-start.2 = (bf16[2048,64]{0,1:T(8,128)(2,1)S(1)}, bf16[2048,64]{0,1:T(8,128)(2,1)}, u32[]{:S(2)}) copy-start(bf16[2048,64]{0,1:T(8,128)(2,1)} %param.10) | copy-start | bytes 786436
  2.1 18.4 %all-to-all-start = ((bf16[4,64,2048]{2,1,0:T(8,128)(2,1)}), bf16[4,64,2048]{2,1,0:T(8,128)(2,1)S(1)}, u32[]{:S(2)}, u32[]{:S(2)}) async-start(bf16[4,64,2048]{2,1,0:T(8,128)(2,1)} %broadcast_in_dim.16), calls=%async_computation | async-start | bytes 2097152 | tf_op jit(solution)/shard_map/all_to_all | solution.py:341
  6.2 0.7 copy-start.3
  20.4 6.5 %copy-start.4 = (f32[4]{0:T(128)S(1)}, f32[4]{0:T(128)}, u32[]{:S(2)}) copy-start(f32[4]{0:T(128)} %param.12) | copy-start | bytes 52
  23.1 4.7 %collective-permute-start = (bf16[260,256]{1,0:T(8,128)(2,1)S(1)}, bf16[260,256]{1,0:T(8,128)(2,1)S(1)}, u32[]{:S(2)}, u32[]{:S(2)}) collective-permute-start(bf16[260,256]{1,0:T(8,128)(2,1)S(1)} %slice.4), channel_id=1, source_target_pairs={{0,4},{4,0},{1,5},{5,1},{2,6},{6,2},{3,7},{7,3},{8,12},{12,8},{9,1... | collective-permute-start | bytes 399368 | tf_op jit(solution)/shard_map/ppermute | solution.py:345
  43.1 78.6 %copy-start = (bf16[256,2048]{1,0:T(8,128)(2,1)S(1)}, bf16[256,2048]{1,0:T(8,128)(2,1)}, u32[]{:S(2)}) copy-start(bf16[256,2048]{1,0:T(8,128)(2,1)} %refs_0_.1) | copy-start | bytes 3145732
  43.1 30.9 %all-to-all-start.2 = ((bf16[8,136,256]{2,1,0:T(8,128)(2,1)}), bf16[8,136,256]{2,1,0:T(8,128)(2,1)S(1)}, u32[]{:S(2)}, u32[]{:S(2)}) async-start(bf16[8,136,256]{2,1,0:T(8,128)(2,1)} %broadcast_in_dim.20), calls=%async_computation.2 | async-start | bytes 1114112 | tf_op jit(solution)/shard_map/all_to_all | solution.py:351
  52.6 12.9 %collective-permute-start.1 = (bf16[256,256]{1,0:T(8,128)(2,1)S(1)}, bf16[256,256]{1,0:T(8,128)(2,1)S(1)}, u32[]{:S(2)}, u32[]{:S(2)}) collective-permute-start(bf16[256,256]{1,0:T(8,128)(2,1)S(1)} %get-tuple-element.24), channel_id=1, source_target_pairs={{0,504},{4,508},{8,496},{12,500},{16,488},{20,492},{24,480},{28,48... | collective-permute-start | bytes 393224 | tf_op jit(solution)/shard_map/ppermute | solution.py:348
  75.0 15.8 %collective-permute-start.2 = (bf16[8,144,256]{2,1,0:T(8,128)(2,1)S(1)}, bf16[8,144,256]{2,1,0:T(8,128)(2,1)S(1)}, u32[]{:S(2)}, u32[]{:S(2)}) collective-permute-start(bf16[8,144,256]{2,1,0:T(8,128)(2,1)S(1)} %get-tuple-element.26.refs_2_), channel_id=1, source_target_pairs={{0,8},{8,16},{16,24},{24,32},{32,40},{40,48},{48,56},{56,0},{1,9},... | collective-permute-start | bytes 1769480 | tf_op jit(solution)/shard_map/ppermute | solution.py:361
  76.9 15.8 %collective-permute-start.3 = (bf16[8,144,256]{2,1,0:T(8,128)(2,1)S(1)}, bf16[8,144,256]{2,1,0:T(8,128)(2,1)S(1)}, u32[]{:S(2)}, u32[]{:S(2)}) collective-permute-start(bf16[8,144,256]{2,1,0:T(8,128)(2,1)S(1)} %get-tuple-element.26.refs_2_), channel_id=1, source_target_pairs={{0,56},{8,0},{16,8},{24,16},{32,24},{40,32},{48,40},{56,48},{1,57}... | collective-permute-start | bytes 1769480 | tf_op jit(solution)/shard_map/ppermute | solution.py:364
  90.8 14.9 %collective-permute-start.4 = (bf16[8,144,256]{2,1,0:T(8,128)(2,1)S(1)}, bf16[8,144,256]{2,1,0:T(8,128)(2,1)S(1)}, u32[]{:S(2)}, u32[]{:S(2)}) collective-permute-start(bf16[8,144,256]{2,1,0:T(8,128)(2,1)S(1)} %collective-permute-done.2.refs_2_), channel_id=1, source_target_pairs={{0,8},{8,16},{16,24},{24,32},{32,40},{40,48},{48,56},{56,0},{1,9},... | collective-permute-start | bytes 1769480 | tf_op jit(solution)/shard_map/ppermute | solution.py:361
  92.7 14.9 %collective-permute-start.5 = (bf16[8,144,256]{2,1,0:T(8,128)(2,1)S(1)}, bf16[8,144,256]{2,1,0:T(8,128)(2,1)S(1)}, u32[]{:S(2)}, u32[]{:S(2)}) collective-permute-start(bf16[8,144,256]{2,1,0:T(8,128)(2,1)S(1)} %collective-permute-done.3.refs_3_), channel_id=1, source_target_pairs={{0,56},{8,0},{16,8},{24,16},{32,24},{40,32},{48,40},{56,48},{1,57}... | collective-permute-start | bytes 1769480 | tf_op jit(solution)/shard_map/ppermute | solution.py:364
  105.7 14.1 %collective-permute-start.6 = (bf16[8,144,256]{2,1,0:T(8,128)(2,1)S(1)}, bf16[8,144,256]{2,1,0:T(8,128)(2,1)S(1)}, u32[]{:S(2)}, u32[]{:S(2)}) collective-permute-start(bf16[8,144,256]{2,1,0:T(8,128)(2,1)S(1)} %collective-permute-done.4.refs_2_), channel_id=1, source_target_pairs={{0,8},{8,16},{16,24},{24,32},{32,40},{40,48},{48,56},{56,0},{1,9},... | collective-permute-start | bytes 1769480 | tf_op jit(solution)/shard_map/ppermute | solution.py:361
  107.6 41.8 %collective-permute-start.7 = (bf16[8,144,256]{2,1,0:T(8,128)(2,1)S(1)}, bf16[8,144,256]{2,1,0:T(8,128)(2,1)S(1)}, u32[]{:S(2)}, u32[]{:S(2)}) collective-permute-start(bf16[8,144,256]{2,1,0:T(8,128)(2,1)S(1)} %collective-permute-done.5.refs_3_), channel_id=1, source_target_pairs={{0,56},{8,0},{16,8},{24,16},{32,24},{40,32},{48,40},{56,48},{1,57}... | collective-permute-start | bytes 1769480 | tf_op jit(solution)/shard_map/ppermute | solution.py:364
  119.8 37.0 %collective-permute-start.8 = (bf16[8,144,256]{2,1,0:T(8,128)(2,1)S(1)}, bf16[8,144,256]{2,1,0:T(8,128)(2,1)S(1)}, u32[]{:S(2)}, u32[]{:S(2)}) collective-permute-start(bf16[8,144,256]{2,1,0:T(8,128)(2,1)S(1)} %collective-permute-done.6.refs_2_), channel_id=1, source_target_pairs={{0,8},{8,16},{16,24},{24,32},{32,40},{40,48},{48,56},{56,0},{1,9},... | collective-permute-start | bytes 1769480 | tf_op jit(solution)/shard_map/ppermute | solution.py:361
  121.7 66.1 %collective-permute-start.12 = (bf16[256,2048]{1,0:T(8,128)(2,1)S(1)}, bf16[256,2048]{1,0:T(8,128)(2,1)S(1)}, u32[]{:S(2)}, u32[]{:S(2)}) collective-permute-start(bf16[256,2048]{1,0:T(8,128)(2,1)S(1)} %copy-done), channel_id=1, source_target_pairs={{0,3},{1,0},{2,1},{3,2},{4,7},{5,4},{6,5},{7,6},{8,11},{9,8},{10,9... | collective-permute-start | bytes 3145736 | tf_op jit(solution)/shard_map/ppermute | solution.py:354
  124.5 63.3 %collective-permute-start.11 = (bf16[256,2048]{1,0:T(8,128)(2,1)S(1)}, bf16[256,2048]{1,0:T(8,128)(2,1)}, u32[]{:S(2)}, u32[]{:S(2)}) collective-permute-start(bf16[256,2048]{1,0:T(8,128)(2,1)S(1)} %copy-done), channel_id=1, source_target_pairs={{0,1},{1,2},{2,3},{3,0},{4,5},{5,6},{6,7},{7,4},{8,9},{9,10},{10,1... | collective-permute-start | bytes 3145736 | tf_op jit(solution)/shard_map/ppermute | solution.py:354
  127.0 60.8 %collective-permute-start.13 = (bf16[256,2048]{1,0:T(8,128)(2,1)S(1)}, bf16[256,2048]{1,0:T(8,128)(2,1)}, u32[]{:S(2)}, u32[]{:S(2)}) collective-permute-start(bf16[256,2048]{1,0:T(8,128)(2,1)S(1)} %copy-done), channel_id=1, source_target_pairs={{0,2},{1,3},{2,0},{3,1},{4,6},{5,7},{6,4},{7,5},{8,10},{9,11},{10,... | collective-permute-start | bytes 3145736 | tf_op jit(solution)/shard_map/ppermute | solution.py:354
  162.5 8.4 %collective-permute-start.9 = (f32[264,256]{1,0:T(8,128)S(1)}, f32[264,256]{1,0:T(8,128)S(1)}, u32[]{:S(2)}, u32[]{:S(2)}) collective-permute-start(f32[264,256]{1,0:T(8,128)S(1)} %get-tuple-element.38), channel_id=1, source_target_pairs={{0,4},{4,0},{1,5},{5,1},{2,6},{6,2},{3,7},{7,3},{8,12},{12,8},{9,1... | collective-permute-start | bytes 811016 | tf_op jit(solution)/shard_map/ppermute | solution.py:371
  171.0 12.2 %collective-permute-start.10 = (bf16[256,256]{1,0:T(8,128)(2,1)S(1)}, bf16[256,256]{1,0:T(8,128)(2,1)S(1)}, u32[]{:S(2)}, u32[]{:S(2)}) collective-permute-start(bf16[256,256]{1,0:T(8,128)(2,1)S(1)} %finish.1), channel_id=1, source_target_pairs={{4,508},{12,500},{20,492},{28,484},{36,476},{44,468},{52,460},{60,... | collective-permute-start | bytes 393224 | tf_op jit(solution)/shard_map/ppermute | solution.py:374
  183.9 8.7 %all-to-all-start.3 = ((bf16[4,64,256]{2,1,0:T(8,128)(2,1)}), bf16[4,64,256]{2,1,0:T(8,128)(2,1)S(1)}, u32[]{:S(2)}, u32[]{:S(2)}) async-start(bf16[4,64,256]{2,1,0:T(8,128)(2,1)} %bitcast.8), calls=%async_computation.3 | async-start | bytes 262144 | tf_op jit(solution)/shard_map/all_to_all | solution.py:376
